TPU v7x, 512 devices: a whole 4x4x16 slice. The times are simulated.
512 devices in a mesh: ep: 128 (over z, x, core), tp: 4 (over y).
Axes of the slice: x: 4, y: 4, z: 16, core: 2. Of those that a mesh axis runs over, the one named last changes fastest.
Arguments:
- tokens: bfloat16 [1024, 2048], P('ep'), may hold values from -6 to 6
- norm_gain: float32 [2048], replicated, may hold values from 0.1 to 1.9
- query_weight: bfloat16 [2048, 1024], P('ep', 'tp'), may hold values from -0.125 to 0.125
- key_weight: bfloat16 [2048, 512], P('ep', 'tp'), may hold values from -0.125 to 0.125
- value_weight: bfloat16 [2048, 512], P('ep', 'tp'), may hold values from -0.125 to 0.125
- query_gain: float32 [64], replicated, may hold values from 0.9 to 1.9
- key_gain: float32 [64], replicated, may hold values from 0.9 to 1.9
- lambdas: float32 [8], P('tp'), may hold values from 0.3 to 0.8
- key_cache: bfloat16 [1024, 4, 320, 128], P('ep', 'tp'), may hold values from -5 to 5
- value_cache: bfloat16 [1024, 4, 320, 128], P('ep', 'tp'), may hold values from -6 to 6
- lengths: int32 [1024], P('ep'), may hold values from 1 to 320
- head_gain: float32 [128], replicated, may hold values from 0.1 to 1.9
- out_weight: bfloat16 [1024, 2048], P('tp', 'ep'), may hold values from -0.1875 to 0.1875
- ffn_gain: float32 [2048], replicated, may hold values from 0.1 to 1.9
- dense_gate_weight: bfloat16 [2048, 1024], P('ep', 'tp'), may hold values from -0.125 to 0.125
- dense_up_weight: bfloat16 [2048, 1024], P('ep', 'tp'), may hold values from -0.125 to 0.125
- dense_down_weight: bfloat16 [1024, 2048], P('tp', 'ep'), may hold values from -0.1875 to 0.1875
- branch_gate: float32 [2048], replicated, may hold values from -0.125 to 0.125
- expert_ids: int32 [1024, 2], P('ep'), may hold values from 0 to 15, all different within a row; in each aligned block of 8 rows (0 to 7, 8 to 15, ...) at most 2 rows name the same one
- expert_probs: float32 [1024, 2], P('ep'), may hold values from 0.1 to 0.9
- expert_gate: bfloat16 [128, 2048, 704], P('ep', None, 'tp'), may hold values from -0.125 to 0.125
- expert_up: bfloat16 [128, 2048, 704], P('ep', None, 'tp'), may hold values from -0.125 to 0.125
- expert_down: bfloat16 [128, 704, 2048], P('ep', 'tp'), may hold values from -0.078125 to 0.078125
Outputs:
- mixed: bfloat16 [1024, 2048], P('ep', 'tp')
Inputs may be any that keep to these rules, and one draw needn't show every extreme that they name: `expert_ids`: each row names 2 different experts. Within each aligned block of 8 rows (the sequences of one index of ep) no expert is named more than 2 times, and in every draw some block names some expert exactly 2 times.
All inputs are finite; a program needn't handle non-finite values.
Results may differ from a plain program's by a relative error of at most 0.014.
Values may be sent and summed in bfloat16 or wider, within the bound.
No kernel may reach another device: no remote copies, remote signals or barrier semaphores. Data moves between devices by JAX's collectives and lax.ppermute only.
A program may use at most 64 MiB of HBM per device.

v0:
```python
import jax
import jax.numpy as jnp
from jax import lax
from jax.sharding import PartitionSpec as P

SUB = 64
VD = 128
EXPERTS = 16
TOP = 2
CAP = 2


epsilon = 1e-06


def rms_scale(values, scaling):
    return values * lax.rsqrt(jnp.mean(values * values, axis=-1, keepdims=True) + epsilon) * scaling


def project_rows(normed, weights):
    stacked = jnp.concatenate(weights, axis=1)
    spread = lax.all_to_all(normed, "ep", split_axis=1, concat_axis=0, tiled=True)
    return lax.psum_scatter(
        jnp.dot(spread, stacked, preferred_element_type=jnp.float32),
        "ep",
        scatter_dimension=0,
        tiled=True,
    )


def project_back(operand, weight):
    products = jnp.dot(
        lax.all_gather(operand, "ep", axis=0, tiled=True),
        weight,
        preferred_element_type=jnp.float32,
    ).astype(jnp.bfloat16)
    partial_value = lax.all_to_all(products, "ep", split_axis=0, concat_axis=1, tiled=True)
    return lax.psum(
        lax.optimization_barrier(partial_value).astype(jnp.float32).astype(jnp.bfloat16), "tp"
    ).astype(jnp.float32)


def attend(packed, key_cache, value_cache, lengths, query_gain, key_gain, lambdas, head_gain):
    seq_here = packed.shape[0]
    kv_here = key_cache.shape[1]
    cache_len = key_cache.shape[2]
    heads_here = lambdas.shape[0]
    per_group = heads_here // kv_here
    query_end = heads_here * 2 * SUB
    key_end = query_end + kv_here * 2 * SUB
    mixed = lax.optimization_barrier(packed.astype(jnp.bfloat16))
    query_parts = rms_scale(
        mixed[:, :query_end].astype(jnp.float32).reshape(seq_here, kv_here, per_group, 2, SUB),
        query_gain,
    ).astype(jnp.bfloat16)
    key_parts = rms_scale(
        mixed[:, query_end:key_end].astype(jnp.float32).reshape(seq_here, kv_here, 2, SUB), key_gain
    ).astype(jnp.bfloat16)
    new_values = mixed[:, key_end:].reshape(seq_here, kv_here, VD)
    cached = rms_scale(
        key_cache.astype(jnp.float32).reshape(seq_here, kv_here, cache_len, 2, SUB), key_gain
    ).astype(jnp.bfloat16)
    score_scale = SUB ** (-0.5)
    scores = (
        jnp.einsum("sgqcd,sgjcd->sgqcj", query_parts, cached, preferred_element_type=jnp.float32)
        * score_scale
    )
    own_score = (
        jnp.einsum("sgqcd,sgcd->sgqc", query_parts, key_parts, preferred_element_type=jnp.float32)
        * score_scale
    )
    live_mask = lax.broadcasted_iota(jnp.int32, (seq_here, cache_len), 1) < lengths[:, None]
    exponent = jnp.where(live_mask[:, None, None, None, :], jnp.exp(scores), 0.0)
    own_exponent = jnp.exp(own_score)
    denominator = jnp.sum(exponent, axis=4) + own_exponent
    shares = exponent / denominator[..., None]
    own_shares = own_exponent / denominator
    lam_heads = lambdas.reshape(1, kv_here, per_group)
    mixing = (shares[:, :, :, 0] - lam_heads[..., None] * shares[:, :, :, 1]).astype(jnp.bfloat16)
    own_mixing = lax.optimization_barrier(
        (own_shares[:, :, :, 0] - lam_heads * own_shares[:, :, :, 1]).astype(jnp.bfloat16)
    )
    head_out = jnp.einsum(
        "sgqj,sgje->sgqe", mixing, value_cache, preferred_element_type=jnp.float32
    )
    head_out = (
        head_out
        + own_mixing.astype(jnp.float32)[..., None] * new_values.astype(jnp.float32)[:, :, None, :]
    )
    return rms_scale(head_out, head_gain).astype(jnp.bfloat16).reshape(seq_here, heads_here * VD)


def route_tables(expert_ids, expert_probs):
    seq_here = expert_ids.shape[0]
    paired = expert_ids.reshape(-1)
    total_pairs = paired.shape[0]
    onehot = (paired[:, None] == lax.broadcasted_iota(jnp.int32, (total_pairs, EXPERTS), 1)).astype(
        jnp.float32
    )
    earlier = (
        lax.broadcasted_iota(jnp.int32, (total_pairs, total_pairs), 1)
        < lax.broadcasted_iota(jnp.int32, (total_pairs, total_pairs), 0)
    ).astype(jnp.float32)
    before = jnp.dot(earlier, onehot, precision=lax.Precision.HIGHEST)
    slot_ranks = jnp.sum(before * onehot, axis=1).astype(jnp.int32)
    slot_codes = (paired * CAP + slot_ranks).reshape(seq_here, TOP)
    slots_iota = lax.broadcasted_iota(jnp.int32, (seq_here, TOP, EXPERTS * CAP), 2)
    picked = (slot_codes[:, :, None] == slots_iota).astype(jnp.float32)
    select = jnp.sum(picked, axis=1)
    combine_weights = jnp.sum(picked * expert_probs[:, :, None], axis=1)
    return (select, combine_weights)


def mixture(ffn_input, expert_ids, expert_probs, expert_gate, expert_up, expert_down):
    here_count = expert_gate.shape[0]
    ep_count = lax.axis_size("ep")
    tp_count = lax.axis_size("tp")
    slot_count = ep_count * here_count
    rep_count = slot_count // EXPERTS
    model_width = ffn_input.shape[1]
    feature_share = model_width // tp_count
    select, combine_weights = route_tables(expert_ids, expert_probs)
    sent_width = ffn_input.shape[1]
    chosen = jnp.einsum(
        "sk,sd->kd", select.astype(jnp.bfloat16), ffn_input, preferred_element_type=jnp.float32
    ).astype(jnp.bfloat16)
    outgoing = jnp.broadcast_to(
        chosen.reshape(1, EXPERTS, CAP, sent_width), (rep_count, EXPERTS, CAP, sent_width)
    ).reshape(slot_count, CAP, sent_width)
    incoming = lax.all_to_all(outgoing, "ep", split_axis=0, concat_axis=0, tiled=True)
    grouped = incoming.reshape(ep_count, here_count, incoming.shape[1], model_width)
    gate_val = jnp.einsum(
        "ihcd,hdf->ihcf", grouped, expert_gate, preferred_element_type=jnp.float32
    )
    up_val = jnp.einsum("ihcd,hdf->ihcf", grouped, expert_up, preferred_element_type=jnp.float32)
    hidden = (jax.nn.silu(gate_val) * up_val).astype(jnp.bfloat16)
    partial_value = jnp.einsum(
        "ihcf,hfd->ihcd", hidden, expert_down, preferred_element_type=jnp.float32
    ).astype(jnp.bfloat16)
    summed = lax.all_to_all(partial_value, "tp", split_axis=3, concat_axis=0, tiled=True)
    block_out = jnp.sum(
        summed.reshape(tp_count, ep_count, here_count, CAP, feature_share).astype(jnp.float32),
        axis=0,
    ).astype(jnp.bfloat16)
    returned = lax.all_to_all(block_out, "ep", split_axis=0, concat_axis=0, tiled=True)
    expert_out = jnp.sum(
        returned.reshape(rep_count, EXPERTS * CAP, feature_share).astype(jnp.float32), axis=0
    )
    return jnp.dot(combine_weights, expert_out, precision=lax.Precision.HIGHEST)


def own_columns(values, tp_start, share_width):
    return lax.dynamic_slice_in_dim(values, tp_start, share_width, 1)


def shards(
    tokens,
    norm_gain,
    query_weight,
    key_weight,
    value_weight,
    query_gain,
    key_gain,
    lambdas,
    key_cache,
    value_cache,
    lengths,
    head_gain,
    out_weight,
    ffn_gain,
    dense_gate_weight,
    dense_up_weight,
    dense_down_weight,
    branch_gate,
    expert_ids,
    expert_probs,
    expert_gate,
    expert_up,
    expert_down,
):
    residual = tokens.astype(jnp.float32)
    normed = rms_scale(residual, norm_gain).astype(jnp.bfloat16)
    packed = project_rows(normed, (query_weight, key_weight, value_weight))
    head_out = attend(
        packed, key_cache, value_cache, lengths, query_gain, key_gain, lambdas, head_gain
    )
    attended = project_back(head_out, out_weight)
    middle = lax.optimization_barrier((residual + attended).astype(jnp.bfloat16))
    middle_f32 = middle.astype(jnp.float32)
    ffn_input = lax.optimization_barrier(rms_scale(middle_f32, ffn_gain).astype(jnp.bfloat16))
    dense_both = project_rows(ffn_input, (dense_gate_weight, dense_up_weight))
    half_width = dense_both.shape[1] // 2
    hidden = (jax.nn.silu(dense_both[:, :half_width]) * dense_both[:, half_width:]).astype(
        jnp.bfloat16
    )
    dense = project_back(hidden, dense_down_weight)
    branch_weight = jax.nn.sigmoid(
        jnp.sum(ffn_input.astype(jnp.float32) * branch_gate, axis=1, keepdims=True)
    )
    routed = mixture(ffn_input, expert_ids, expert_probs, expert_gate, expert_up, expert_down)
    share_width = routed.shape[1]
    tp_start = lax.axis_index("tp") * share_width
    combined = (
        own_columns(middle_f32, tp_start, share_width)
        + own_columns(branch_weight * dense, tp_start, share_width)
        + routed
    )
    return combined.astype(jnp.bfloat16)


def solution(mesh):
    return jax.shard_map(
        shards,
        mesh=mesh,
        in_specs=(
            P("ep", None),
            P(),
            P("ep", "tp"),
            P("ep", "tp"),
            P("ep", "tp"),
            P(),
            P(),
            P("tp"),
            P("ep", "tp", None, None),
            P("ep", "tp", None, None),
            P("ep"),
            P(),
            P("tp", "ep"),
            P(),
            P("ep", "tp"),
            P("ep", "tp"),
            P("tp", "ep"),
            P(),
            P("ep", None),
            P("ep", None),
            P("ep", None, "tp"),
            P("ep", None, "tp"),
            P("ep", "tp", None),
        ),
        out_specs=P("ep", "tp"),
        check_vma=False,
    )
```

profile of v0, /device:TPU:33, one launch (start us, length us, event | category | flops | bytes accessed | tf_op | source)
XLA Modules:
  0.0 908.0 jit_solution(11844619829971463060)
XLA Ops:
  6.5 1.0 fusion.32
  7.5 0.8 fusion.34
  8.3 0.2 all_to_all.71
  8.6 0.2 copy.97
  8.8 41.7 %all_to_all.98 = bf16[8,128,16]{2,0,1:T(8,128)(2,1)S(1)} all-to-all(bf16[8,128,16]{2,0,1:T(8,128)(2,1)S(1)} %copy.97), channel_id=1, replica_groups=mesh['ep'=128,'tp'=4] {'ep'}, dimensions={1} | all-to-all | bytes 65536 | tf_op jit(solution)/shard_map/all_to_all | solution.py:22
  50.4 2.5 fusion.24
  52.9 1.1 copy-done.2
  54.0 0.4 copy.96
  55.1 0.4 copy-done.17
  55.5 239.6 %reduce-scatter.3.cloned.1.call-done = f32[8,512]{1,0:T(8,128)} async-done(((f32[1024,512]{1,0:T(8,128)}), f32[8,512]{1,0:T(8,128)}) %reduce-scatter.3.cloned.1.call-update) | async-done | bytes 16400 | tf_op jit(solution)/shard_map/reduce_scatter | solution.py:23
  295.1 0.7 convert_element_type.143
  297.0 0.5 fusion.66
  298.0 0.3 multiply_reduce_fusion.2
  298.4 93.9 %all_gather.6 = bf16[1024,256]{1,0:T(8,128)(2,1)S(1)} all-gather(bf16[8,256]{1,0:T(8,128)(2,1)S(1)} %bitcast.148), channel_id=1, replica_groups=mesh['ep'=128,'tp'=4] {'ep'}, dimensions={0}, use_global_device_ids=true | all-gather | bytes 528384 | tf_op jit(solution)/shard_map/all_gather | solution.py:33
  392.3 0.2 convolution_convert_fusion.3
  392.6 0.9 copy.106
  393.4 12.8 %all-to-all-start.1 = ((bf16[128,8,16]{2,1,0:T(8,128)(2,1)}), bf16[128,8,16]{2,1,0:T(8,128)(2,1)S(1)}, u32[]{:S(2)}, u32[]{:S(2)}) async-start(bf16[128,8,16]{2,1,0:T(8,128)(2,1)} %bitcast.18), calls=%async_computation.2 | async-start | bytes 524288 | tf_op jit(solution)/shard_map/all_to_all | solution.py:37
  406.4 22.4 %all-to-all-done.1 = bf16[128,8,16]{2,1,0:T(8,128)(2,1)S(1)} async-done(((bf16[128,8,16]{2,1,0:T(8,128)(2,1)}), bf16[128,8,16]{2,1,0:T(8,128)(2,1)S(1)}, u32[]{:S(2)}, u32[]{:S(2)}) %all-to-all-start.1) | async-done | bytes 32800 | tf_op jit(solution)/shard_map/all_to_all | solution.py:37
  428.8 0.3 all_to_all.78
  429.2 13.3 %psum.14 = bf16[8,2048]{1,0:T(8,128)(2,1)S(1)} all-reduce(bf16[8,2048]{1,0:T(8,128)(2,1)S(1)} %all_to_all.78), channel_id=1, replica_groups=mesh['ep'=128,'tp'=4] {'tp'}, use_global_device_ids=true, to_apply=%region_7.8 | all-reduce | flops 16384 | bytes 65536 | tf_op jit(solution)/shard_map/psum | solution.py:38
  442.6 0.5 copy-done.3
  443.2 0.2 all_to_all.79
  443.4 0.9 copy.108
  444.3 9.9 %all-to-all-start.2 = ((bf16[8,128,16]{2,0,1:T(8,128)(2,1)}), bf16[8,128,16]{2,0,1:T(8,128)(2,1)S(1)}, u32[]{:S(2)}, u32[]{:S(2)}) async-start(bf16[8,128,16]{2,0,1:T(8,128)(2,1)} %copy.108), calls=%async_computation.3 | async-start | bytes 524288 | tf_op jit(solution)/shard_map/all_to_all | solution.py:22
  454.2 0.2 convolution_convert_fusion.1
  454.6 22.2 %all-to-all-done.2 = bf16[8,128,16]{2,0,1:T(8,128)(2,1)S(1)} async-done(((bf16[8,128,16]{2,0,1:T(8,128)(2,1)}), bf16[8,128,16]{2,0,1:T(8,128)(2,1)S(1)}, u32[]{:S(2)}, u32[]{:S(2)}) %all-to-all-start.2) | async-done | bytes 32800 | tf_op jit(solution)/shard_map/all_to_all | solution.py:22
  476.8 1.7 broadcast_in_dim.19
  478.5 6.2 all-to-all-start.4
  484.8 1.7 fusion.22
  486.5 53.7 %all-to-all-done.4 = bf16[128,2,2048]{2,1,0:T(2,128)(2,1)S(1)} async-done(((bf16[128,2,2048]{2,1,0:T(2,128)(2,1)}), bf16[128,2,2048]{2,1,0:T(2,128)(2,1)S(1)}, u32[]{:S(2)}, u32[]{:S(2)}) %all-to-all-start.4) | async-done | bytes 1048608 | tf_op jit(solution)/shard_map/all_to_all | solution.py:130
  540.3 1.5 convolution_bitcast_fusion.1
  541.8 2.4 fusion
  544.1 2.0 copy.116
  546.2 3.6 all-to-all-start.5
  549.8 190.6 %reduce-scatter.5.cloned.1.call-done = f32[8,512]{1,0:T(8,128)} async-done(((f32[1024,512]{1,0:T(8,128)}), f32[8,512]{1,0:T(8,128)}) %reduce-scatter.5.cloned.1.call-update) | async-done | bytes 16400 | tf_op jit(solution)/shard_map/reduce_scatter | solution.py:23
  740.4 0.7 fusion.50
  741.2 93.9 %all_gather.7 = bf16[1024,256]{1,0:T(8,128)(2,1)S(1)} all-gather(bf16[8,256]{1,0:T(8,128)(2,1)S(1)} %fusion.50), channel_id=1, replica_groups=mesh['ep'=128,'tp'=4] {'ep'}, dimensions={0}, use_global_device_ids=true | all-gather | bytes 528384 | tf_op jit(solution)/shard_map/all_gather | solution.py:33
  835.0 0.2 convolution_convert_fusion.2
  835.3 0.9 copy.109
  836.1 12.8 %all-to-all-start.3 = ((bf16[128,8,16]{2,1,0:T(8,128)(2,1)}), bf16[128,8,16]{2,1,0:T(8,128)(2,1)S(1)}, u32[]{:S(2)}, u32[]{:S(2)}) async-start(bf16[128,8,16]{2,1,0:T(8,128)(2,1)} %bitcast.22), calls=%async_computation.5 | async-start | bytes 524288 | tf_op jit(solution)/shard_map/all_to_all | solution.py:37
  849.0 1.6 reduce_sum.136
  850.7 1.0 copy.118
  851.7 19.8 %all-to-all-done.3 = bf16[128,8,16]{2,1,0:T(8,128)(2,1)S(1)} async-done(((bf16[128,8,16]{2,1,0:T(8,128)(2,1)}), bf16[128,8,16]{2,1,0:T(8,128)(2,1)S(1)}, u32[]{:S(2)}, u32[]{:S(2)}) %all-to-all-start.3) | async-done | bytes 32800 | tf_op jit(solution)/shard_map/all_to_all | solution.py:37
  871.5 6.2 all-to-all-start.6
  878.0 0.3 all_to_all.86
  878.3 14.5 %psum.15 = bf16[8,2048]{1,0:T(8,128)(2,1)S(1)} all-reduce(bf16[8,2048]{1,0:T(8,128)(2,1)S(1)} %all_to_all.86), channel_id=1, replica_groups=mesh['ep'=128,'tp'=4] {'tp'}, use_global_device_ids=true, to_apply=%region_11.12 | all-reduce | flops 16384 | bytes 65536 | tf_op jit(solution)/shard_map/psum | solution.py:38
  892.8 7.5 all-to-all-done.6
  900.4 0.8 fusion.6
  (104 shorter events, 3.6 us)
Async XLA Ops:
  6.5 535.2 %copy-start = (bf16[1,176,2048]{2,1,0:T(8,128)(2,1)S(1)}, bf16[1,176,2048]{2,1,0:T(8,128)(2,1)}, u32[]{:S(2)}) copy-start(bf16[1,176,2048]{2,1,0:T(8,128)(2,1)} %param.45) | copy-start | bytes 2162692
  6.5 288.6 %reduce-scatter.3.cloned.1.call-start = ((), (), s32[]{:S(2)}) async-start(), calls=%async_computation.9 | async-start | bytes 2113536 | tf_op jit(solution)/shard_map/reduce_scatter | solution.py:23
  52.9 1.1 copy-start.2
  52.9 1.5 copy-start.14
  54.8 0.7 copy-start.17
  54.8 241.8 %copy-start.18 = (f32[64]{0:T(128)S(1)}, f32[64]{0:T(128)}, u32[]{:S(2)}) copy-start(f32[64]{0:T(128)} %param.29) | copy-start | bytes 772
  54.8 241.9 %copy-start.16 = (f32[64]{0:T(128)S(1)}, f32[64]{0:T(128)}, u32[]{:S(2)}) copy-start(f32[64]{0:T(128)} %param.28) | copy-start | bytes 772
  54.9 242.7 %copy-start.20 = (f32[2]{0:T(128)S(1)}, f32[2]{0:T(128)}, u32[]{:S(2)}) copy-start(f32[2]{0:T(128)} %param.30) | copy-start | bytes 28
  55.4 242.5 %copy-start.22 = (bf16[8,1,320,128]{3,2,1,0:T(8,128)(2,1)S(1)}, bf16[8,1,320,128]{3,2,1,0:T(8,128)(2,1)}, u32[]{:S(2)}) copy-start(bf16[8,1,320,128]{3,2,1,0:T(8,128)(2,1)} %param.32) | copy-start | bytes 1966084
  55.4 242.9 %copy-start.19 = (f32[128]{0:T(128)S(1)}, f32[128]{0:T(128)}, u32[]{:S(2)}) copy-start(f32[128]{0:T(128)} %param.34) | copy-start | bytes 1540
  297.0 95.3 %copy-start.8 = (bf16[256,16]{0,1:T(8,128)(2,1)S(1)}, bf16[256,16]{0,1:T(8,128)(2,1)}, u32[]{:S(2)}) copy-start(bf16[256,16]{0,1:T(8,128)(2,1)} %param.35) | copy-start | bytes 24580
  297.5 108.9 %copy-start.15 = (f32[8,2]{0,1:T(2,128)S(1)}, f32[8,2]{0,1:T(2,128)}, u32[]{:S(2)}) copy-start(f32[8,2]{0,1:T(2,128)} %param.42) | copy-start | bytes 196
  298.3 144.2 %copy-start.7 = (bf16[8,2048]{1,0:T(8,128)(2,1)S(1)}, bf16[8,2048]{1,0:T(8,128)(2,1)}, u32[]{:S(2)}) copy-start(bf16[8,2048]{1,0:T(8,128)(2,1)} %param.23) | copy-start | bytes 98308
  298.3 144.8 %copy-start.12 = (f32[2048]{0:T(1024)S(1)}, f32[2048]{0:T(1024)}, u32[]{:S(2)}) copy-start(f32[2048]{0:T(1024)} %param.36) | copy-start | bytes 24580
  393.4 35.4 %all-to-all-start.1 = ((bf16[128,8,16]{2,1,0:T(8,128)(2,1)}), bf16[128,8,16]{2,1,0:T(8,128)(2,1)S(1)}, u32[]{:S(2)}, u32[]{:S(2)}) async-start(bf16[128,8,16]{2,1,0:T(8,128)(2,1)} %bitcast.18), calls=%async_computation.2 | async-start | bytes 524288 | tf_op jit(solution)/shard_map/all_to_all | solution.py:37
  442.5 0.6 copy-start.3
  443.2 35.3 %copy-start.5 = (bf16[8,2048]{1,0:T(8,128)(2,1)}, bf16[8,2048]{1,0:T(8,128)(2,1)S(1)}, u32[]{:S(2)}) copy-start(bf16[8,2048]{1,0:T(8,128)(2,1)S(1)} %multiply_convert_fusion.2) | copy-start | bytes 98308
  444.3 32.5 %all-to-all-start.2 = ((bf16[8,128,16]{2,0,1:T(8,128)(2,1)}), bf16[8,128,16]{2,0,1:T(8,128)(2,1)S(1)}, u32[]{:S(2)}, u32[]{:S(2)}) async-start(bf16[8,128,16]{2,0,1:T(8,128)(2,1)} %copy.108), calls=%async_computation.3 | async-start | bytes 524288 | tf_op jit(solution)/shard_map/all_to_all | solution.py:22
  454.6 30.2 %copy-start.9 = (bf16[16,256]{1,0:T(8,128)(2,1)S(1)}, bf16[16,256]{1,0:T(8,128)(2,1)}, u32[]{:S(2)}) copy-start(bf16[16,256]{1,0:T(8,128)(2,1)} %param.38) | copy-start | bytes 24580
  454.6 30.2 %copy-start.10 = (bf16[16,256]{1,0:T(8,128)(2,1)S(1)}, bf16[16,256]{1,0:T(8,128)(2,1)}, u32[]{:S(2)}) copy-start(bf16[16,256]{1,0:T(8,128)(2,1)} %param.37) | copy-start | bytes 24580
  478.5 61.8 %all-to-all-start.4 = ((bf16[128,2,2048]{2,1,0:T(2,128)(2,1)}), bf16[128,2,2048]{2,1,0:T(2,128)(2,1)S(1)}, u32[]{:S(2)}, u32[]{:S(2)}) async-start(bf16[128,2,2048]{2,1,0:T(2,128)(2,1)} %bitcast.24), calls=%async_computation.6 | async-start | bytes 2097152 | tf_op jit(solution)/shard_map/all_to_all | solution.py:130
  484.7 255.7 %reduce-scatter.5.cloned.1.call-start = ((), (), s32[]{:S(2)}) async-start(), calls=%async_computation.10 | async-start | bytes 2113536 | tf_op jit(solution)/shard_map/reduce_scatter | solution.py:23
  486.5 53.8 %copy-start.21 = (bf16[1,2048,176]{1,2,0:T(8,128)(2,1)S(1)}, bf16[1,2048,176]{1,2,0:T(8,128)(2,1)}, u32[]{:S(2)}) copy-start(bf16[1,2048,176]{1,2,0:T(8,128)(2,1)} %param.43) | copy-start | bytes 2162692
  486.5 55.2 %copy-start.1 = (bf16[1,2048,176]{1,2,0:T(8,128)(2,1)S(1)}, bf16[1,2048,176]{1,2,0:T(8,128)(2,1)}, u32[]{:S(2)}) copy-start(bf16[1,2048,176]{1,2,0:T(8,128)(2,1)} %param.44) | copy-start | bytes 2162692
  546.2 288.9 %copy-start.11 = (bf16[256,16]{0,1:T(8,128)(2,1)S(1)}, bf16[256,16]{0,1:T(8,128)(2,1)}, u32[]{:S(2)}) copy-start(bf16[256,16]{0,1:T(8,128)(2,1)} %param.39) | copy-start | bytes 24580
  546.2 290.0 %all-to-all-start.5 = ((bf16[128,1,2,2048]{0,2,1,3:T(2,128)(2,1)}), bf16[128,1,2,2048]{0,2,1,3:T(2,128)(2,1)S(1)}, u32[]{:S(2)}, u32[]{:S(2)}) async-start(bf16[128,1,2,2048]{0,2,1,3:T(2,128)(2,1)} %copy.116), calls=%async_computation.7 | async-start | bytes 2097152 | tf_op jit(solution)/shard_map/all_to_all | solution.py:140
  836.1 35.4 %all-to-all-start.3 = ((bf16[128,8,16]{2,1,0:T(8,128)(2,1)}), bf16[128,8,16]{2,1,0:T(8,128)(2,1)S(1)}, u32[]{:S(2)}, u32[]{:S(2)}) async-start(bf16[128,8,16]{2,1,0:T(8,128)(2,1)} %bitcast.22), calls=%async_computation.5 | async-start | bytes 524288 | tf_op jit(solution)/shard_map/all_to_all | solution.py:37
  849.0 28.8 %copy-start.4 = (bf16[8,2048]{1,0:T(8,128)(2,1)S(1)}, bf16[8,2048]{1,0:T(8,128)(2,1)}, u32[]{:S(2)}) copy-start(bf16[8,2048]{1,0:T(8,128)(2,1)} %copy-done.3) | copy-start | bytes 98308
  849.0 28.8 %copy-start.6 = (bf16[8,2048]{1,0:T(8,128)(2,1)S(1)}, bf16[8,2048]{1,0:T(8,128)(2,1)}, u32[]{:S(2)}) copy-start(bf16[8,2048]{1,0:T(8,128)(2,1)} %copy-done.5) | copy-start | bytes 98308
  849.0 28.8 %copy-start.13 = (f32[2048]{0:T(1024)S(1)}, f32[2048]{0:T(1024)}, u32[]{:S(2)}) copy-start(f32[2048]{0:T(1024)} %param.40) | copy-start | bytes 24580
  871.5 28.8 %all-to-all-start.6 = ((bf16[128,1,2,512]{3,2,1,0:T(2,128)(2,1)}), bf16[128,1,2,512]{3,2,1,0:T(2,128)(2,1)S(1)}, u32[]{:S(2)}, u32[]{:S(2)}) async-start(bf16[128,1,2,512]{3,2,1,0:T(2,128)(2,1)} %copy.118), calls=%async_computation.8 | async-start | bytes 524288 | tf_op jit(solution)/shard_map/all_to_all | solution.py:145
Sparse Core Ops, SparseCore 0:
  53.0 242.0 reduce-scatter.2
  490.1 250.2 reduce-scatter.4
where the time goes:
time: 909 us; the launch traced here: 908 us
  waiting for transfers between devices  556 us (61%)
  blocking collectives  257 us (28%)
  starting transfers between devices  51.6 us (6%)
  between operations  13.8 us (2%)
  local copies, waits for them, and re-layouts  12.5 us (1%)
  matrix products  10.6 us (1%)
    reduce_scatter x2, waiting for transfers between devices, project_rows(): lax.psum_scatter(jnp.dot(spread, stacked, preferred_element_type=jnp.floa...  430 us
    all_gather x2, blocking collectives, project_back(): lax.all_gather(operand, 'ep', axis=0, tiled=True)  188 us
    all_to_all x1, waiting for transfers between devices, mixture(): lax.all_to_all(outgoing, 'ep', split_axis=0, concat_axis=0, tiled=True)  53.7 us
    all_to_all x2, waiting for transfers between devices, project_back(): lax.all_to_all(products, 'ep', split_axis=0, concat_axis=1, tiled=True)  42.2 us
    all_to_all x1, blocking collectives, project_rows(): lax.all_to_all(normed, 'ep', split_axis=1, concat_axis=0, tiled=True)  41.7 us
    psum x2, blocking collectives, project_back(): lax.psum(lax.optimization_barrier(partial_value).astype(jnp.float32).asty...  27.8 us
    all_to_all x2, starting transfers between devices, project_back(): lax.all_to_all(products, 'ep', split_axis=0, concat_axis=1, tiled=True)  25.6 us
    all_to_all x1, waiting for transfers between devices, project_rows(): lax.all_to_all(normed, 'ep', split_axis=1, concat_axis=0, tiled=True)  22.2 us
  transfers between devices with their start and end apart: 8, of which 7 were waited for; matrix products, arithmetic and copies ran while one was open for 2% of the time, Pallas kernels for 0%

commit v1 on v0

v1 whole, which is shorter than its diff:
```python
import jax
import jax.numpy as jnp
from jax import lax
from jax.sharding import Mesh, PartitionSpec as P

SUB = 64
VD = 128
EXPERTS = 16
TOP = 2
CAP = 2


REP = 8
N_Z = 16
N_XC = 8
N_EP = 128
N_TP = 4
SEQ = 8
EP = ("b", "zp", "x", "c")
Z = ("b", "zp")
XC = ("x", "c")

epsilon = 1e-06


def rms_scale(values, scaling):
    return values * lax.rsqrt(jnp.mean(values * values, axis=-1, keepdims=True) + epsilon) * scaling


def exchange(values, axes):
    return lax.all_to_all(values, axes, split_axis=0, concat_axis=0, tiled=True)


def gather_small(values, axes, count):
    return exchange(jnp.broadcast_to(values[None], (count,) + values.shape), axes)


def to_mixed(rows):
    count = rows.shape[0]
    return rows.reshape(count, N_Z, N_XC, -1).transpose(0, 2, 1, 3).reshape(count, -1)


def from_mixed(rows):
    count = rows.shape[0]
    return rows.reshape(count, N_XC, N_Z, -1).transpose(0, 2, 1, 3).reshape(count, -1)


def attend(packed, key_cache, value_cache, lengths, query_gain, key_gain, lambdas, head_gain):
    seq_here = packed.shape[0]
    kv_here = key_cache.shape[1]
    cache_len = key_cache.shape[2]
    heads_here = lambdas.shape[0]
    per_group = heads_here // kv_here
    query_end = heads_here * 2 * SUB
    key_end = query_end + kv_here * 2 * SUB
    mixed = lax.optimization_barrier(packed.astype(jnp.bfloat16))
    query_parts = rms_scale(
        mixed[:, :query_end].astype(jnp.float32).reshape(seq_here, kv_here, per_group, 2, SUB),
        query_gain,
    ).astype(jnp.bfloat16)
    key_parts = rms_scale(
        mixed[:, query_end:key_end].astype(jnp.float32).reshape(seq_here, kv_here, 2, SUB), key_gain
    ).astype(jnp.bfloat16)
    new_values = mixed[:, key_end:].reshape(seq_here, kv_here, VD)
    cached = rms_scale(
        key_cache.astype(jnp.float32).reshape(seq_here, kv_here, cache_len, 2, SUB), key_gain
    ).astype(jnp.bfloat16)
    score_scale = SUB ** (-0.5)
    scores = (
        jnp.einsum("sgqcd,sgjcd->sgqcj", query_parts, cached, preferred_element_type=jnp.float32)
        * score_scale
    )
    own_score = (
        jnp.einsum("sgqcd,sgcd->sgqc", query_parts, key_parts, preferred_element_type=jnp.float32)
        * score_scale
    )
    live_mask = lax.broadcasted_iota(jnp.int32, (seq_here, cache_len), 1) < lengths[:, None]
    exponent = jnp.where(live_mask[:, None, None, None, :], jnp.exp(scores), 0.0)
    own_exponent = jnp.exp(own_score)
    denominator = jnp.sum(exponent, axis=4) + own_exponent
    shares = exponent / denominator[..., None]
    own_shares = own_exponent / denominator
    lam_heads = lambdas.reshape(1, kv_here, per_group)
    mixing = (shares[:, :, :, 0] - lam_heads[..., None] * shares[:, :, :, 1]).astype(jnp.bfloat16)
    own_mixing = lax.optimization_barrier(
        (own_shares[:, :, :, 0] - lam_heads * own_shares[:, :, :, 1]).astype(jnp.bfloat16)
    )
    head_out = jnp.einsum(
        "sgqj,sgje->sgqe", mixing, value_cache, preferred_element_type=jnp.float32
    )
    head_out = (
        head_out
        + own_mixing.astype(jnp.float32)[..., None] * new_values.astype(jnp.float32)[:, :, None, :]
    )
    return rms_scale(head_out, head_gain).astype(jnp.bfloat16).reshape(seq_here, heads_here * VD)


def route_tables(expert_ids, expert_probs):
    seq_here = expert_ids.shape[0]
    paired = expert_ids.reshape(-1)
    total_pairs = paired.shape[0]
    onehot = (paired[:, None] == lax.broadcasted_iota(jnp.int32, (total_pairs, EXPERTS), 1)).astype(
        jnp.float32
    )
    earlier = (
        lax.broadcasted_iota(jnp.int32, (total_pairs, total_pairs), 1)
        < lax.broadcasted_iota(jnp.int32, (total_pairs, total_pairs), 0)
    ).astype(jnp.float32)
    before = jnp.dot(earlier, onehot, precision=lax.Precision.HIGHEST)
    slot_ranks = jnp.sum(before * onehot, axis=1).astype(jnp.int32)
    slot_codes = (paired * CAP + slot_ranks).reshape(seq_here, TOP)
    slots_iota = lax.broadcasted_iota(jnp.int32, (seq_here, TOP, EXPERTS * CAP), 2)
    picked = (slot_codes[:, :, None] == slots_iota).astype(jnp.float32)
    select = jnp.sum(picked, axis=1)
    combine_weights = jnp.sum(picked * expert_probs[:, :, None], axis=1)
    return (select, combine_weights)


def own_columns(values, tp_start, share_width):
    return lax.dynamic_slice_in_dim(values, tp_start, share_width, 1)


def shards(
    tokens,
    norm_gain,
    query_weight,
    key_weight,
    value_weight,
    query_gain,
    key_gain,
    lambdas,
    key_cache,
    value_cache,
    lengths,
    head_gain,
    out_weight,
    ffn_gain,
    dense_gate_weight,
    dense_up_weight,
    dense_down_weight,
    branch_gate,
    expert_ids,
    expert_probs,
    expert_gate,
    expert_up,
    expert_down,
):
    residual = tokens.astype(jnp.float32)
    normed = rms_scale(residual, norm_gain).astype(jnp.bfloat16)
    width = residual.shape[1]
    share_width = width // N_TP
    tp_start = lax.axis_index("tp") * share_width

    spread = exchange(
        to_mixed(normed).reshape(SEQ, N_XC, width // N_XC).transpose(1, 0, 2), XC
    ).reshape(N_XC * SEQ, width // N_XC)
    shard = jnp.concatenate(
        (
            query_weight,
            key_weight,
            value_weight,
            out_weight.T,
            dense_gate_weight,
            dense_up_weight,
            dense_down_weight.T,
        ),
        axis=1,
    )
    held = lax.all_gather(shard, Z, axis=0, tiled=True)
    out_held = lax.all_gather(held[:, 512:768], XC, axis=0, tiled=True)
    dense_held = lax.all_gather(held[:, 768:], XC, axis=0, tiled=True)

    partial_rows = jnp.dot(spread, held[:, :512], preferred_element_type=jnp.float32)
    packed = jnp.sum(exchange(partial_rows.reshape(N_XC, SEQ, 512), XC), axis=0)
    head_out = attend(
        packed, key_cache, value_cache, lengths, query_gain, key_gain, lambdas, head_gain
    )
    attended_part = from_mixed(
        lax.dot_general(
            head_out, out_held, (((1,), (1,)), ((), ())), preferred_element_type=jnp.float32
        ).astype(jnp.bfloat16)
    )
    attended = jnp.sum(gather_small(attended_part, "tp", N_TP).astype(jnp.float32), axis=0)
    middle = lax.optimization_barrier((residual + attended).astype(jnp.bfloat16))
    middle_f32 = middle.astype(jnp.float32)
    ffn_input = lax.optimization_barrier(rms_scale(middle_f32, ffn_gain).astype(jnp.bfloat16))

    select, combine_weights = route_tables(expert_ids, expert_probs)
    ffn_share = own_columns(ffn_input, tp_start, share_width)
    chosen = jnp.dot(
        select.astype(jnp.bfloat16).T, ffn_share, preferred_element_type=jnp.float32
    ).astype(jnp.bfloat16)
    outgoing = jnp.broadcast_to(
        chosen.reshape(1, EXPERTS, CAP, share_width), (REP, EXPERTS, CAP, share_width)
    ).reshape(N_EP, CAP, share_width)
    incoming = exchange(outgoing, EP).reshape(N_EP * CAP, share_width)

    dense_both = jnp.dot(
        to_mixed(ffn_input), dense_held[:, :512], preferred_element_type=jnp.float32
    )
    dense_hidden = (jax.nn.silu(dense_both[:, :256]) * dense_both[:, 256:]).astype(jnp.bfloat16)
    dense_part = from_mixed(
        lax.dot_general(
            dense_hidden,
            dense_held[:, 512:],
            (((1,), (1,)), ((), ())),
            preferred_element_type=jnp.float32,
        ).astype(jnp.bfloat16)
    )
    branch_weight = jax.nn.sigmoid(
        jnp.sum(ffn_input.astype(jnp.float32) * branch_gate, axis=1, keepdims=True)
    )

    rows = gather_small(incoming, "tp", N_TP)
    rows = rows.transpose(1, 0, 2).reshape(N_EP * CAP, width)
    gate_val = jnp.dot(rows, expert_gate[0], preferred_element_type=jnp.float32)
    up_val = jnp.dot(rows, expert_up[0], preferred_element_type=jnp.float32)
    hidden = (jax.nn.silu(gate_val) * up_val).astype(jnp.bfloat16)
    expert_part = jnp.dot(hidden, expert_down[0], preferred_element_type=jnp.float32).astype(
        jnp.bfloat16
    )
    both_parts = jnp.concatenate((expert_part, dense_part), axis=0)
    both_parts = both_parts.reshape(N_EP * CAP + SEQ, N_TP, share_width).transpose(1, 0, 2)
    summed = jnp.sum(exchange(both_parts, "tp").astype(jnp.float32), axis=0)
    block_out = summed[: N_EP * CAP].astype(jnp.bfloat16).reshape(N_EP, CAP, share_width)
    dense = summed[N_EP * CAP :]
    returned = exchange(block_out, EP)
    expert_out = jnp.sum(
        returned.reshape(REP, EXPERTS * CAP, share_width).astype(jnp.float32), axis=0
    )
    routed = jnp.dot(combine_weights, expert_out, precision=lax.Precision.HIGHEST)
    combined = (
        own_columns(middle_f32, tp_start, share_width) + branch_weight * dense + routed
    )
    return combined.astype(jnp.bfloat16)


def solution(mesh):
    fine = Mesh(mesh.devices.reshape(8, 2, 4, 2, 4), ("b", "zp", "x", "c", "tp"))
    return jax.shard_map(
        shards,
        mesh=fine,
        in_specs=(
            P(EP, None),
            P(),
            P(EP, "tp"),
            P(EP, "tp"),
            P(EP, "tp"),
            P(),
            P(),
            P("tp"),
            P(EP, "tp", None, None),
            P(EP, "tp", None, None),
            P(EP),
            P(),
            P("tp", EP),
            P(),
            P(EP, "tp"),
            P(EP, "tp"),
            P("tp", EP),
            P(),
            P(EP, None),
            P(EP, None),
            P(EP, None, "tp"),
            P(EP, None, "tp"),
            P(EP, "tp", None),
        ),
        out_specs=P(EP, "tp"),
        check_vma=False,
    )
```

time: 909 us -> 217 us (0.24)
  waiting for transfers between devices: 556 us -> 50 us
  blocking collectives: 257 us -> 86.7 us
  starting transfers between devices: 51.6 us -> 31.1 us
    reduce_scatter x2 -> x0, waiting for transfers between devices: 430 us -> none  [project_rows(): lax.psum_scatter(jnp.dot(spread, stacked, preferred_element_type=jnp.floa...]
    all_gather x2 -> x1, blocking collectives: 188 us -> 30.8 us  [shards(): held = lax.all_gather(shard, Z, axis=0, tiled=True)]
    all_to_all x6 -> x5, waiting for transfers between devices: 126 us -> 47.6 us  [exchange(): return lax.all_to_all(values, axes, split_axis=0, concat_axis=0, tiled=True)]
    psum x2 -> x0, blocking collectives: 27.8 us -> none  [project_back(): lax.psum(lax.optimization_barrier(partial_value).astype(jnp.float32).asty...]
    all_to_all x6 -> x5, starting transfers between devices: 51.6 us -> 31.1 us  [exchange(): return lax.all_to_all(values, axes, split_axis=0, concat_axis=0, tiled=True)]
    all_to_all x1 -> x2, blocking collectives: 41.7 us -> 55.9 us  [exchange(): return lax.all_to_all(values, axes, split_axis=0, concat_axis=0, tiled=True)]
  transfers between devices with their start and end apart: 8 -> 7, of which waited for: 7 -> 6; matrix products, arithmetic and copies ran while one was open for 2% -> 10% of each run, Pallas kernels for 0% -> 0%
where the time goes in v1:
time: 217 us; the launch traced here: 216 us
  blocking collectives  86.7 us (40%)
  waiting for transfers between devices  50 us (23%)
  starting transfers between devices  31.1 us (14%)
  local copies, waits for them, and re-layouts  16.3 us (8%)
  between operations  13.9 us (6%)
  matrix products  13.4 us (6%)
  other arithmetic  4.68 us (2%)
    all_to_all x2, blocking collectives, exchange(): return lax.all_to_all(values, axes, split_axis=0, concat_axis=0, tiled=True)  55.9 us
    all_to_all x5, waiting for transfers between devices, exchange(): return lax.all_to_all(values, axes, split_axis=0, concat_axis=0, tiled=True)  47.6 us
    all_to_all x5, starting transfers between devices, exchange(): return lax.all_to_all(values, axes, split_axis=0, concat_axis=0, tiled=True)  31.1 us
    all_gather x1, blocking collectives, shards(): held = lax.all_gather(shard, Z, axis=0, tiled=True)  30.8 us
    unnamed x46, local copies, waits for them, and re-layouts  6.65 us
  transfers between devices with their start and end apart: 7, of which 6 were waited for; matrix products, arithmetic and copies ran while one was open for 10% of the time, Pallas kernels for 0%

profile of v1, /device:TPU:33, one launch (start us, length us, event | category | flops | bytes accessed | tf_op | source)
XLA Modules:
  0.0 216.1 jit_solution(8337824748790621756)
XLA Ops:
  6.5 0.8 constant_dynamic-update-slice_fusion.6
  7.3 0.7 constant_dynamic-update-slice_fusion.5
  8.0 0.7 constant_dynamic-update-slice_fusion.4
  8.7 0.7 constant_dynamic-update-slice_fusion.3
  9.4 0.7 constant_dynamic-update-slice_fusion.2
  10.1 0.7 constant_dynamic-update-slice_fusion.1
  10.8 0.7 constant_dynamic-update-slice_fusion
  11.5 30.8 %all_gather.9 = bf16[256,1536]{1,0:T(8,128)(2,1)S(1)} all-gather(bf16[16,1536]{1,0:T(8,128)(2,1)S(1)} %constant_dynamic-update-slice_fusion), channel_id=1, replica_groups=mesh['b'=8,'zp'=2,'x'=4,'c'=2,'tp'=4] {'b','zp'}, dimensions={0}, use_global_device_ids=true | all-gather | bytes 835584 | tf_op jit(solution)/shard_map/all_gather | solution.py:169
  42.3 0.7 slice.73
  43.0 0.9 fusion.25
  43.9 0.8 fusion.27
  44.7 0.2 reshape.334
  45.0 0.8 reshape_reshape.3
  45.8 11.8 %all-to-all-start = ((bf16[8,8,256]{2,1,0:T(8,128)(2,1)}), bf16[8,8,256]{2,1,0:T(8,128)(2,1)S(1)}, u32[]{:S(2)}, u32[]{:S(2)}) async-start(bf16[8,8,256]{2,1,0:T(8,128)(2,1)} %bitcast.3), calls=%async_computation | async-start | bytes 65536 | tf_op jit(solution)/shard_map/all_to_all | solution.py:31
  57.7 0.8 slice.74
  58.5 1.2 copy.94
  59.6 1.3 convert_multiply_fusion
  61.7 0.7 all-to-all-done
  62.4 0.8 fusion.18
  63.2 4.1 %all-to-all-start.1 = ((f32[8,8,512]{2,1,0:T(8,128)}), f32[8,8,512]{2,1,0:T(8,128)S(1)}, u32[]{:S(2)}, u32[]{:S(2)}) async-start(f32[8,8,512]{2,1,0:T(8,128)} %fusion.18), calls=%async_computation.1 | async-start | bytes 262144 | tf_op jit(solution)/shard_map/all_to_all | solution.py:31
  67.4 6.1 %all-to-all-done.1 = f32[8,8,512]{2,1,0:T(8,128)S(1)} async-done(((f32[8,8,512]{2,1,0:T(8,128)}), f32[8,8,512]{2,1,0:T(8,128)S(1)}, u32[]{:S(2)}, u32[]{:S(2)}) %all-to-all-start.1) | async-done | bytes 131104 | tf_op jit(solution)/shard_map/all_to_all | solution.py:31
  74.5 1.6 fusion.57
  76.6 0.3 multiply_reduce_fusion.2
  77.0 2.3 %all-gather.3.cloned.1.call-done = bf16[2048,256]{1,0:T(8,128)(2,1)} async-done(((bf16[256,256]{1,0:T(8,128)(2,1)}), bf16[2048,256]{1,0:T(8,128)(2,1)}) %all-gather.3.cloned.1.call-update) | async-done | bytes 1048592 | tf_op jit(solution)/shard_map/all_gather | solution.py:170
  79.4 1.6 convolution_convert_fusion.2
  80.9 0.2 reshape.339
  81.3 0.3 broadcast_in_dim.26
  81.6 0.7 broadcast_in_dim.27
  82.2 4.0 %all-to-all-start.2 = ((bf16[4,8,2048]{2,1,0:T(8,128)(2,1)}), bf16[4,8,2048]{2,1,0:T(8,128)(2,1)S(1)}, u32[]{:S(2)}, u32[]{:S(2)}) async-start(bf16[4,8,2048]{2,1,0:T(8,128)(2,1)} %broadcast_in_dim.27), calls=%async_computation.2 | async-start | bytes 262144 | tf_op jit(solution)/shard_map/all_to_all | solution.py:31
  86.3 4.7 %all-to-all-done.2 = bf16[4,8,2048]{2,1,0:T(8,128)(2,1)S(1)} async-done(((bf16[4,8,2048]{2,1,0:T(8,128)(2,1)}), bf16[4,8,2048]{2,1,0:T(8,128)(2,1)S(1)}, u32[]{:S(2)}, u32[]{:S(2)}) %all-to-all-start.2) | async-done | bytes 131104 | tf_op jit(solution)/shard_map/all_to_all | solution.py:31
  91.3 0.5 copy-done.3
  92.2 39.2 %all_to_all.35 = bf16[128,2,512]{2,1,0:T(2,128)(2,1)S(1)} all-to-all(bf16[128,2,512]{2,1,0:T(2,128)(2,1)S(1)} %bitcast.137), channel_id=1, replica_groups=mesh['b'=8,'zp'=2,'x'=4,'c'=2,'tp'=4] {'b','zp','x','c'}, dimensions={0} | all-to-all | bytes 524288 | tf_op jit(solution)/shard_map/all_to_all | solution.py:31
  131.6 1.1 broadcast_in_dim.31
  132.6 3.5 %all-to-all-start.4 = ((bf16[4,256,512]{1,2,0:T(8,128)(2,1)}), bf16[4,256,512]{1,2,0:T(8,128)(2,1)S(1)}, u32[]{:S(2)}, u32[]{:S(2)}) async-start(bf16[4,256,512]{1,2,0:T(8,128)(2,1)} %broadcast_in_dim.31), calls=%async_computation.4 | async-start | bytes 2097152 | tf_op jit(solution)/shard_map/all_to_all | solution.py:31
  136.4 0.9 reshape.343
  137.4 13.6 %all-to-all-done.4 = bf16[4,256,512]{1,2,0:T(8,128)(2,1)S(1)} async-done(((bf16[4,256,512]{1,2,0:T(8,128)(2,1)}), bf16[4,256,512]{1,2,0:T(8,128)(2,1)S(1)}, u32[]{:S(2)}, u32[]{:S(2)}) %all-to-all-start.4) | async-done | bytes 1048608 | tf_op jit(solution)/shard_map/all_to_all | solution.py:31
  151.0 2.1 fusion.15
  153.1 2.1 convolution_convert_fusion
  155.4 0.6 copy-done.8
  156.0 2.0 fusion
  157.9 1.6 convolution_convert_fusion.1
  159.5 0.2 reshape.344
  159.9 0.3 concatenate.13
  160.3 16.8 %all_to_all.36 = bf16[4,264,512]{2,1,0:T(8,128)(2,1)S(1)} all-to-all(bf16[4,264,512]{2,1,0:T(8,128)(2,1)S(1)} %maximum_bitcast_fusion), channel_id=1, replica_groups=mesh['b'=8,'zp'=2,'x'=4,'c'=2,'tp'=4] {'tp'}, dimensions={0} | all-to-all | bytes 2162688 | tf_op jit(solution)/shard_map/all_to_all | solution.py:31
  177.2 0.8 reshape.345
  178.0 7.7 %all-to-all-start.6 = ((bf16[128,2,512]{2,1,0:T(2,128)(2,1)}), bf16[128,2,512]{2,1,0:T(2,128)(2,1)S(1)}, u32[]{:S(2)}, u32[]{:S(2)}) async-start(bf16[128,2,512]{2,1,0:T(2,128)(2,1)} %reshape.345), calls=%async_computation.6 | async-start | bytes 524288 | tf_op jit(solution)/shard_map/all_to_all | solution.py:31
  185.9 22.4 %all-to-all-done.6 = bf16[128,2,512]{2,1,0:T(2,128)(2,1)S(1)} async-done(((bf16[128,2,512]{2,1,0:T(2,128)(2,1)}), bf16[128,2,512]{2,1,0:T(2,128)(2,1)S(1)}, u32[]{:S(2)}, u32[]{:S(2)}) %all-to-all-start.6) | async-done | bytes 262176 | tf_op jit(solution)/shard_map/all_to_all | solution.py:31
  208.5 0.8 fusion.5
  (106 shorter events, 4.3 us)
Async XLA Ops:
  6.5 146.6 %copy-start = (bf16[1,176,2048]{2,1,0:T(8,128)(2,1)S(1)}, bf16[1,176,2048]{2,1,0:T(8,128)(2,1)}, u32[]{:S(2)}) copy-start(bf16[1,176,2048]{2,1,0:T(8,128)(2,1)} %param.45) | copy-start | bytes 2162692
  6.5 72.8 %all-gather.3.cloned.1.call-start = ((), (), s32[]{:S(2)}) async-start(), calls=%async_computation.7 | async-start | bytes 1179648 | tf_op jit(solution)/shard_map/all_gather | solution.py:170
  42.3 16.2 %copy-start.2 = (bf16[8,1,320,128]{3,2,1,0:T(8,128)(2,1)S(1)}, bf16[8,1,320,128]{3,2,1,0:T(8,128)(2,1)}, u32[]{:S(2)}) copy-start(bf16[8,1,320,128]{3,2,1,0:T(8,128)(2,1)} %param.31) | copy-start | bytes 1966084
  45.8 16.5 %all-to-all-start = ((bf16[8,8,256]{2,1,0:T(8,128)(2,1)}), bf16[8,8,256]{2,1,0:T(8,128)(2,1)S(1)}, u32[]{:S(2)}, u32[]{:S(2)}) async-start(bf16[8,8,256]{2,1,0:T(8,128)(2,1)} %bitcast.3), calls=%async_computation | async-start | bytes 65536 | tf_op jit(solution)/shard_map/all_to_all | solution.py:31
  57.7 97.7 %all-gather.5.cloned.1.call-start = ((), (), s32[]{:S(2)}) async-start(), calls=%async_computation.8 | async-start | bytes 3538944 | tf_op jit(solution)/shard_map/all_gather | solution.py:171
  59.6 1.5 copy-start.11
  60.9 6.4 %copy-start.14 = (s32[8]{0:T(128)S(1)}, s32[8]{0:T(128)}, u32[]{:S(2)}) copy-start(s32[8]{0:T(128)} %param.33) | copy-start | bytes 100
  60.9 13.1 %copy-start.15 = (f32[64]{0:T(128)S(1)}, f32[64]{0:T(128)}, u32[]{:S(2)}) copy-start(f32[64]{0:T(128)} %param.29) | copy-start | bytes 772
  60.9 13.2 %copy-start.13 = (f32[64]{0:T(128)S(1)}, f32[64]{0:T(128)}, u32[]{:S(2)}) copy-start(f32[64]{0:T(128)} %param.28) | copy-start | bytes 772
  61.1 15.1 %copy-start.17 = (f32[2]{0:T(128)S(1)}, f32[2]{0:T(128)}, u32[]{:S(2)}) copy-start(f32[2]{0:T(128)} %param.30) | copy-start | bytes 28
  61.2 15.4 %copy-start.18 = (bf16[8,1,320,128]{3,2,1,0:T(8,128)(2,1)S(1)}, bf16[8,1,320,128]{3,2,1,0:T(8,128)(2,1)}, u32[]{:S(2)}) copy-start(bf16[8,1,320,128]{3,2,1,0:T(8,128)(2,1)} %param.32) | copy-start | bytes 1966084
  63.2 10.2 %all-to-all-start.1 = ((f32[8,8,512]{2,1,0:T(8,128)}), f32[8,8,512]{2,1,0:T(8,128)S(1)}, u32[]{:S(2)}, u32[]{:S(2)}) async-start(f32[8,8,512]{2,1,0:T(8,128)} %fusion.18), calls=%async_computation.1 | async-start | bytes 262144 | tf_op jit(solution)/shard_map/all_to_all | solution.py:31
  67.3 9.6 %copy-start.16 = (f32[128]{0:T(128)S(1)}, f32[128]{0:T(128)}, u32[]{:S(2)}) copy-start(f32[128]{0:T(128)} %param.34) | copy-start | bytes 1540
  76.6 9.7 %copy-start.12 = (f32[8,2]{0,1:T(2,128)S(1)}, f32[8,2]{0,1:T(2,128)}, u32[]{:S(2)}) copy-start(f32[8,2]{0,1:T(2,128)} %param.42) | copy-start | bytes 196
  76.9 14.2 %copy-start.7 = (bf16[8,2048]{1,0:T(8,128)(2,1)S(1)}, bf16[8,2048]{1,0:T(8,128)(2,1)}, u32[]{:S(2)}) copy-start(bf16[8,2048]{1,0:T(8,128)(2,1)} %param.23) | copy-start | bytes 98308
  76.9 14.8 %copy-start.9 = (f32[2048]{0:T(1024)S(1)}, f32[2048]{0:T(1024)}, u32[]{:S(2)}) copy-start(f32[2048]{0:T(1024)} %param.36) | copy-start | bytes 24580
  82.2 8.8 %all-to-all-start.2 = ((bf16[4,8,2048]{2,1,0:T(8,128)(2,1)}), bf16[4,8,2048]{2,1,0:T(8,128)(2,1)S(1)}, u32[]{:S(2)}, u32[]{:S(2)}) async-start(bf16[4,8,2048]{2,1,0:T(8,128)(2,1)} %broadcast_in_dim.27), calls=%async_computation.2 | async-start | bytes 262144 | tf_op jit(solution)/shard_map/all_to_all | solution.py:31
  91.1 0.6 copy-start.3
  91.8 44.3 %copy-start.5 = (bf16[8,2048]{1,0:T(8,128)(2,1)}, bf16[8,2048]{1,0:T(8,128)(2,1)S(1)}, u32[]{:S(2)}) copy-start(bf16[8,2048]{1,0:T(8,128)(2,1)S(1)} %multiply_convert_fusion.2) | copy-start | bytes 98308
  132.6 18.4 %all-to-all-start.4 = ((bf16[4,256,512]{1,2,0:T(8,128)(2,1)}), bf16[4,256,512]{1,2,0:T(8,128)(2,1)S(1)}, u32[]{:S(2)}, u32[]{:S(2)}) async-start(bf16[4,256,512]{1,2,0:T(8,128)(2,1)} %broadcast_in_dim.31), calls=%async_computation.4 | async-start | bytes 2097152 | tf_op jit(solution)/shard_map/all_to_all | solution.py:31
  136.2 17.0 %copy-start.1 = (bf16[1,2048,176]{1,2,0:T(8,128)(2,1)S(1)}, bf16[1,2048,176]{1,2,0:T(8,128)(2,1)}, u32[]{:S(2)}) copy-start(bf16[1,2048,176]{1,2,0:T(8,128)(2,1)} %param.44) | copy-start | bytes 2162692
  155.2 0.8 copy-start.8
  177.0 8.7 %copy-start.4 = (bf16[8,2048]{1,0:T(8,128)(2,1)S(1)}, bf16[8,2048]{1,0:T(8,128)(2,1)}, u32[]{:S(2)}) copy-start(bf16[8,2048]{1,0:T(8,128)(2,1)} %copy-done.3) | copy-start | bytes 98308
  177.0 8.8 %copy-start.6 = (bf16[8,2048]{1,0:T(8,128)(2,1)S(1)}, bf16[8,2048]{1,0:T(8,128)(2,1)}, u32[]{:S(2)}) copy-start(bf16[8,2048]{1,0:T(8,128)(2,1)} %copy-done.5) | copy-start | bytes 98308
  177.0 8.8 %copy-start.10 = (f32[2048]{0:T(1024)S(1)}, f32[2048]{0:T(1024)}, u32[]{:S(2)}) copy-start(f32[2048]{0:T(1024)} %param.40) | copy-start | bytes 24580
  178.0 30.3 %all-to-all-start.6 = ((bf16[128,2,512]{2,1,0:T(2,128)(2,1)}), bf16[128,2,512]{2,1,0:T(2,128)(2,1)S(1)}, u32[]{:S(2)}, u32[]{:S(2)}) async-start(bf16[128,2,512]{2,1,0:T(2,128)(2,1)} %reshape.345), calls=%async_computation.6 | async-start | bytes 524288 | tf_op jit(solution)/shard_map/all_to_all | solution.py:31
Sparse Core Ops, SparseCore 0:
  43.1 36.1 all-gather.2
  81.5 36.5 all-gather.4

commit v2 on v1

--- a/solution.py
+++ b/solution.py
@@ -27,6 +27,11 @@
     return values * lax.rsqrt(jnp.mean(values * values, axis=-1, keepdims=True) + epsilon) * scaling
 
 
+def mixed_scale(values, scaling):
+    mean = jnp.mean(values * values, axis=(0, 2), keepdims=True)
+    return values * lax.rsqrt(mean + epsilon) * scaling
+
+
 def exchange(values, axes):
     return lax.all_to_all(values, axes, split_axis=0, concat_axis=0, tiled=True)
 
@@ -37,12 +42,12 @@
 
 def to_mixed(rows):
     count = rows.shape[0]
-    return rows.reshape(count, N_Z, N_XC, -1).transpose(0, 2, 1, 3).reshape(count, -1)
+    return rows.reshape(count, N_Z, N_XC, -1).transpose(2, 0, 1, 3).reshape(N_XC, count, -1)
 
 
 def from_mixed(rows):
-    count = rows.shape[0]
-    return rows.reshape(count, N_XC, N_Z, -1).transpose(0, 2, 1, 3).reshape(count, -1)
+    count = rows.shape[1]
+    return rows.reshape(N_XC, count, N_Z, -1).transpose(1, 2, 0, 3).reshape(count, -1)
 
 
 def attend(packed, key_cache, value_cache, lengths, query_gain, key_gain, lambdas, head_gain):
@@ -113,7 +118,13 @@
     picked = (slot_codes[:, :, None] == slots_iota).astype(jnp.float32)
     select = jnp.sum(picked, axis=1)
     combine_weights = jnp.sum(picked * expert_probs[:, :, None], axis=1)
-    return (select, combine_weights)
+    lead_scale = jnp.sum(picked[:, 0] / expert_probs[:, :1], axis=0)
+    return (select, combine_weights, lead_scale)
+
+
+def split_pair(values):
+    high = lax.reduce_precision(values, 8, 7)
+    return high.astype(jnp.bfloat16), (values - high).astype(jnp.bfloat16)
 
 
 def own_columns(values, tp_start, share_width):
@@ -145,15 +156,15 @@
     expert_up,
     expert_down,
 ):
-    residual = tokens.astype(jnp.float32)
-    normed = rms_scale(residual, norm_gain).astype(jnp.bfloat16)
-    width = residual.shape[1]
+    width = tokens.shape[1]
     share_width = width // N_TP
     tp_start = lax.axis_index("tp") * share_width
-
-    spread = exchange(
-        to_mixed(normed).reshape(SEQ, N_XC, width // N_XC).transpose(1, 0, 2), XC
-    ).reshape(N_XC * SEQ, width // N_XC)
+    block = width // N_XC
+
+    residual = to_mixed(tokens).astype(jnp.float32)
+    normed = mixed_scale(residual, to_mixed(norm_gain[None])).astype(jnp.bfloat16)
+    with jax.named_scope("spread"):
+        spread = exchange(normed, XC).reshape(N_XC * SEQ, block)
     shard = jnp.concatenate(
         (
             query_weight,
@@ -166,73 +177,93 @@
         ),
         axis=1,
     )
-    held = lax.all_gather(shard, Z, axis=0, tiled=True)
-    out_held = lax.all_gather(held[:, 512:768], XC, axis=0, tiled=True)
-    dense_held = lax.all_gather(held[:, 768:], XC, axis=0, tiled=True)
+    with jax.named_scope("hold"):
+        held = lax.all_gather(shard, Z, axis=0, tiled=True)
 
     partial_rows = jnp.dot(spread, held[:, :512], preferred_element_type=jnp.float32)
-    packed = jnp.sum(exchange(partial_rows.reshape(N_XC, SEQ, 512), XC), axis=0)
+    with jax.named_scope("project"):
+        packed = jnp.sum(exchange(partial_rows.reshape(N_XC, SEQ, 512), XC), axis=0)
     head_out = attend(
         packed, key_cache, value_cache, lengths, query_gain, key_gain, lambdas, head_gain
     )
-    attended_part = from_mixed(
-        lax.dot_general(
-            head_out, out_held, (((1,), (1,)), ((), ())), preferred_element_type=jnp.float32
-        ).astype(jnp.bfloat16)
-    )
-    attended = jnp.sum(gather_small(attended_part, "tp", N_TP).astype(jnp.float32), axis=0)
-    middle = lax.optimization_barrier((residual + attended).astype(jnp.bfloat16))
-    middle_f32 = middle.astype(jnp.float32)
-    ffn_input = lax.optimization_barrier(rms_scale(middle_f32, ffn_gain).astype(jnp.bfloat16))
-
-    select, combine_weights = route_tables(expert_ids, expert_probs)
+    with jax.named_scope("heads"):
+        all_heads = gather_small(head_out, XC, N_XC).reshape(N_XC * SEQ, 256)
+    attended_part = lax.dot_general(
+        all_heads, held[:, 512:768], (((1,), (1,)), ((), ())), preferred_element_type=jnp.float32
+    ).astype(jnp.bfloat16)
+    with jax.named_scope("attended"):
+        parts = exchange(
+            jnp.broadcast_to(
+                attended_part.reshape(N_XC, 1, SEQ, block), (N_XC, N_TP, SEQ, block)
+            ).reshape(N_XC * N_TP, SEQ, block),
+            XC + ("tp",),
+        ).reshape(N_XC, N_TP, SEQ, block)
+    attended = jnp.sum(parts.astype(jnp.float32), axis=1)
+    middle_mixed = lax.optimization_barrier((residual + attended).astype(jnp.bfloat16))
+    ffn_input = from_mixed(
+        mixed_scale(middle_mixed.astype(jnp.float32), to_mixed(ffn_gain[None])).astype(jnp.bfloat16)
+    )
+    middle = from_mixed(middle_mixed).astype(jnp.float32)
+
+    select, combine_weights, lead_scale = route_tables(expert_ids, expert_probs)
+    scale_high, scale_low = split_pair(lead_scale)
+    tags = jnp.pad(jnp.stack((scale_high, scale_low), axis=1), ((0, 0), (0, 126)))
     ffn_share = own_columns(ffn_input, tp_start, share_width)
     chosen = jnp.dot(
         select.astype(jnp.bfloat16).T, ffn_share, preferred_element_type=jnp.float32
     ).astype(jnp.bfloat16)
+    chosen = jnp.concatenate((chosen, tags), axis=1)
+    sent = share_width + 128
     outgoing = jnp.broadcast_to(
-        chosen.reshape(1, EXPERTS, CAP, share_width), (REP, EXPERTS, CAP, share_width)
-    ).reshape(N_EP, CAP, share_width)
-    incoming = exchange(outgoing, EP).reshape(N_EP * CAP, share_width)
-
-    dense_both = jnp.dot(
-        to_mixed(ffn_input), dense_held[:, :512], preferred_element_type=jnp.float32
-    )
-    dense_hidden = (jax.nn.silu(dense_both[:, :256]) * dense_both[:, 256:]).astype(jnp.bfloat16)
-    dense_part = from_mixed(
-        lax.dot_general(
-            dense_hidden,
-            dense_held[:, 512:],
-            (((1,), (1,)), ((), ())),
-            preferred_element_type=jnp.float32,
-        ).astype(jnp.bfloat16)
-    )
+        chosen.reshape(1, EXPERTS, CAP, sent), (REP, EXPERTS, CAP, sent)
+    ).reshape(N_EP, CAP, sent)
+    with jax.named_scope("route"):
+        incoming = exchange(outgoing, EP).reshape(N_EP * CAP, sent)
+
+    rep_start = lax.axis_index("b") * 32
+    mine = jnp.concatenate(
+        [
+            lax.dynamic_slice_in_dim(held[:, start : start + 256], rep_start, 32, 1)
+            for start in (768, 1024, 1280)
+        ],
+        axis=1,
+    )
+    with jax.named_scope("dense"):
+        dense_held = lax.all_gather(mine, XC, axis=0, tiled=True)
+    dense_held = (
+        dense_held.reshape(N_XC, N_Z, 16, 96).transpose(1, 0, 2, 3).reshape(width, 96)
+    )
+
+    with jax.named_scope("join"):
+        rows = gather_small(incoming[:, :share_width], "tp", N_TP)
+    rows = rows.transpose(1, 0, 2).reshape(N_EP * CAP, width)
+    tag = incoming[:, share_width : share_width + 2].astype(jnp.float32)
     branch_weight = jax.nn.sigmoid(
-        jnp.sum(ffn_input.astype(jnp.float32) * branch_gate, axis=1, keepdims=True)
-    )
-
-    rows = gather_small(incoming, "tp", N_TP)
-    rows = rows.transpose(1, 0, 2).reshape(N_EP * CAP, width)
+        jnp.sum(rows.astype(jnp.float32) * branch_gate, axis=1, keepdims=True)
+    )
+    dense_scale = branch_weight * (tag[:, :1] + tag[:, 1:])
     gate_val = jnp.dot(rows, expert_gate[0], preferred_element_type=jnp.float32)
     up_val = jnp.dot(rows, expert_up[0], preferred_element_type=jnp.float32)
     hidden = (jax.nn.silu(gate_val) * up_val).astype(jnp.bfloat16)
-    expert_part = jnp.dot(hidden, expert_down[0], preferred_element_type=jnp.float32).astype(
-        jnp.bfloat16
-    )
-    both_parts = jnp.concatenate((expert_part, dense_part), axis=0)
-    both_parts = both_parts.reshape(N_EP * CAP + SEQ, N_TP, share_width).transpose(1, 0, 2)
-    summed = jnp.sum(exchange(both_parts, "tp").astype(jnp.float32), axis=0)
-    block_out = summed[: N_EP * CAP].astype(jnp.bfloat16).reshape(N_EP, CAP, share_width)
-    dense = summed[N_EP * CAP :]
-    returned = exchange(block_out, EP)
+    dense_both = jnp.dot(rows, dense_held[:, :64], preferred_element_type=jnp.float32)
+    dense_hidden = (
+        jax.nn.silu(dense_both[:, :32]) * dense_both[:, 32:] * dense_scale
+    ).astype(jnp.bfloat16)
+    down = jnp.concatenate((expert_down[0], dense_held[:, 64:].T), axis=0)
+    both_parts = jnp.dot(
+        jnp.concatenate((hidden, dense_hidden), axis=1), down, preferred_element_type=jnp.float32
+    ).astype(jnp.bfloat16)
+    both_parts = both_parts.reshape(N_EP * CAP, N_TP, share_width).transpose(1, 0, 2)
+    with jax.named_scope("reduce"):
+        summed = jnp.sum(exchange(both_parts, "tp").astype(jnp.float32), axis=0)
+    block_out = summed.astype(jnp.bfloat16).reshape(N_EP, CAP, share_width)
+    with jax.named_scope("return"):
+        returned = exchange(block_out, EP)
     expert_out = jnp.sum(
         returned.reshape(REP, EXPERTS * CAP, share_width).astype(jnp.float32), axis=0
     )
     routed = jnp.dot(combine_weights, expert_out, precision=lax.Precision.HIGHEST)
-    combined = (
-        own_columns(middle_f32, tp_start, share_width) + branch_weight * dense + routed
-    )
-    return combined.astype(jnp.bfloat16)
+    return (own_columns(middle, tp_start, share_width) + routed).astype(jnp.bfloat16)
 
 
 def solution(mesh):

time: 217 us -> 202 us (0.931)
  blocking collectives: 86.7 us -> 60.9 us
  starting transfers between devices: 31.1 us -> 49.8 us
  waiting for transfers between devices: 50 us -> 65.4 us
  between operations: 13.9 us -> 0.66 us
  matrix products: 13.4 us -> 7.83 us
  local copies, waits for them, and re-layouts: 16.3 us -> 11 us
    all_to_all x2 -> x1, blocking collectives: 55.9 us -> 17 us  [exchange(): return lax.all_to_all(values, axes, split_axis=0, concat_axis=0, tiled=True)]
    all_to_all x5 -> x7, starting transfers between devices: 31.1 us -> 49.8 us  [exchange(): return lax.all_to_all(values, axes, split_axis=0, concat_axis=0, tiled=True)]
    all_to_all x5 -> x7, waiting for transfers between devices: 47.6 us -> 65.4 us  [exchange(): return lax.all_to_all(values, axes, split_axis=0, concat_axis=0, tiled=True)]
    all_gather x0 -> x1, blocking collectives: none -> 13 us  [shards(): dense_held = lax.all_gather(mine, XC, axis=0, tiled=True)]
    unnamed x46 -> x49, local copies, waits for them, and re-layouts: 6.65 us -> 1.37 us
    dot_general x4, matrix products: 7.24 us -> 3.5 us  [the longest x1 1.57 us: shards(): jnp.dot(jnp.concatenate((hidden, dense_hidden), axis=1), down, preferred_...]
    all_gather x2 -> x0, waiting for transfers between devices: 2.35 us -> none  [the longest x1 2.33 us: shards(): out_held = lax.all_gather(held[:, 512:768], XC, axis=0, tiled=True)]
    convert_element_type x0 -> x6, local copies, waits for them, and re-layouts: none -> 2.18 us  [the longest x3 1.43 us: shards(): residual = to_mixed(tokens).astype(jnp.float32)]
  transfers between devices with their start and end apart: 7 -> 7, of which waited for: 6 -> 6; matrix products, arithmetic and copies ran while one was open for 10% -> 3% of each run, Pallas kernels for 0% -> 0%
where the time goes in v2:
time: 202 us; the launch traced here: 201 us
  waiting for transfers between devices  65.4 us (32%)
  blocking collectives  60.9 us (30%)
  starting transfers between devices  49.8 us (25%)
  local copies, waits for them, and re-layouts  11 us (5%)
  matrix products  7.83 us (4%)
  other arithmetic  5.35 us (3%)
    all_to_all x7, waiting for transfers between devices, exchange(): return lax.all_to_all(values, axes, split_axis=0, concat_axis=0, tiled=True)  65.4 us
    all_to_all x7, starting transfers between devices, exchange(): return lax.all_to_all(values, axes, split_axis=0, concat_axis=0, tiled=True)  49.8 us
    all_gather x1, blocking collectives, shards(): held = lax.all_gather(shard, Z, axis=0, tiled=True)  30.8 us
    all_to_all x1, blocking collectives, exchange(): return lax.all_to_all(values, axes, split_axis=0, concat_axis=0, tiled=True)  17 us
    all_gather x1, blocking collectives, shards(): dense_held = lax.all_gather(mine, XC, axis=0, tiled=True)  13 us
  transfers between devices with their start and end apart: 7, of which 6 were waited for; matrix products, arithmetic and copies ran while one was open for 3% of the time, Pallas kernels for 0%

profile of v2, /device:TPU:33, one launch (start us, length us, event | category | flops | bytes accessed | tf_op | source)
XLA Modules:
  0.0 200.9 jit_solution(4771035173444185747)
XLA Ops:
  0.1 1.1 reshape.416
  1.2 1.0 multiply_reduce_fusion.2
  2.2 0.2 reshape.411
  2.7 0.7 multiply_convert_fusion.3
  3.4 5.0 %all-to-all-start = ((bf16[8,8,256]{2,1,0:T(8,128)(2,1)}), bf16[8,8,256]{2,1,0:T(8,128)(2,1)S(1)}, u32[]{:S(2)}, u32[]{:S(2)}) async-start(bf16[8,8,256]{2,1,0:T(8,128)(2,1)} %multiply_convert_fusion.3), calls=%async_computation | async-start | bytes 65536 | tf_op jit(solution)/shard_map/spread/all_to_all | solution.py:36
  8.5 30.8 %all_gather.6 = bf16[256,1536]{1,0:T(8,128)(2,1)S(1)} all-gather(bf16[16,1536]{1,0:T(8,128)(2,1)S(1)} %constant_dynamic-update-slice_fusion), channel_id=1, replica_groups=mesh['b'=8,'zp'=2,'x'=4,'c'=2,'tp'=4] {'b','zp'}, dimensions={0}, use_global_device_ids=true | all-gather | bytes 835584 | tf_op jit(solution)/shard_map/hold/all_gather | solution.py:181
  39.3 1.2 copy.96
  40.5 1.3 convert_multiply_fusion
  42.7 0.8 fusion.19
  43.5 11.9 %all-to-all-start.1 = ((f32[8,8,512]{2,1,0:T(8,128)}), f32[8,8,512]{2,1,0:T(8,128)S(1)}, u32[]{:S(2)}, u32[]{:S(2)}) async-start(f32[8,8,512]{2,1,0:T(8,128)} %fusion.19), calls=%async_computation.1 | async-start | bytes 262144 | tf_op jit(solution)/shard_map/project/all_to_all | solution.py:36
  55.5 5.1 %all-to-all-done.1 = f32[8,8,512]{2,1,0:T(8,128)S(1)} async-done(((f32[8,8,512]{2,1,0:T(8,128)}), f32[8,8,512]{2,1,0:T(8,128)S(1)}, u32[]{:S(2)}, u32[]{:S(2)}) %all-to-all-start.1) | async-done | bytes 131104 | tf_op jit(solution)/shard_map/project/all_to_all | solution.py:36
  61.7 1.6 fusion.58
  63.8 0.4 multiply_reduce_fusion.3
  64.2 0.6 broadcast_in_dim.29
  64.8 4.1 %all-to-all-start.2 = ((bf16[8,8,256]{2,1,0:T(8,128)(2,1)}), bf16[8,8,256]{2,1,0:T(8,128)(2,1)S(1)}, u32[]{:S(2)}, u32[]{:S(2)}) async-start(bf16[8,8,256]{2,1,0:T(8,128)(2,1)} %broadcast_in_dim.29), calls=%async_computation.2 | async-start | bytes 65536 | tf_op jit(solution)/shard_map/heads/all_to_all | solution.py:36
  68.9 4.7 %all-to-all-done.2 = bf16[8,8,256]{2,1,0:T(8,128)(2,1)S(1)} async-done(((bf16[8,8,256]{2,1,0:T(8,128)(2,1)}), bf16[8,8,256]{2,1,0:T(8,128)(2,1)S(1)}, u32[]{:S(2)}, u32[]{:S(2)}) %all-to-all-start.2) | async-done | bytes 32800 | tf_op jit(solution)/shard_map/heads/all_to_all | solution.py:36
  73.7 0.2 fusion.3
  73.8 0.7 broadcast_in_dim.31
  74.5 5.9 %all-to-all-start.3 = ((bf16[32,8,256]{2,1,0:T(8,128)(2,1)}), bf16[32,8,256]{2,1,0:T(8,128)(2,1)S(1)}, u32[]{:S(2)}, u32[]{:S(2)}) async-start(bf16[32,8,256]{2,1,0:T(8,128)(2,1)} %bitcast.23), calls=%async_computation.3 | async-start | bytes 262144 | tf_op jit(solution)/shard_map/attended/all_to_all | solution.py:36
  80.9 7.2 %all-to-all-done.3 = bf16[32,8,256]{2,1,0:T(8,128)(2,1)S(1)} async-done(((bf16[32,8,256]{2,1,0:T(8,128)(2,1)}), bf16[32,8,256]{2,1,0:T(8,128)(2,1)S(1)}, u32[]{:S(2)}, u32[]{:S(2)}) %all-to-all-start.3) | async-done | bytes 131104 | tf_op jit(solution)/shard_map/attended/all_to_all | solution.py:36
  88.3 0.2 reshape.402
  88.5 0.2 copy.137
  88.7 0.3 reshape.403
  89.0 0.2 convolution_convert_fusion.1
  89.3 0.9 broadcast_in_dim.33
  90.1 11.1 %all-to-all-start.4 = ((bf16[128,2,640]{2,1,0:T(2,128)(2,1)}), bf16[128,2,640]{2,1,0:T(2,128)(2,1)S(1)}, u32[]{:S(2)}, u32[]{:S(2)}) async-start(bf16[128,2,640]{2,1,0:T(2,128)(2,1)} %bitcast.31), calls=%async_computation.4 | async-start | bytes 655360 | tf_op jit(solution)/shard_map/route/all_to_all | solution.py:36
  101.6 25.0 %all-to-all-done.4 = bf16[128,2,640]{2,1,0:T(2,128)(2,1)S(1)} async-done(((bf16[128,2,640]{2,1,0:T(2,128)(2,1)}), bf16[128,2,640]{2,1,0:T(2,128)(2,1)S(1)}, u32[]{:S(2)}, u32[]{:S(2)}) %all-to-all-start.4) | async-done | bytes 327712 | tf_op jit(solution)/shard_map/route/all_to_all | solution.py:36
  126.9 1.1 broadcast_in_dim.34
  127.9 3.6 %all-to-all-start.5 = ((bf16[4,256,512]{1,2,0:T(8,128)(2,1)}), bf16[4,256,512]{1,2,0:T(8,128)(2,1)S(1)}, u32[]{:S(2)}, u32[]{:S(2)}) async-start(bf16[4,256,512]{1,2,0:T(8,128)(2,1)} %broadcast_in_dim.34), calls=%async_computation.5 | async-start | bytes 2097152 | tf_op jit(solution)/shard_map/join/all_to_all | solution.py:36
  131.6 13.0 %all_gather.7 = bf16[2048,96]{1,0:T(8,128)(2,1)S(1)} all-gather(bf16[256,96]{1,0:T(8,128)(2,1)S(1)} %pad_maximum_fusion), channel_id=1, replica_groups=mesh['b'=8,'zp'=2,'x'=4,'c'=2,'tp'=4] {'x','c'}, dimensions={0}, use_global_device_ids=true | all-gather | bytes 442368 | tf_op jit(solution)/shard_map/dense/all_gather | solution.py:232
  144.7 0.2 slice_bitcast_fusion
  144.9 0.2 copy.114
  145.1 1.5 all-to-all-done.5
  146.7 0.3 fusion.17
  147.0 0.4 fusion.14
  147.4 0.4 multiply_reduce_fusion
  147.9 1.5 fusion
  149.3 0.2 fusion.21
  149.6 1.6 convolution_convert_fusion
  151.2 17.0 %all_to_all.40 = bf16[4,256,512]{2,1,0:T(8,128)(2,1)S(1)} all-to-all(bf16[4,256,512]{2,1,0:T(8,128)(2,1)S(1)} %bitcast.160), channel_id=1, replica_groups=mesh['b'=8,'zp'=2,'x'=4,'c'=2,'tp'=4] {'tp'}, dimensions={0} | all-to-all | bytes 2097152 | tf_op jit(solution)/shard_map/reduce/all_to_all | solution.py:36
  168.2 0.2 reduce_sum.167
  168.5 0.8 reshape.410
  169.3 8.2 %all-to-all-start.7 = ((bf16[128,2,512]{2,1,0:T(2,128)(2,1)}), bf16[128,2,512]{2,1,0:T(2,128)(2,1)S(1)}, u32[]{:S(2)}, u32[]{:S(2)}) async-start(bf16[128,2,512]{2,1,0:T(2,128)(2,1)} %reshape.410), calls=%async_computation.7 | async-start | bytes 524288 | tf_op jit(solution)/shard_map/return/all_to_all | solution.py:36
  177.4 0.2 reshape.417
  177.6 0.3 copy.104
  177.9 0.3 reshape.414
  178.2 21.8 %all-to-all-done.7 = bf16[128,2,512]{2,1,0:T(2,128)(2,1)S(1)} async-done(((bf16[128,2,512]{2,1,0:T(2,128)(2,1)}), bf16[128,2,512]{2,1,0:T(2,128)(2,1)S(1)}, u32[]{:S(2)}, u32[]{:S(2)}) %all-to-all-start.7) | async-done | bytes 262176 | tf_op jit(solution)/shard_map/return/all_to_all | solution.py:36
  200.1 0.8 fusion.4
  (125 shorter events, 4.5 us)
Async XLA Ops:
  0.0 147.0 %copy-start = (bf16[1,2048,176]{1,2,0:T(8,128)(2,1)S(1)}, bf16[1,2048,176]{1,2,0:T(8,128)(2,1)}, u32[]{:S(2)}) copy-start(bf16[1,2048,176]{1,2,0:T(8,128)(2,1)} %param.43) | copy-start | bytes 2162692
  0.0 2.5 %copy-start.2 = (f32[2048]{0:T(1024)S(1)}, f32[2048]{0:T(1024)}, u32[]{:S(2)}) copy-start(f32[2048]{0:T(1024)} %param.24) | copy-start | bytes 24580
  0.0 8.3 %copy-start.4 = (bf16[16,256]{1,0:T(8,128)(2,1)S(1)}, bf16[16,256]{1,0:T(8,128)(2,1)}, u32[]{:S(2)}) copy-start(bf16[16,256]{1,0:T(8,128)(2,1)} %param.25) | copy-start | bytes 24580
  0.0 8.3 %copy-start.10 = (bf16[16,128]{1,0:T(8,128)(2,1)S(1)}, bf16[16,128]{1,0:T(8,128)(2,1)}, u32[]{:S(2)}) copy-start(bf16[16,128]{1,0:T(8,128)(2,1)} %param.26) | copy-start | bytes 12292
  0.0 8.3 %copy-start.11 = (bf16[16,128]{1,0:T(8,128)(2,1)S(1)}, bf16[16,128]{1,0:T(8,128)(2,1)}, u32[]{:S(2)}) copy-start(bf16[16,128]{1,0:T(8,128)(2,1)} %param.27) | copy-start | bytes 12292
  0.0 8.4 %copy-start.5 = (bf16[256,16]{0,1:T(8,128)(2,1)S(1)}, bf16[256,16]{0,1:T(8,128)(2,1)}, u32[]{:S(2)}) copy-start(bf16[256,16]{0,1:T(8,128)(2,1)} %param.35) | copy-start | bytes 24580
  0.0 8.4 %copy-start.6 = (bf16[16,256]{1,0:T(8,128)(2,1)S(1)}, bf16[16,256]{1,0:T(8,128)(2,1)}, u32[]{:S(2)}) copy-start(bf16[16,256]{1,0:T(8,128)(2,1)} %param.37) | copy-start | bytes 24580
  0.1 8.4 %copy-start.7 = (bf16[16,256]{1,0:T(8,128)(2,1)S(1)}, bf16[16,256]{1,0:T(8,128)(2,1)}, u32[]{:S(2)}) copy-start(bf16[16,256]{1,0:T(8,128)(2,1)} %param.38) | copy-start | bytes 24580
  0.1 8.4 %copy-start.8 = (bf16[256,16]{0,1:T(8,128)(2,1)S(1)}, bf16[256,16]{0,1:T(8,128)(2,1)}, u32[]{:S(2)}) copy-start(bf16[256,16]{0,1:T(8,128)(2,1)} %param.39) | copy-start | bytes 24580
  1.2 38.2 %copy-start.1 = (bf16[8,1,320,128]{3,2,1,0:T(8,128)(2,1)S(1)}, bf16[8,1,320,128]{3,2,1,0:T(8,128)(2,1)}, u32[]{:S(2)}) copy-start(bf16[8,1,320,128]{3,2,1,0:T(8,128)(2,1)} %param.31) | copy-start | bytes 1966084
  3.4 39.3 %all-to-all-start = ((bf16[8,8,256]{2,1,0:T(8,128)(2,1)}), bf16[8,8,256]{2,1,0:T(8,128)(2,1)S(1)}, u32[]{:S(2)}, u32[]{:S(2)}) async-start(bf16[8,8,256]{2,1,0:T(8,128)(2,1)} %multiply_convert_fusion.3), calls=%async_computation | async-start | bytes 65536 | tf_op jit(solution)/shard_map/spread/all_to_all | solution.py:36
  40.5 1.5 copy-start.12
  40.5 2.1 %copy-start.15 = (s32[8]{0:T(128)S(1)}, s32[8]{0:T(128)}, u32[]{:S(2)}) copy-start(s32[8]{0:T(128)} %param.33) | copy-start | bytes 100
  41.8 13.7 %copy-start.13 = (f32[8,2]{0,1:T(2,128)S(1)}, f32[8,2]{0,1:T(2,128)}, u32[]{:S(2)}) copy-start(f32[8,2]{0,1:T(2,128)} %param.42) | copy-start | bytes 196
  41.8 19.5 %copy-start.16 = (f32[64]{0:T(128)S(1)}, f32[64]{0:T(128)}, u32[]{:S(2)}) copy-start(f32[64]{0:T(128)} %param.29) | copy-start | bytes 772
  41.8 19.6 %copy-start.14 = (f32[64]{0:T(128)S(1)}, f32[64]{0:T(128)}, u32[]{:S(2)}) copy-start(f32[64]{0:T(128)} %param.28) | copy-start | bytes 772
  42.0 21.4 %copy-start.18 = (f32[2]{0:T(128)S(1)}, f32[2]{0:T(128)}, u32[]{:S(2)}) copy-start(f32[2]{0:T(128)} %param.30) | copy-start | bytes 28
  42.0 21.7 %copy-start.19 = (bf16[8,1,320,128]{3,2,1,0:T(8,128)(2,1)S(1)}, bf16[8,1,320,128]{3,2,1,0:T(8,128)(2,1)}, u32[]{:S(2)}) copy-start(bf16[8,1,320,128]{3,2,1,0:T(8,128)(2,1)} %param.32) | copy-start | bytes 1966084
  43.5 17.2 %all-to-all-start.1 = ((f32[8,8,512]{2,1,0:T(8,128)}), f32[8,8,512]{2,1,0:T(8,128)S(1)}, u32[]{:S(2)}, u32[]{:S(2)}) async-start(f32[8,8,512]{2,1,0:T(8,128)} %fusion.19), calls=%async_computation.1 | async-start | bytes 262144 | tf_op jit(solution)/shard_map/project/all_to_all | solution.py:36
  55.4 8.7 %copy-start.17 = (f32[128]{0:T(128)S(1)}, f32[128]{0:T(128)}, u32[]{:S(2)}) copy-start(f32[128]{0:T(128)} %param.34) | copy-start | bytes 1540
  61.7 18.8 %copy-start.3 = (f32[2048]{0:T(1024)S(1)}, f32[2048]{0:T(1024)}, u32[]{:S(2)}) copy-start(f32[2048]{0:T(1024)} %param.36) | copy-start | bytes 24580
  64.8 8.8 %all-to-all-start.2 = ((bf16[8,8,256]{2,1,0:T(8,128)(2,1)}), bf16[8,8,256]{2,1,0:T(8,128)(2,1)S(1)}, u32[]{:S(2)}, u32[]{:S(2)}) async-start(bf16[8,8,256]{2,1,0:T(8,128)(2,1)} %broadcast_in_dim.29), calls=%async_computation.2 | async-start | bytes 65536 | tf_op jit(solution)/shard_map/heads/all_to_all | solution.py:36
  74.5 13.5 %all-to-all-start.3 = ((bf16[32,8,256]{2,1,0:T(8,128)(2,1)}), bf16[32,8,256]{2,1,0:T(8,128)(2,1)S(1)}, u32[]{:S(2)}, u32[]{:S(2)}) async-start(bf16[32,8,256]{2,1,0:T(8,128)(2,1)} %bitcast.23), calls=%async_computation.3 | async-start | bytes 262144 | tf_op jit(solution)/shard_map/attended/all_to_all | solution.py:36
  90.1 36.4 %all-to-all-start.4 = ((bf16[128,2,640]{2,1,0:T(2,128)(2,1)}), bf16[128,2,640]{2,1,0:T(2,128)(2,1)S(1)}, u32[]{:S(2)}, u32[]{:S(2)}) async-start(bf16[128,2,640]{2,1,0:T(2,128)(2,1)} %bitcast.31), calls=%async_computation.4 | async-start | bytes 655360 | tf_op jit(solution)/shard_map/route/all_to_all | solution.py:36
  127.9 16.7 %copy-start.9 = (f32[2048]{0:T(1024)S(1)}, f32[2048]{0:T(1024)}, u32[]{:S(2)}) copy-start(f32[2048]{0:T(1024)} %param.40) | copy-start | bytes 24580
  127.9 18.7 %all-to-all-start.5 = ((bf16[4,256,512]{1,2,0:T(8,128)(2,1)}), bf16[4,256,512]{1,2,0:T(8,128)(2,1)S(1)}, u32[]{:S(2)}, u32[]{:S(2)}) async-start(bf16[4,256,512]{1,2,0:T(8,128)(2,1)} %broadcast_in_dim.34), calls=%async_computation.5 | async-start | bytes 2097152 | tf_op jit(solution)/shard_map/join/all_to_all | solution.py:36
  169.3 30.8 %all-to-all-start.7 = ((bf16[128,2,512]{2,1,0:T(2,128)(2,1)}), bf16[128,2,512]{2,1,0:T(2,128)(2,1)S(1)}, u32[]{:S(2)}, u32[]{:S(2)}) async-start(bf16[128,2,512]{2,1,0:T(2,128)(2,1)} %reshape.410), calls=%async_computation.7 | async-start | bytes 524288 | tf_op jit(solution)/shard_map/return/all_to_all | solution.py:36

commit v3 on v2

--- a/solution.py
+++ b/solution.py
@@ -2,6 +2,7 @@
 import jax.numpy as jnp
 from jax import lax
 from jax.sharding import Mesh, PartitionSpec as P
+
 
 SUB = 64
 VD = 128
@@ -125,6 +126,23 @@
 def split_pair(values):
     high = lax.reduce_precision(values, 8, 7)
     return high.astype(jnp.bfloat16), (values - high).astype(jnp.bfloat16)
+
+
+def trade_columns(weight, tp_index):
+    share = weight.shape[1] // N_TP
+    kept = [own_columns(weight, tp_index * share, share)]
+    for shift in (1, 2, 3):
+        sent = own_columns(weight, ((tp_index + shift) & 3) * share, share)
+        pairs = [(index, (index + shift) % N_TP) for index in range(N_TP)]
+        kept.append(lax.ppermute(sent, "tp", pairs))
+    kept = jnp.stack(kept)
+    return jnp.concatenate(
+        [
+            lax.dynamic_index_in_dim(kept, (tp_index - index) & 3, 0, False)
+            for index in range(N_TP)
+        ],
+        axis=0,
+    )
 
 
 def own_columns(values, tp_start, share_width):
@@ -158,46 +176,54 @@
 ):
     width = tokens.shape[1]
     share_width = width // N_TP
-    tp_start = lax.axis_index("tp") * share_width
+    tp_index = lax.axis_index("tp")
+    tp_start = tp_index * share_width
     block = width // N_XC
+
+    select, combine_weights, lead_scale = route_tables(expert_ids, expert_probs)
+    tags = jnp.stack(split_pair(lead_scale), axis=1).reshape(2, 16, 2)
+    tags = jnp.pad(tags, ((0, 0), (0, 0), (0, 30)))
+
+    def by_rep(weight):
+        return weight.reshape(16, REP, 32).transpose(1, 0, 2)
+
+    shared = jnp.concatenate(
+        (query_weight, key_weight, value_weight, out_weight.T), axis=1
+    )
+    dense_parts = jnp.concatenate(
+        (by_rep(dense_gate_weight), by_rep(dense_up_weight), by_rep(dense_down_weight.T)), axis=2
+    )
+    message = jnp.concatenate(
+        (
+            jnp.broadcast_to(shared[None, None], (REP, 2, 16, 768)),
+            jnp.broadcast_to(dense_parts[:, None], (REP, 2, 16, 96)),
+            jnp.broadcast_to(tags[None], (REP, 2, 16, 32)),
+        ),
+        axis=3,
+    ).reshape(N_Z, 16, 896)
+    held = exchange(message, Z).reshape(N_Z * 16, 896)
 
     residual = to_mixed(tokens).astype(jnp.float32)
     normed = mixed_scale(residual, to_mixed(norm_gain[None])).astype(jnp.bfloat16)
-    with jax.named_scope("spread"):
-        spread = exchange(normed, XC).reshape(N_XC * SEQ, block)
-    shard = jnp.concatenate(
-        (
-            query_weight,
-            key_weight,
-            value_weight,
-            out_weight.T,
-            dense_gate_weight,
-            dense_up_weight,
-            dense_down_weight.T,
-        ),
-        axis=1,
-    )
-    with jax.named_scope("hold"):
-        held = lax.all_gather(shard, Z, axis=0, tiled=True)
+    xc_index = lax.axis_index(XC)
+    spread = lax.all_gather(normed, XC, axis=0)
+    spread = lax.dynamic_index_in_dim(spread, xc_index, 1, False).reshape(N_XC * SEQ, block)
 
     partial_rows = jnp.dot(spread, held[:, :512], preferred_element_type=jnp.float32)
-    with jax.named_scope("project"):
-        packed = jnp.sum(exchange(partial_rows.reshape(N_XC, SEQ, 512), XC), axis=0)
+    packed = jnp.sum(exchange(partial_rows.reshape(N_XC, SEQ, 512), XC), axis=0)
     head_out = attend(
         packed, key_cache, value_cache, lengths, query_gain, key_gain, lambdas, head_gain
     )
-    with jax.named_scope("heads"):
-        all_heads = gather_small(head_out, XC, N_XC).reshape(N_XC * SEQ, 256)
+    all_heads = gather_small(head_out, XC, N_XC).reshape(N_XC * SEQ, 256)
     attended_part = lax.dot_general(
         all_heads, held[:, 512:768], (((1,), (1,)), ((), ())), preferred_element_type=jnp.float32
     ).astype(jnp.bfloat16)
-    with jax.named_scope("attended"):
-        parts = exchange(
-            jnp.broadcast_to(
-                attended_part.reshape(N_XC, 1, SEQ, block), (N_XC, N_TP, SEQ, block)
-            ).reshape(N_XC * N_TP, SEQ, block),
-            XC + ("tp",),
-        ).reshape(N_XC, N_TP, SEQ, block)
+    parts = exchange(
+        jnp.broadcast_to(
+            attended_part.reshape(N_XC, 1, SEQ, block), (N_XC, N_TP, SEQ, block)
+        ).reshape(N_XC * N_TP, SEQ, block),
+        XC + ("tp",),
+    ).reshape(N_XC, N_TP, SEQ, block)
     attended = jnp.sum(parts.astype(jnp.float32), axis=1)
     middle_mixed = lax.optimization_barrier((residual + attended).astype(jnp.bfloat16))
     ffn_input = from_mixed(
@@ -205,60 +231,52 @@
     )
     middle = from_mixed(middle_mixed).astype(jnp.float32)
 
-    select, combine_weights, lead_scale = route_tables(expert_ids, expert_probs)
-    scale_high, scale_low = split_pair(lead_scale)
-    tags = jnp.pad(jnp.stack((scale_high, scale_low), axis=1), ((0, 0), (0, 126)))
     ffn_share = own_columns(ffn_input, tp_start, share_width)
     chosen = jnp.dot(
         select.astype(jnp.bfloat16).T, ffn_share, preferred_element_type=jnp.float32
     ).astype(jnp.bfloat16)
-    chosen = jnp.concatenate((chosen, tags), axis=1)
-    sent = share_width + 128
     outgoing = jnp.broadcast_to(
-        chosen.reshape(1, EXPERTS, CAP, sent), (REP, EXPERTS, CAP, sent)
-    ).reshape(N_EP, CAP, sent)
-    with jax.named_scope("route"):
-        incoming = exchange(outgoing, EP).reshape(N_EP * CAP, sent)
-
-    rep_start = lax.axis_index("b") * 32
-    mine = jnp.concatenate(
-        [
-            lax.dynamic_slice_in_dim(held[:, start : start + 256], rep_start, 32, 1)
-            for start in (768, 1024, 1280)
-        ],
-        axis=1,
-    )
-    with jax.named_scope("dense"):
-        dense_held = lax.all_gather(mine, XC, axis=0, tiled=True)
-    dense_held = (
-        dense_held.reshape(N_XC, N_Z, 16, 96).transpose(1, 0, 2, 3).reshape(width, 96)
-    )
-
-    with jax.named_scope("join"):
-        rows = gather_small(incoming[:, :share_width], "tp", N_TP)
+        chosen.reshape(1, EXPERTS, CAP, share_width), (REP, EXPERTS, CAP, share_width)
+    ).reshape(N_EP, CAP, share_width)
+    incoming = exchange(outgoing, EP).reshape(N_EP * CAP, share_width)
+
+    down = trade_columns(expert_down[0], tp_index)
+    dense_held = lax.all_gather(held[:, 768:], XC, axis=0).reshape(N_XC, N_Z, 16, 128)
+    incoming, dense_held = lax.optimization_barrier((incoming, dense_held))
+    tag = lax.dynamic_slice_in_dim(dense_held, 2 * xc_index, CAP, 2)[..., 96:98]
+    tag = jnp.sum(tag.transpose(1, 0, 2, 3).reshape(N_EP * CAP, 2).astype(jnp.float32), axis=1)
+    dense_held = dense_held.transpose(1, 0, 2, 3).reshape(width, 128)
+    dense_down = trade_columns(dense_held[:, 64:96].T, tp_index)
+
+    rows = gather_small(incoming, "tp", N_TP)
+    rows, dense_down = lax.optimization_barrier((rows, dense_down))
     rows = rows.transpose(1, 0, 2).reshape(N_EP * CAP, width)
-    tag = incoming[:, share_width : share_width + 2].astype(jnp.float32)
-    branch_weight = jax.nn.sigmoid(
-        jnp.sum(rows.astype(jnp.float32) * branch_gate, axis=1, keepdims=True)
-    )
-    dense_scale = branch_weight * (tag[:, :1] + tag[:, 1:])
-    gate_val = jnp.dot(rows, expert_gate[0], preferred_element_type=jnp.float32)
-    up_val = jnp.dot(rows, expert_up[0], preferred_element_type=jnp.float32)
-    hidden = (jax.nn.silu(gate_val) * up_val).astype(jnp.bfloat16)
-    dense_both = jnp.dot(rows, dense_held[:, :64], preferred_element_type=jnp.float32)
+    branch_weight = jax.nn.sigmoid(jnp.sum(rows.astype(jnp.float32) * branch_gate, axis=1))
+    dense_scale = branch_weight * tag
+
+    def units(weight):
+        return lax.dot_general(
+            weight, rows, (((0,), (1,)), ((), ())), preferred_element_type=jnp.float32
+        )
+
+    hidden = (jax.nn.silu(units(expert_gate[0])) * units(expert_up[0])).astype(jnp.bfloat16)
+    dense_both = units(dense_held[:, :64])
     dense_hidden = (
-        jax.nn.silu(dense_both[:, :32]) * dense_both[:, 32:] * dense_scale
-    ).astype(jnp.bfloat16)
-    down = jnp.concatenate((expert_down[0], dense_held[:, 64:].T), axis=0)
-    both_parts = jnp.dot(
-        jnp.concatenate((hidden, dense_hidden), axis=1), down, preferred_element_type=jnp.float32
-    ).astype(jnp.bfloat16)
-    both_parts = both_parts.reshape(N_EP * CAP, N_TP, share_width).transpose(1, 0, 2)
-    with jax.named_scope("reduce"):
-        summed = jnp.sum(exchange(both_parts, "tp").astype(jnp.float32), axis=0)
-    block_out = summed.astype(jnp.bfloat16).reshape(N_EP, CAP, share_width)
-    with jax.named_scope("return"):
-        returned = exchange(block_out, EP)
+        jax.nn.silu(dense_both[:32]) * dense_both[32:] * dense_scale[None]
+    ).astype(jnp.bfloat16)
+    all_hidden = gather_small(jnp.concatenate((hidden, dense_hidden), axis=0), "tp", N_TP)
+
+    def summed(values, weight):
+        return lax.dot_general(
+            values.reshape(-1, N_EP * CAP),
+            weight,
+            (((0,), (0,)), ((), ())),
+            preferred_element_type=jnp.float32,
+        )
+
+    block_out = summed(all_hidden[:, :176], down) + summed(all_hidden[:, 176:], dense_down)
+    block_out = block_out.astype(jnp.bfloat16).reshape(N_EP, CAP, share_width)
+    returned = exchange(block_out, EP)
     expert_out = jnp.sum(
         returned.reshape(REP, EXPERTS * CAP, share_width).astype(jnp.float32), axis=0
     )

time: 202 us -> 195 us (0.965)
  blocking collectives: 60.9 us -> 36 us
  starting transfers between devices: 49.8 us -> 74 us
  waiting for transfers between devices: 65.4 us -> 52.9 us
  local copies, waits for them, and re-layouts: 11 us -> 18 us
  matrix products: 7.83 us -> 5.78 us
    ppermute x0 -> x6, starting transfers between devices: none -> 18.5 us  [trade_columns(): kept.append(lax.ppermute(sent, 'tp', pairs))]
    all_gather x2, blocking collectives: 43.9 us -> 28.1 us  [the longest x1 14.3 us: shards(): spread = lax.all_gather(normed, XC, axis=0)]
    all_to_all x7, waiting for transfers between devices: 65.4 us -> 52.9 us  [exchange(): return lax.all_to_all(values, axes, split_axis=0, concat_axis=0, tiled=True)]
    all_to_all x1, blocking collectives: 17 us -> 7.95 us  [exchange(): return lax.all_to_all(values, axes, split_axis=0, concat_axis=0, tiled=True)]
    all_to_all x7, starting transfers between devices: 49.8 us -> 55.5 us  [exchange(): return lax.all_to_all(values, axes, split_axis=0, concat_axis=0, tiled=True)]
    another operation x1 -> x5, local copies, waits for them, and re-layouts: 0.1 us -> 2.89 us  [trade_columns(): kept = jnp.stack(kept)]
    reshape x4 -> x5, local copies, waits for them, and re-layouts: 1.05 us -> 3.27 us  [the longest x3 2.37 us: by_rep(): return weight.reshape(16, REP, 32).transpose(1, 0, 2)]
    dot_general x4 -> x5, matrix products: 3.7 us -> 1.67 us  [the longest x3 1.02 us: units(): lax.dot_general(weight, rows, (((0,), (1,)), ((), ())), preferred_element...]
  transfers between devices with their start and end apart: 7 -> 13, of which waited for: 6 -> 6; matrix products, arithmetic and copies ran while one was open for 3% -> 7% of each run, Pallas kernels for 0% -> 0%
where the time goes in v3:
time: 195 us; the launch traced here: 194 us
  starting transfers between devices  74 us (38%)
  waiting for transfers between devices  52.9 us (27%)
  blocking collectives  36 us (18%)
  local copies, waits for them, and re-layouts  18 us (9%)
  other arithmetic  6.54 us (3%)
  matrix products  5.78 us (3%)
    all_to_all x7, starting transfers between devices, exchange(): return lax.all_to_all(values, axes, split_axis=0, concat_axis=0, tiled=True)  55.5 us
    all_to_all x7, waiting for transfers between devices, exchange(): return lax.all_to_all(values, axes, split_axis=0, concat_axis=0, tiled=True)  52.9 us
    ppermute x6, starting transfers between devices, trade_columns(): kept.append(lax.ppermute(sent, 'tp', pairs))  18.5 us
    all_gather x1, blocking collectives, shards(): spread = lax.all_gather(normed, XC, axis=0)  14.3 us
    all_gather x1, blocking collectives, shards(): lax.all_gather(held[:, 768:], XC, axis=0).reshape(N_XC, N_Z, 16, 128)  13.8 us
    all_to_all x1, blocking collectives, exchange(): return lax.all_to_all(values, axes, split_axis=0, concat_axis=0, tiled=True)  7.95 us
  transfers between devices with their start and end apart: 13, of which 6 were waited for; matrix products, arithmetic and copies ran while one was open for 7% of the time, Pallas kernels for 0%

profile of v3, /device:TPU:33, one launch (start us, length us, event | category | flops | bytes accessed | tf_op | source)
XLA Modules:
  0.0 194.1 jit_solution(8332625319455724443)
XLA Ops:
  0.0 0.8 copy.101
  1.3 0.7 slice_bitcast_fusion.5
  2.3 0.8 reshape.452
  3.1 0.8 reshape.451
  3.9 0.8 reshape.450
  4.8 0.8 pad_maximum_fusion.6
  5.6 0.9 pad_maximum_fusion.1
  6.5 14.8 %all-to-all-start = ((bf16[16,16,896]{2,1,0:T(8,128)(2,1)}), bf16[16,16,896]{2,1,0:T(8,128)(2,1)S(1)}, u32[]{:S(2)}, u32[]{:S(2)}) async-start(bf16[16,16,896]{2,1,0:T(8,128)(2,1)} %bitcast.13), calls=%async_computation | async-start | bytes 917504 | tf_op jit(solution)/shard_map/all_to_all | solution.py:37
  22.0 1.2 copy.97
  23.2 1.2 convert_multiply_fusion
  24.9 14.3 %all_gather.10 = bf16[8,8,8,256]{3,2,0,1:T(8,128)(2,1)S(1)} all-gather(bf16[1,8,8,256]{3,2,0,1:T(8,128)(2,1)S(1)} %fusion.28), channel_id=1, replica_groups=mesh['b'=8,'zp'=2,'x'=4,'c'=2,'tp'=4] {'x','c'}, dimensions={0}, use_global_device_ids=true | all-gather | bytes 294912 | tf_op jit(solution)/shard_map/all_gather | solution.py:209
  39.2 5.0 %all-to-all-done = bf16[16,16,896]{2,1,0:T(8,128)(2,1)S(1)} async-done(((bf16[16,16,896]{2,1,0:T(8,128)(2,1)}), bf16[16,16,896]{2,1,0:T(8,128)(2,1)S(1)}, u32[]{:S(2)}, u32[]{:S(2)}) %all-to-all-start) | async-done | bytes 458784 | tf_op jit(solution)/shard_map/all_to_all | solution.py:37
  44.1 0.8 fusion.25
  45.0 6.8 %all-to-all-start.1 = ((f32[8,8,512]{2,1,0:T(8,128)}), f32[8,8,512]{2,1,0:T(8,128)S(1)}, u32[]{:S(2)}, u32[]{:S(2)}) async-start(f32[8,8,512]{2,1,0:T(8,128)} %fusion.25), calls=%async_computation.1 | async-start | bytes 262144 | tf_op jit(solution)/shard_map/all_to_all | solution.py:37
  51.9 5.2 %all-to-all-done.1 = f32[8,8,512]{2,1,0:T(8,128)S(1)} async-done(((f32[8,8,512]{2,1,0:T(8,128)}), f32[8,8,512]{2,1,0:T(8,128)S(1)}, u32[]{:S(2)}, u32[]{:S(2)}) %all-to-all-start.1) | async-done | bytes 131104 | tf_op jit(solution)/shard_map/all_to_all | solution.py:37
  57.5 1.6 fusion.61
  60.6 7.9 %all_to_all.40 = bf16[8,8,256]{2,1,0:T(8,128)(2,1)S(1)} all-to-all(bf16[8,8,256]{2,1,0:T(8,128)(2,1)S(1)} %broadcast_in_dim.40), channel_id=1, replica_groups=mesh['b'=8,'zp'=2,'x'=4,'c'=2,'tp'=4] {'x','c'}, dimensions={0} | all-to-all | bytes 65536 | tf_op jit(solution)/shard_map/all_to_all | solution.py:37
  68.7 0.7 broadcast_in_dim.42
  69.4 6.0 %all-to-all-start.3 = ((bf16[32,8,256]{2,1,0:T(8,128)(2,1)}), bf16[32,8,256]{2,1,0:T(8,128)(2,1)S(1)}, u32[]{:S(2)}, u32[]{:S(2)}) async-start(bf16[32,8,256]{2,1,0:T(8,128)(2,1)} %bitcast.32), calls=%async_computation.3 | async-start | bytes 262144 | tf_op jit(solution)/shard_map/all_to_all | solution.py:37
  75.9 7.0 %all-to-all-done.3 = bf16[32,8,256]{2,1,0:T(8,128)(2,1)S(1)} async-done(((bf16[32,8,256]{2,1,0:T(8,128)(2,1)}), bf16[32,8,256]{2,1,0:T(8,128)(2,1)S(1)}, u32[]{:S(2)}, u32[]{:S(2)}) %all-to-all-start.3) | async-done | bytes 131104 | tf_op jit(solution)/shard_map/all_to_all | solution.py:37
  84.1 0.8 broadcast_in_dim.44
  85.0 10.6 %all-to-all-start.4 = ((bf16[128,2,512]{2,1,0:T(2,128)(2,1)}), bf16[128,2,512]{2,1,0:T(2,128)(2,1)S(1)}, u32[]{:S(2)}, u32[]{:S(2)}) async-start(bf16[128,2,512]{2,1,0:T(2,128)(2,1)} %bitcast.37), calls=%async_computation.4 | async-start | bytes 524288 | tf_op jit(solution)/shard_map/all_to_all | solution.py:37
  95.6 13.8 %all-gather = bf16[2048,128]{1,0:T(8,128)(2,1)S(1)} all-gather(bf16[256,128]{1,0:T(8,128)(2,1)S(1)} %slice.86), channel_id=2, replica_groups=mesh['b'=8,'zp'=2,'x'=4,'c'=2,'tp'=4] {'x','c'}, dimensions={0}, use_global_device_ids=true | all-gather | bytes 589824 | tf_op jit(solution)/shard_map/all_gather | solution.py:244
  109.4 8.7 %all-to-all-done.4 = bf16[128,2,512]{2,1,0:T(2,128)(2,1)S(1)} async-done(((bf16[128,2,512]{2,1,0:T(2,128)(2,1)}), bf16[128,2,512]{2,1,0:T(2,128)(2,1)S(1)}, u32[]{:S(2)}, u32[]{:S(2)}) %all-to-all-start.4) | async-done | bytes 262176 | tf_op jit(solution)/shard_map/all_to_all | solution.py:37
  118.4 1.1 broadcast_in_dim.45
  119.4 3.5 %all-to-all-start.5 = ((bf16[4,256,512]{1,2,0:T(8,128)(2,1)}), bf16[4,256,512]{1,2,0:T(8,128)(2,1)S(1)}, u32[]{:S(2)}, u32[]{:S(2)}) async-start(bf16[4,256,512]{1,2,0:T(8,128)(2,1)} %broadcast_in_dim.45), calls=%async_computation.5 | async-start | bytes 2097152 | tf_op jit(solution)/shard_map/all_to_all | solution.py:37
  123.2 0.8 dynamic-slice_bitcast_fusion.10
  124.0 4.5 %collective-permute-start.2 = (bf16[32,512]{0,1:T(8,128)(2,1)}, bf16[32,512]{0,1:T(8,128)(2,1)}, u32[]{:S(2)}, u32[]{:S(2)}) collective-permute-start(bf16[32,512]{0,1:T(8,128)(2,1)} %get-tuple-element.24), channel_id=1, source_target_pairs={{0,3},{1,0},{2,1},{3,2},{4,7},{5,4},{6,5},{7,6},{8,11},{9,8},{10,9... | collective-permute-start | bytes 98312 | tf_op jit(solution)/shard_map/ppermute | solution.py:137
  128.5 2.5 %collective-permute-start.1 = (bf16[32,512]{0,1:T(8,128)(2,1)}, bf16[32,512]{0,1:T(8,128)(2,1)}, u32[]{:S(2)}, u32[]{:S(2)}) collective-permute-start(bf16[32,512]{0,1:T(8,128)(2,1)} %get-tuple-element.25), channel_id=1, source_target_pairs={{0,2},{1,3},{2,0},{3,1},{4,6},{5,7},{6,4},{7,5},{8,10},{9,11},{10,... | collective-permute-start | bytes 98312 | tf_op jit(solution)/shard_map/ppermute | solution.py:137
  131.0 2.5 %collective-permute-start = (bf16[32,512]{0,1:T(8,128)(2,1)}, bf16[32,512]{0,1:T(8,128)(2,1)S(1)}, u32[]{:S(2)}, u32[]{:S(2)}) collective-permute-start(bf16[32,512]{0,1:T(8,128)(2,1)} %get-tuple-element.26), channel_id=1, source_target_pairs={{0,1},{1,2},{2,3},{3,0},{4,5},{5,6},{6,7},{7,4},{8,9},{9,10},{10,1... | collective-permute-start | bytes 98312 | tf_op jit(solution)/shard_map/ppermute | solution.py:137
  133.5 0.8 constant_dynamic-slice_fusion
  134.3 4.0 %collective-permute-start.5 = (bf16[176,512]{1,0:T(8,128)(2,1)}, bf16[176,512]{1,0:T(8,128)(2,1)}, u32[]{:S(2)}, u32[]{:S(2)}) collective-permute-start(bf16[176,512]{1,0:T(8,128)(2,1)} %get-tuple-element.21), channel_id=1, source_target_pairs={{0,3},{1,0},{2,1},{3,2},{4,7},{5,4},{6,5},{7,6},{8,11},{9,8},{10,9... | collective-permute-start | bytes 540680 | tf_op jit(solution)/shard_map/ppermute | solution.py:137
  138.3 3.1 %collective-permute-start.4 = (bf16[176,512]{1,0:T(8,128)(2,1)}, bf16[176,512]{1,0:T(8,128)(2,1)}, u32[]{:S(2)}, u32[]{:S(2)}) collective-permute-start(bf16[176,512]{1,0:T(8,128)(2,1)} %get-tuple-element.22), channel_id=1, source_target_pairs={{0,2},{1,3},{2,0},{3,1},{4,6},{5,7},{6,4},{7,5},{8,10},{9,11},{10,... | collective-permute-start | bytes 540680 | tf_op jit(solution)/shard_map/ppermute | solution.py:137
  142.1 1.9 collective-permute-start.3
  144.0 1.0 copy.119
  145.0 1.0 copy.118
  146.9 0.4 convolution_bitcast_fusion.1
  147.3 0.4 copy-done.13
  147.6 0.4 fusion.2
  148.0 0.8 broadcast_in_dim.46
  148.8 3.9 %all-to-all-start.6 = ((bf16[4,208,256]{2,1,0:T(8,128)(2,1)}), bf16[4,208,256]{2,1,0:T(8,128)(2,1)S(1)}, u32[]{:S(2)}, u32[]{:S(2)}) async-start(bf16[4,208,256]{2,1,0:T(8,128)(2,1)} %broadcast_in_dim.46), calls=%async_computation.6 | async-start | bytes 851968 | tf_op jit(solution)/shard_map/all_to_all | solution.py:37
  152.8 1.1 pad_maximum_fusion
  153.9 5.2 %all-to-all-done.6 = bf16[4,208,256]{2,1,0:T(8,128)(2,1)S(1)} async-done(((bf16[4,208,256]{2,1,0:T(8,128)(2,1)}), bf16[4,208,256]{2,1,0:T(8,128)(2,1)S(1)}, u32[]{:S(2)}, u32[]{:S(2)}) %all-to-all-start.6) | async-done | bytes 426016 | tf_op jit(solution)/shard_map/all_to_all | solution.py:37
  159.2 0.4 fusion.12
  159.9 0.8 reshape.469
  160.7 10.0 %all-to-all-start.7 = ((bf16[128,2,512]{2,1,0:T(2,128)(2,1)}), bf16[128,2,512]{2,1,0:T(2,128)(2,1)S(1)}, u32[]{:S(2)}, u32[]{:S(2)}) async-start(bf16[128,2,512]{2,1,0:T(2,128)(2,1)} %reshape.469), calls=%async_computation.7 | async-start | bytes 524288 | tf_op jit(solution)/shard_map/all_to_all | solution.py:37
  171.4 21.8 %all-to-all-done.7 = bf16[128,2,512]{2,1,0:T(2,128)(2,1)S(1)} async-done(((bf16[128,2,512]{2,1,0:T(2,128)(2,1)}), bf16[128,2,512]{2,1,0:T(2,128)(2,1)S(1)}, u32[]{:S(2)}, u32[]{:S(2)}) %all-to-all-start.7) | async-done | bytes 262176 | tf_op jit(solution)/shard_map/all_to_all | solution.py:37
  193.3 0.8 fusion.6
  (141 shorter events, 9.0 us)
Async XLA Ops:
  0.0 146.9 %copy-start = (bf16[1,2048,176]{1,2,0:T(8,128)(2,1)S(1)}, bf16[1,2048,176]{1,2,0:T(8,128)(2,1)}, u32[]{:S(2)}) copy-start(bf16[1,2048,176]{1,2,0:T(8,128)(2,1)} %param.43) | copy-start | bytes 2162692
  0.0 21.3 %copy-start.3 = (bf16[8,2048]{1,0:T(8,128)(2,1)S(1)}, bf16[8,2048]{1,0:T(8,128)(2,1)}, u32[]{:S(2)}) copy-start(bf16[8,2048]{1,0:T(8,128)(2,1)} %param.23) | copy-start | bytes 98308
  6.5 15.3 %copy-start.4 = (f32[2048]{0:T(1024)S(1)}, f32[2048]{0:T(1024)}, u32[]{:S(2)}) copy-start(f32[2048]{0:T(1024)} %param.24) | copy-start | bytes 24580
  6.5 15.5 %copy-start.2 = (bf16[8,1,320,128]{3,2,1,0:T(8,128)(2,1)S(1)}, bf16[8,1,320,128]{3,2,1,0:T(8,128)(2,1)}, u32[]{:S(2)}) copy-start(bf16[8,1,320,128]{3,2,1,0:T(8,128)(2,1)} %param.31) | copy-start | bytes 1966084
  6.5 37.6 %all-to-all-start = ((bf16[16,16,896]{2,1,0:T(8,128)(2,1)}), bf16[16,16,896]{2,1,0:T(8,128)(2,1)S(1)}, u32[]{:S(2)}, u32[]{:S(2)}) async-start(bf16[16,16,896]{2,1,0:T(8,128)(2,1)} %bitcast.13), calls=%async_computation | async-start | bytes 917504 | tf_op jit(solution)/shard_map/all_to_all | solution.py:37
  24.5 27.3 %copy-start.9 = (s32[8]{0:T(128)S(1)}, s32[8]{0:T(128)}, u32[]{:S(2)}) copy-start(s32[8]{0:T(128)} %param.33) | copy-start | bytes 100
  24.5 32.9 %copy-start.8 = (f32[64]{0:T(128)S(1)}, f32[64]{0:T(128)}, u32[]{:S(2)}) copy-start(f32[64]{0:T(128)} %param.28) | copy-start | bytes 772
  24.5 33.0 %copy-start.10 = (f32[64]{0:T(128)S(1)}, f32[64]{0:T(128)}, u32[]{:S(2)}) copy-start(f32[64]{0:T(128)} %param.29) | copy-start | bytes 772
  24.9 34.9 %copy-start.12 = (f32[2]{0:T(128)S(1)}, f32[2]{0:T(128)}, u32[]{:S(2)}) copy-start(f32[2]{0:T(128)} %param.30) | copy-start | bytes 28
  39.1 21.0 %copy-start.14 = (bf16[8,1,320,128]{3,2,1,0:T(8,128)(2,1)S(1)}, bf16[8,1,320,128]{3,2,1,0:T(8,128)(2,1)}, u32[]{:S(2)}) copy-start(bf16[8,1,320,128]{3,2,1,0:T(8,128)(2,1)} %param.32) | copy-start | bytes 1966084
  45.0 12.1 %all-to-all-start.1 = ((f32[8,8,512]{2,1,0:T(8,128)}), f32[8,8,512]{2,1,0:T(8,128)S(1)}, u32[]{:S(2)}, u32[]{:S(2)}) async-start(f32[8,8,512]{2,1,0:T(8,128)} %fusion.25), calls=%async_computation.1 | async-start | bytes 262144 | tf_op jit(solution)/shard_map/all_to_all | solution.py:37
  51.8 8.7 %copy-start.11 = (f32[128]{0:T(128)S(1)}, f32[128]{0:T(128)}, u32[]{:S(2)}) copy-start(f32[128]{0:T(128)} %param.34) | copy-start | bytes 1540
  59.0 16.6 %copy-start.5 = (f32[2048]{0:T(1024)S(1)}, f32[2048]{0:T(1024)}, u32[]{:S(2)}) copy-start(f32[2048]{0:T(1024)} %param.36) | copy-start | bytes 24580
  59.0 16.8 %copy-start.7 = (f32[8,2]{0,1:T(2,128)S(1)}, f32[8,2]{0,1:T(2,128)}, u32[]{:S(2)}) copy-start(f32[8,2]{0,1:T(2,128)} %param.42) | copy-start | bytes 196
  69.4 13.5 %all-to-all-start.3 = ((bf16[32,8,256]{2,1,0:T(8,128)(2,1)}), bf16[32,8,256]{2,1,0:T(8,128)(2,1)S(1)}, u32[]{:S(2)}, u32[]{:S(2)}) async-start(bf16[32,8,256]{2,1,0:T(8,128)(2,1)} %bitcast.32), calls=%async_computation.3 | async-start | bytes 262144 | tf_op jit(solution)/shard_map/all_to_all | solution.py:37
  85.0 33.2 %all-to-all-start.4 = ((bf16[128,2,512]{2,1,0:T(2,128)(2,1)}), bf16[128,2,512]{2,1,0:T(2,128)(2,1)S(1)}, u32[]{:S(2)}, u32[]{:S(2)}) async-start(bf16[128,2,512]{2,1,0:T(2,128)(2,1)} %bitcast.37), calls=%async_computation.4 | async-start | bytes 524288 | tf_op jit(solution)/shard_map/all_to_all | solution.py:37
  119.4 26.8 %all-to-all-start.5 = ((bf16[4,256,512]{1,2,0:T(8,128)(2,1)}), bf16[4,256,512]{1,2,0:T(8,128)(2,1)S(1)}, u32[]{:S(2)}, u32[]{:S(2)}) async-start(bf16[4,256,512]{1,2,0:T(8,128)(2,1)} %broadcast_in_dim.45), calls=%async_computation.5 | async-start | bytes 2097152 | tf_op jit(solution)/shard_map/all_to_all | solution.py:37
  123.0 10.6 %copy-start.1 = (bf16[1,176,2048]{2,1,0:T(8,128)(2,1)S(1)}, bf16[1,176,2048]{2,1,0:T(8,128)(2,1)}, u32[]{:S(2)}) copy-start(bf16[1,176,2048]{2,1,0:T(8,128)(2,1)} %param.45) | copy-start | bytes 2162692
  123.0 18.4 %copy-start.6 = (f32[2048]{0:T(1024)S(1)}, f32[2048]{0:T(1024)}, u32[]{:S(2)}) copy-start(f32[2048]{0:T(1024)} %param.40) | copy-start | bytes 24580
  124.0 18.1 %collective-permute-start.2 = (bf16[32,512]{0,1:T(8,128)(2,1)}, bf16[32,512]{0,1:T(8,128)(2,1)}, u32[]{:S(2)}, u32[]{:S(2)}) collective-permute-start(bf16[32,512]{0,1:T(8,128)(2,1)} %get-tuple-element.24), channel_id=1, source_target_pairs={{0,3},{1,0},{2,1},{3,2},{4,7},{5,4},{6,5},{7,6},{8,11},{9,8},{10,9... | collective-permute-start | bytes 98312 | tf_op jit(solution)/shard_map/ppermute | solution.py:137
  128.5 16.5 %collective-permute-start.1 = (bf16[32,512]{0,1:T(8,128)(2,1)}, bf16[32,512]{0,1:T(8,128)(2,1)}, u32[]{:S(2)}, u32[]{:S(2)}) collective-permute-start(bf16[32,512]{0,1:T(8,128)(2,1)} %get-tuple-element.25), channel_id=1, source_target_pairs={{0,2},{1,3},{2,0},{3,1},{4,6},{5,7},{6,4},{7,5},{8,10},{9,11},{10,... | collective-permute-start | bytes 98312 | tf_op jit(solution)/shard_map/ppermute | solution.py:137
  131.0 15.0 %collective-permute-start = (bf16[32,512]{0,1:T(8,128)(2,1)}, bf16[32,512]{0,1:T(8,128)(2,1)S(1)}, u32[]{:S(2)}, u32[]{:S(2)}) collective-permute-start(bf16[32,512]{0,1:T(8,128)(2,1)} %get-tuple-element.26), channel_id=1, source_target_pairs={{0,1},{1,2},{2,3},{3,0},{4,5},{5,6},{6,7},{7,4},{8,9},{9,10},{10,1... | collective-permute-start | bytes 98312 | tf_op jit(solution)/shard_map/ppermute | solution.py:137
  134.3 18.4 %collective-permute-start.5 = (bf16[176,512]{1,0:T(8,128)(2,1)}, bf16[176,512]{1,0:T(8,128)(2,1)}, u32[]{:S(2)}, u32[]{:S(2)}) collective-permute-start(bf16[176,512]{1,0:T(8,128)(2,1)} %get-tuple-element.21), channel_id=1, source_target_pairs={{0,3},{1,0},{2,1},{3,2},{4,7},{5,4},{6,5},{7,6},{8,11},{9,8},{10,9... | collective-permute-start | bytes 540680 | tf_op jit(solution)/shard_map/ppermute | solution.py:137
  138.3 14.4 %collective-permute-start.4 = (bf16[176,512]{1,0:T(8,128)(2,1)}, bf16[176,512]{1,0:T(8,128)(2,1)}, u32[]{:S(2)}, u32[]{:S(2)}) collective-permute-start(bf16[176,512]{1,0:T(8,128)(2,1)} %get-tuple-element.22), channel_id=1, source_target_pairs={{0,2},{1,3},{2,0},{3,1},{4,6},{5,7},{6,4},{7,5},{8,10},{9,11},{10,... | collective-permute-start | bytes 540680 | tf_op jit(solution)/shard_map/ppermute | solution.py:137
  142.1 10.7 %collective-permute-start.3 = (bf16[176,512]{1,0:T(8,128)(2,1)S(1)}, bf16[176,512]{1,0:T(8,128)(2,1)S(1)}, u32[]{:S(2)}, u32[]{:S(2)}) collective-permute-start(bf16[176,512]{1,0:T(8,128)(2,1)S(1)} %get-tuple-element.20), channel_id=1, source_target_pairs={{0,1},{1,2},{2,3},{3,0},{4,5},{5,6},{6,7},{7,4},{8,9},{9,10},{10,1... | collective-permute-start | bytes 540680 | tf_op jit(solution)/shard_map/ppermute | solution.py:137
  146.5 1.1 copy-start.13
  148.8 10.3 %all-to-all-start.6 = ((bf16[4,208,256]{2,1,0:T(8,128)(2,1)}), bf16[4,208,256]{2,1,0:T(8,128)(2,1)S(1)}, u32[]{:S(2)}, u32[]{:S(2)}) async-start(bf16[4,208,256]{2,1,0:T(8,128)(2,1)} %broadcast_in_dim.46), calls=%async_computation.6 | async-start | bytes 851968 | tf_op jit(solution)/shard_map/all_to_all | solution.py:37
  160.7 32.5 %all-to-all-start.7 = ((bf16[128,2,512]{2,1,0:T(2,128)(2,1)}), bf16[128,2,512]{2,1,0:T(2,128)(2,1)S(1)}, u32[]{:S(2)}, u32[]{:S(2)}) async-start(bf16[128,2,512]{2,1,0:T(2,128)(2,1)} %reshape.469), calls=%async_computation.7 | async-start | bytes 524288 | tf_op jit(solution)/shard_map/all_to_all | solution.py:37

commit v4 on v3

--- a/solution.py
+++ b/solution.py
@@ -1,8 +1,9 @@
 import jax
 import jax.numpy as jnp
 from jax import lax
+from jax.experimental import pallas as pl
+from jax.experimental.pallas import tpu as pltpu
 from jax.sharding import Mesh, PartitionSpec as P
-
 
 SUB = 64
 VD = 128
@@ -128,6 +129,31 @@
     return high.astype(jnp.bfloat16), (values - high).astype(jnp.bfloat16)
 
 
+def message_body(query, key, value, out, gate, up, down, tags, message):
+    lanes = lax.broadcasted_iota(jnp.int32, (16, 256), 1)
+    shared = jnp.concatenate((query[...], key[...], value[...], out[...]), axis=1)
+    wide = [part[...].astype(jnp.float32) for part in (gate, up, down)]
+    for rep in range(REP):
+        turned = [
+            pltpu.roll(part, (32 * (place - rep)) % 256, 1) for place, part in enumerate(wide)
+        ]
+        own = jnp.where(
+            lanes < 32, turned[0], jnp.where(lanes < 64, turned[1], turned[2])
+        )[:, :128]
+        own = jnp.where(lanes[:, :128] < 96, own, 0.0)
+        for half in range(2):
+            message[2 * rep + half, :, :768] = shared
+            message[2 * rep + half, :, 768:] = (own + tags[half]).astype(jnp.bfloat16)
+
+
+def build_message(*parts):
+    return pl.pallas_call(
+        message_body,
+        out_shape=jax.ShapeDtypeStruct((N_Z, 16, 896), jnp.bfloat16),
+        name="message",
+    )(*parts)
+
+
 def trade_columns(weight, tp_index):
     share = weight.shape[1] // N_TP
     kept = [own_columns(weight, tp_index * share, share)]
@@ -135,6 +161,10 @@
         sent = own_columns(weight, ((tp_index + shift) & 3) * share, share)
         pairs = [(index, (index + shift) % N_TP) for index in range(N_TP)]
         kept.append(lax.ppermute(sent, "tp", pairs))
+    return kept
+
+
+def in_order(kept, tp_index):
     kept = jnp.stack(kept)
     return jnp.concatenate(
         [
@@ -181,27 +211,24 @@
     block = width // N_XC
 
     select, combine_weights, lead_scale = route_tables(expert_ids, expert_probs)
-    tags = jnp.stack(split_pair(lead_scale), axis=1).reshape(2, 16, 2)
-    tags = jnp.pad(tags, ((0, 0), (0, 0), (0, 30)))
-
-    def by_rep(weight):
-        return weight.reshape(16, REP, 32).transpose(1, 0, 2)
-
-    shared = jnp.concatenate(
-        (query_weight, key_weight, value_weight, out_weight.T), axis=1
-    )
-    dense_parts = jnp.concatenate(
-        (by_rep(dense_gate_weight), by_rep(dense_up_weight), by_rep(dense_down_weight.T)), axis=2
-    )
-    message = jnp.concatenate(
-        (
-            jnp.broadcast_to(shared[None, None], (REP, 2, 16, 768)),
-            jnp.broadcast_to(dense_parts[:, None], (REP, 2, 16, 96)),
-            jnp.broadcast_to(tags[None], (REP, 2, 16, 32)),
-        ),
-        axis=3,
-    ).reshape(N_Z, 16, 896)
+    high, low = split_pair(lead_scale)
+    tags = jnp.concatenate((high.reshape(2, 16, 1), low.reshape(2, 16, 1)), axis=2)
+    tags = jnp.pad(tags.astype(jnp.float32), ((0, 0), (0, 0), (96, 30)))
+    message = build_message(
+        query_weight,
+        key_weight,
+        value_weight,
+        out_weight.T,
+        dense_gate_weight,
+        dense_up_weight,
+        dense_down_weight.T,
+        tags,
+    )
     held = exchange(message, Z).reshape(N_Z * 16, 896)
+    down = trade_columns(expert_down[0], tp_index)
+    held, down = lax.optimization_barrier((held, down))
+    down = in_order(down, tp_index)
+    dense_down = in_order(trade_columns(held[:, 832:864].T, tp_index), tp_index)
 
     residual = to_mixed(tokens).astype(jnp.float32)
     normed = mixed_scale(residual, to_mixed(norm_gain[None])).astype(jnp.bfloat16)
@@ -224,6 +251,7 @@
         ).reshape(N_XC * N_TP, SEQ, block),
         XC + ("tp",),
     ).reshape(N_XC, N_TP, SEQ, block)
+    parts, dense_down = lax.optimization_barrier((parts, dense_down))
     attended = jnp.sum(parts.astype(jnp.float32), axis=1)
     middle_mixed = lax.optimization_barrier((residual + attended).astype(jnp.bfloat16))
     ffn_input = from_mixed(
@@ -240,16 +268,21 @@
     ).reshape(N_EP, CAP, share_width)
     incoming = exchange(outgoing, EP).reshape(N_EP * CAP, share_width)
 
-    down = trade_columns(expert_down[0], tp_index)
-    dense_held = lax.all_gather(held[:, 768:], XC, axis=0).reshape(N_XC, N_Z, 16, 128)
+    dense_held = jnp.concatenate((held[:, 768:], dense_down.T), axis=0)
+    dense_held = lax.all_gather(dense_held, XC, axis=0)
     incoming, dense_held = lax.optimization_barrier((incoming, dense_held))
+    dense_down = (
+        dense_held[:, 256:].reshape(N_XC, 4, 16, 128).transpose(1, 0, 2, 3).reshape(512, 128)
+    )
+    dense_held = dense_held[:, :256].reshape(N_XC, N_Z, 16, 128)
     tag = lax.dynamic_slice_in_dim(dense_held, 2 * xc_index, CAP, 2)[..., 96:98]
     tag = jnp.sum(tag.transpose(1, 0, 2, 3).reshape(N_EP * CAP, 2).astype(jnp.float32), axis=1)
-    dense_held = dense_held.transpose(1, 0, 2, 3).reshape(width, 128)
-    dense_down = trade_columns(dense_held[:, 64:96].T, tp_index)
+    dense_held = dense_held.transpose(1, 0, 2, 3).reshape(width, 128)[:, :64]
 
     rows = gather_small(incoming, "tp", N_TP)
-    rows, dense_down = lax.optimization_barrier((rows, dense_down))
+    rows, dense_held, dense_down, tag = lax.optimization_barrier(
+        (rows, dense_held, dense_down, tag)
+    )
     rows = rows.transpose(1, 0, 2).reshape(N_EP * CAP, width)
     branch_weight = jax.nn.sigmoid(jnp.sum(rows.astype(jnp.float32) * branch_gate, axis=1))
     dense_scale = branch_weight * tag
@@ -260,7 +293,7 @@
         )
 
     hidden = (jax.nn.silu(units(expert_gate[0])) * units(expert_up[0])).astype(jnp.bfloat16)
-    dense_both = units(dense_held[:, :64])
+    dense_both = units(dense_held)
     dense_hidden = (
         jax.nn.silu(dense_both[:32]) * dense_both[32:] * dense_scale[None]
     ).astype(jnp.bfloat16)
@@ -274,7 +307,7 @@
             preferred_element_type=jnp.float32,
         )
 
-    block_out = summed(all_hidden[:, :176], down) + summed(all_hidden[:, 176:], dense_down)
+    block_out = summed(all_hidden[:, :176], down) + summed(all_hidden[:, 176:], dense_down.T)
     block_out = block_out.astype(jnp.bfloat16).reshape(N_EP, CAP, share_width)
     returned = exchange(block_out, EP)
     expert_out = jnp.sum(

time: 195 us -> 202 us (1.036)
  waiting for transfers between devices: 52.9 us -> 62.3 us
  blocking collectives: 36 us -> 29.2 us
  starting transfers between devices: 74 us -> 79.5 us
  local copies, waits for them, and re-layouts: 18 us -> 14.6 us
    all_to_all x7 -> x8, waiting for transfers between devices: 52.9 us -> 62.3 us  [exchange(): return lax.all_to_all(values, axes, split_axis=0, concat_axis=0, tiled=True)]
    all_to_all x1 -> x0, blocking collectives: 7.95 us -> none  [exchange(): return lax.all_to_all(values, axes, split_axis=0, concat_axis=0, tiled=True)]
    all_to_all x7 -> x8, starting transfers between devices: 55.5 us -> 60.7 us  [exchange(): return lax.all_to_all(values, axes, split_axis=0, concat_axis=0, tiled=True)]
    another operation x5 -> x1, local copies, waits for them, and re-layouts: 2.89 us -> 0.02 us  [in_order(): kept = jnp.stack(kept)]
    reshape x3 -> x0, local copies, waits for them, and re-layouts: 2.37 us -> none  [by_rep(): return weight.reshape(16, REP, 32).transpose(1, 0, 2)]
  transfers between devices with their start and end apart: 13 -> 14, of which waited for: 6 -> 6; matrix products, arithmetic and copies ran while one was open for 7% -> 7% of each run, Pallas kernels for 0% -> 0%
where the time goes in v4:
time: 202 us; the launch traced here: 201 us
  starting transfers between devices  79.5 us (39%)
  waiting for transfers between devices  62.3 us (31%)
  blocking collectives  29.2 us (14%)
  local copies, waits for them, and re-layouts  14.6 us (7%)
  other arithmetic  8.18 us (4%)
  matrix products  4.66 us (2%)
    all_to_all x8, waiting for transfers between devices, exchange(): return lax.all_to_all(values, axes, split_axis=0, concat_axis=0, tiled=True)  62.3 us
    all_to_all x8, starting transfers between devices, exchange(): return lax.all_to_all(values, axes, split_axis=0, concat_axis=0, tiled=True)  60.7 us
    ppermute x6, starting transfers between devices, trade_columns(): kept.append(lax.ppermute(sent, 'tp', pairs))  18.8 us
    all_gather x1, blocking collectives, shards(): spread = lax.all_gather(normed, XC, axis=0)  15.1 us
    all_gather x1, blocking collectives, shards(): dense_held = lax.all_gather(dense_held, XC, axis=0)  14.1 us
  transfers between devices with their start and end apart: 14, of which 6 were waited for; matrix products, arithmetic and copies ran while one was open for 7% of the time, Pallas kernels for 0%

profile of v4, /device:TPU:33, one launch (start us, length us, event | category | flops | bytes accessed | tf_op | source)
XLA Modules:
  0.0 200.8 jit_solution(4112493787477626873)
XLA Ops:
  0.0 0.9 copy.120
  1.4 0.7 slice_bitcast_fusion.3
  2.4 0.7 fusion.42.tags
  3.1 1.7 message.1
  4.8 14.7 %all-to-all-start = ((bf16[16,16,896]{2,1,0:T(8,128)(2,1)}), bf16[16,16,896]{2,1,0:T(8,128)(2,1)S(1)}, u32[]{:S(2)}, u32[]{:S(2)}) async-start(bf16[16,16,896]{2,1,0:T(8,128)(2,1)} %message.1), calls=%async_computation | async-start | bytes 917504 | tf_op jit(solution)/shard_map/all_to_all | solution.py:38
  19.5 0.9 dynamic-slice_bitcast_fusion.4
  20.4 3.3 %collective-permute-start = (bf16[176,512]{1,0:T(8,128)(2,1)}, bf16[176,512]{1,0:T(8,128)(2,1)}, u32[]{:S(2)}, u32[]{:S(2)}) collective-permute-start(bf16[176,512]{1,0:T(8,128)(2,1)} %get-tuple-element.38), channel_id=1, source_target_pairs={{0,1},{1,2},{2,3},{3,0},{4,5},{5,6},{6,7},{7,4},{8,9},{9,10},{10,1... | collective-permute-start | bytes 540680 | tf_op jit(solution)/shard_map/ppermute | solution.py:163
  23.7 4.5 %collective-permute-start.1 = (bf16[176,512]{1,0:T(8,128)(2,1)}, bf16[176,512]{1,0:T(8,128)(2,1)}, u32[]{:S(2)}, u32[]{:S(2)}) collective-permute-start(bf16[176,512]{1,0:T(8,128)(2,1)} %get-tuple-element.40), channel_id=1, source_target_pairs={{0,2},{1,3},{2,0},{3,1},{4,6},{5,7},{6,4},{7,5},{8,10},{9,11},{10,... | collective-permute-start | bytes 540680 | tf_op jit(solution)/shard_map/ppermute | solution.py:163
  28.2 3.0 %collective-permute-start.2 = (bf16[176,512]{1,0:T(8,128)(2,1)}, bf16[176,512]{1,0:T(8,128)(2,1)}, u32[]{:S(2)}, u32[]{:S(2)}) collective-permute-start(bf16[176,512]{1,0:T(8,128)(2,1)} %get-tuple-element.37), channel_id=1, source_target_pairs={{0,3},{1,0},{2,1},{3,2},{4,7},{5,4},{6,5},{7,6},{8,11},{9,8},{10,9... | collective-permute-start | bytes 540680 | tf_op jit(solution)/shard_map/ppermute | solution.py:163
  31.5 0.9 reshape.445
  32.4 0.9 reshape.446
  34.0 0.8 reduce_sum.152
  34.7 0.9 multiply_reduce_fusion.2
  35.6 0.9 fusion.28
  36.6 15.1 %all_gather.10 = bf16[8,8,8,256]{3,2,0,1:T(8,128)(2,1)S(1)} all-gather(bf16[1,8,8,256]{3,2,0,1:T(8,128)(2,1)S(1)} %fusion.28), channel_id=1, replica_groups=mesh['b'=8,'zp'=2,'x'=4,'c'=2,'tp'=4] {'x','c'}, dimensions={0}, use_global_device_ids=true | all-gather | bytes 294912 | tf_op jit(solution)/shard_map/all_gather | solution.py:236
  51.7 0.8 add_rsqrt_fusion
  52.5 0.7 iota_compare_fusion.2
  53.3 0.8 fusion.23
  54.1 4.0 %all-to-all-start.1 = ((f32[8,8,512]{2,1,0:T(8,128)}), f32[8,8,512]{2,1,0:T(8,128)S(1)}, u32[]{:S(2)}, u32[]{:S(2)}) async-start(f32[8,8,512]{2,1,0:T(8,128)} %fusion.23), calls=%async_computation.1 | async-start | bytes 262144 | tf_op jit(solution)/shard_map/all_to_all | solution.py:38
  58.1 0.8 reshape_broadcast_in_dim.7
  59.1 1.9 collective-permute-start.5
  61.0 4.1 %collective-permute-start.4 = (bf16[32,64]{0,1:T(8,128)(2,1)S(1)}, bf16[32,64]{0,1:T(8,128)(2,1)S(1)}, u32[]{:S(2)}, u32[]{:S(2)}) collective-permute-start(bf16[32,64]{0,1:T(8,128)(2,1)S(1)} %get-tuple-element.47), channel_id=1, source_target_pairs={{0,2},{1,3},{2,0},{3,1},{4,6},{5,7},{6,4},{7,5},{8,10},{9,11},{10,... | collective-permute-start | bytes 12296 | tf_op jit(solution)/shard_map/ppermute | solution.py:163
  65.1 1.9 collective-permute-start.3
  67.5 0.4 fusion.66
  69.5 0.6 broadcast_in_dim.31
  70.1 5.4 %all-to-all-start.2 = ((bf16[8,8,256]{2,1,0:T(8,128)(2,1)}), bf16[8,8,256]{2,1,0:T(8,128)(2,1)S(1)}, u32[]{:S(2)}, u32[]{:S(2)}) async-start(bf16[8,8,256]{2,1,0:T(8,128)(2,1)} %broadcast_in_dim.31), calls=%async_computation.2 | async-start | bytes 65536 | tf_op jit(solution)/shard_map/all_to_all | solution.py:38
  75.5 4.7 %all-to-all-done.2 = bf16[8,8,256]{2,1,0:T(8,128)(2,1)S(1)} async-done(((bf16[8,8,256]{2,1,0:T(8,128)(2,1)}), bf16[8,8,256]{2,1,0:T(8,128)(2,1)S(1)}, u32[]{:S(2)}, u32[]{:S(2)}) %all-to-all-start.2) | async-done | bytes 32800 | tf_op jit(solution)/shard_map/all_to_all | solution.py:38
  80.3 0.7 broadcast_in_dim.33
  81.0 6.2 %all-to-all-start.3 = ((bf16[32,8,256]{2,1,0:T(8,128)(2,1)}), bf16[32,8,256]{2,1,0:T(8,128)(2,1)S(1)}, u32[]{:S(2)}, u32[]{:S(2)}) async-start(bf16[32,8,256]{2,1,0:T(8,128)(2,1)} %bitcast.32), calls=%async_computation.3 | async-start | bytes 262144 | tf_op jit(solution)/shard_map/all_to_all | solution.py:38
  87.3 7.4 %all-to-all-done.3 = bf16[32,8,256]{2,1,0:T(8,128)(2,1)S(1)} async-done(((bf16[32,8,256]{2,1,0:T(8,128)(2,1)}), bf16[32,8,256]{2,1,0:T(8,128)(2,1)S(1)}, u32[]{:S(2)}, u32[]{:S(2)}) %all-to-all-start.3) | async-done | bytes 131104 | tf_op jit(solution)/shard_map/all_to_all | solution.py:38
  96.0 0.8 broadcast_in_dim.35
  96.8 14.2 %all-to-all-start.4 = ((bf16[128,2,512]{2,1,0:T(2,128)(2,1)}), bf16[128,2,512]{2,1,0:T(2,128)(2,1)S(1)}, u32[]{:S(2)}, u32[]{:S(2)}) async-start(bf16[128,2,512]{2,1,0:T(2,128)(2,1)} %bitcast.49), calls=%async_computation.4 | async-start | bytes 524288 | tf_op jit(solution)/shard_map/all_to_all | solution.py:38
  111.0 14.1 %all-gather = bf16[2560,128]{1,0:T(8,128)(2,1)S(1)} all-gather(bf16[320,128]{1,0:T(8,128)(2,1)S(1)} %pad_maximum_fusion.2), channel_id=2, replica_groups=mesh['b'=8,'zp'=2,'x'=4,'c'=2,'tp'=4] {'x','c'}, dimensions={0}, use_global_device_ids=true | all-gather | bytes 737280 | tf_op jit(solution)/shard_map/all_gather | solution.py:272
  125.1 8.5 %all-to-all-done.4 = bf16[128,2,512]{2,1,0:T(2,128)(2,1)S(1)} async-done(((bf16[128,2,512]{2,1,0:T(2,128)(2,1)}), bf16[128,2,512]{2,1,0:T(2,128)(2,1)S(1)}, u32[]{:S(2)}, u32[]{:S(2)}) %all-to-all-start.4) | async-done | bytes 262176 | tf_op jit(solution)/shard_map/all_to_all | solution.py:38
  133.8 1.1 broadcast_in_dim.36
  134.9 3.5 %all-to-all-start.5 = ((bf16[4,256,512]{1,2,0:T(8,128)(2,1)}), bf16[4,256,512]{1,2,0:T(8,128)(2,1)S(1)}, u32[]{:S(2)}, u32[]{:S(2)}) async-start(bf16[4,256,512]{1,2,0:T(8,128)(2,1)} %broadcast_in_dim.36), calls=%async_computation.5 | async-start | bytes 2097152 | tf_op jit(solution)/shard_map/all_to_all | solution.py:38
  139.1 14.2 %all-to-all-done.5 = bf16[4,256,512]{1,2,0:T(8,128)(2,1)S(1)} async-done(((bf16[4,256,512]{1,2,0:T(8,128)(2,1)}), bf16[4,256,512]{1,2,0:T(8,128)(2,1)S(1)}, u32[]{:S(2)}, u32[]{:S(2)}) %all-to-all-start.5) | async-done | bytes 1048608 | tf_op jit(solution)/shard_map/all_to_all | solution.py:38
  154.4 0.4 copy-done.13
  154.7 0.4 fusion.2
  155.1 0.8 broadcast_in_dim.37
  155.9 3.5 %all-to-all-start.6 = ((bf16[4,208,256]{2,1,0:T(8,128)(2,1)}), bf16[4,208,256]{2,1,0:T(8,128)(2,1)S(1)}, u32[]{:S(2)}, u32[]{:S(2)}) async-start(bf16[4,208,256]{2,1,0:T(8,128)(2,1)} %broadcast_in_dim.37), calls=%async_computation.6 | async-start | bytes 851968 | tf_op jit(solution)/shard_map/all_to_all | solution.py:38
  159.4 1.2 pad_maximum_fusion
  160.6 5.7 %all-to-all-done.6 = bf16[4,208,256]{2,1,0:T(8,128)(2,1)S(1)} async-done(((bf16[4,208,256]{2,1,0:T(8,128)(2,1)}), bf16[4,208,256]{2,1,0:T(8,128)(2,1)S(1)}, u32[]{:S(2)}, u32[]{:S(2)}) %all-to-all-start.6) | async-done | bytes 426016 | tf_op jit(solution)/shard_map/all_to_all | solution.py:38
  166.4 0.4 fusion.12
  167.1 0.8 reshape.444
  167.9 9.4 %all-to-all-start.7 = ((bf16[128,2,512]{2,1,0:T(2,128)(2,1)}), bf16[128,2,512]{2,1,0:T(2,128)(2,1)S(1)}, u32[]{:S(2)}, u32[]{:S(2)}) async-start(bf16[128,2,512]{2,1,0:T(2,128)(2,1)} %reshape.444), calls=%async_computation.7 | async-start | bytes 524288 | tf_op jit(solution)/shard_map/all_to_all | solution.py:38
  178.1 21.8 %all-to-all-done.7 = bf16[128,2,512]{2,1,0:T(2,128)(2,1)S(1)} async-done(((bf16[128,2,512]{2,1,0:T(2,128)(2,1)}), bf16[128,2,512]{2,1,0:T(2,128)(2,1)S(1)}, u32[]{:S(2)}, u32[]{:S(2)}) %all-to-all-start.7) | async-done | bytes 262176 | tf_op jit(solution)/shard_map/all_to_all | solution.py:38
  200.0 0.8 fusion.6
  (134 shorter events, 8.6 us)
Async XLA Ops:
  0.0 153.9 %copy-start = (bf16[1,2048,176]{1,2,0:T(8,128)(2,1)S(1)}, bf16[1,2048,176]{1,2,0:T(8,128)(2,1)}, u32[]{:S(2)}) copy-start(bf16[1,2048,176]{1,2,0:T(8,128)(2,1)} %param.43) | copy-start | bytes 2162692
  0.0 19.4 %copy-start.1 = (bf16[1,176,2048]{2,1,0:T(8,128)(2,1)S(1)}, bf16[1,176,2048]{2,1,0:T(8,128)(2,1)}, u32[]{:S(2)}) copy-start(bf16[1,176,2048]{2,1,0:T(8,128)(2,1)} %param.45) | copy-start | bytes 2162692
  0.0 31.2 %copy-start.5 = (bf16[8,2048]{1,0:T(8,128)(2,1)S(1)}, bf16[8,2048]{1,0:T(8,128)(2,1)}, u32[]{:S(2)}) copy-start(bf16[8,2048]{1,0:T(8,128)(2,1)} %param.23) | copy-start | bytes 98308
  4.8 48.4 %all-to-all-start = ((bf16[16,16,896]{2,1,0:T(8,128)(2,1)}), bf16[16,16,896]{2,1,0:T(8,128)(2,1)S(1)}, u32[]{:S(2)}, u32[]{:S(2)}) async-start(bf16[16,16,896]{2,1,0:T(8,128)(2,1)} %message.1), calls=%async_computation | async-start | bytes 917504 | tf_op jit(solution)/shard_map/all_to_all | solution.py:38
  20.4 12.9 %copy-start.6 = (f32[2048]{0:T(1024)S(1)}, f32[2048]{0:T(1024)}, u32[]{:S(2)}) copy-start(f32[2048]{0:T(1024)} %param.24) | copy-start | bytes 24580
  20.4 13.1 %copy-start.3 = (bf16[8,1,320,128]{3,2,1,0:T(8,128)(2,1)S(1)}, bf16[8,1,320,128]{3,2,1,0:T(8,128)(2,1)}, u32[]{:S(2)}) copy-start(bf16[8,1,320,128]{3,2,1,0:T(8,128)(2,1)} %param.31) | copy-start | bytes 1966084
  20.4 32.8 %collective-permute-start = (bf16[176,512]{1,0:T(8,128)(2,1)}, bf16[176,512]{1,0:T(8,128)(2,1)}, u32[]{:S(2)}, u32[]{:S(2)}) collective-permute-start(bf16[176,512]{1,0:T(8,128)(2,1)} %get-tuple-element.38), channel_id=1, source_target_pairs={{0,1},{1,2},{2,3},{3,0},{4,5},{5,6},{6,7},{7,4},{8,9},{9,10},{10,1... | collective-permute-start | bytes 540680 | tf_op jit(solution)/shard_map/ppermute | solution.py:163
  23.7 29.5 %collective-permute-start.1 = (bf16[176,512]{1,0:T(8,128)(2,1)}, bf16[176,512]{1,0:T(8,128)(2,1)}, u32[]{:S(2)}, u32[]{:S(2)}) collective-permute-start(bf16[176,512]{1,0:T(8,128)(2,1)} %get-tuple-element.40), channel_id=1, source_target_pairs={{0,2},{1,3},{2,0},{3,1},{4,6},{5,7},{6,4},{7,5},{8,10},{9,11},{10,... | collective-permute-start | bytes 540680 | tf_op jit(solution)/shard_map/ppermute | solution.py:163
  28.2 25.0 %collective-permute-start.2 = (bf16[176,512]{1,0:T(8,128)(2,1)}, bf16[176,512]{1,0:T(8,128)(2,1)}, u32[]{:S(2)}, u32[]{:S(2)}) collective-permute-start(bf16[176,512]{1,0:T(8,128)(2,1)} %get-tuple-element.37), channel_id=1, source_target_pairs={{0,3},{1,0},{2,1},{3,2},{4,7},{5,4},{6,5},{7,6},{8,11},{9,8},{10,9... | collective-permute-start | bytes 540680 | tf_op jit(solution)/shard_map/ppermute | solution.py:163
  34.0 17.7 %copy-start.8 = (f32[8,2]{0,1:T(2,128)S(1)}, f32[8,2]{0,1:T(2,128)}, u32[]{:S(2)}) copy-start(f32[8,2]{0,1:T(2,128)} %param.42) | copy-start | bytes 196
  34.7 32.7 %copy-start.9 = (f32[64]{0:T(128)S(1)}, f32[64]{0:T(128)}, u32[]{:S(2)}) copy-start(f32[64]{0:T(128)} %param.28) | copy-start | bytes 772
  34.7 32.8 %copy-start.10 = (f32[64]{0:T(128)S(1)}, f32[64]{0:T(128)}, u32[]{:S(2)}) copy-start(f32[64]{0:T(128)} %param.29) | copy-start | bytes 772
  54.1 14.6 %copy-start.12 = (f32[2]{0:T(128)S(1)}, f32[2]{0:T(128)}, u32[]{:S(2)}) copy-start(f32[2]{0:T(128)} %param.30) | copy-start | bytes 28
  54.1 14.9 %copy-start.14 = (bf16[8,1,320,128]{3,2,1,0:T(8,128)(2,1)S(1)}, bf16[8,1,320,128]{3,2,1,0:T(8,128)(2,1)}, u32[]{:S(2)}) copy-start(bf16[8,1,320,128]{3,2,1,0:T(8,128)(2,1)} %param.32) | copy-start | bytes 1966084
  54.1 12.9 %all-to-all-start.1 = ((f32[8,8,512]{2,1,0:T(8,128)}), f32[8,8,512]{2,1,0:T(8,128)S(1)}, u32[]{:S(2)}, u32[]{:S(2)}) async-start(f32[8,8,512]{2,1,0:T(8,128)} %fusion.23), calls=%async_computation.1 | async-start | bytes 262144 | tf_op jit(solution)/shard_map/all_to_all | solution.py:38
  59.1 10.3 %copy-start.11 = (f32[128]{0:T(128)S(1)}, f32[128]{0:T(128)}, u32[]{:S(2)}) copy-start(f32[128]{0:T(128)} %param.34) | copy-start | bytes 1540
  59.1 16.4 %collective-permute-start.5 = (bf16[32,64]{0,1:T(8,128)(2,1)S(1)}, bf16[32,64]{0,1:T(8,128)(2,1)S(1)}, u32[]{:S(2)}, u32[]{:S(2)}) collective-permute-start(bf16[32,64]{0,1:T(8,128)(2,1)S(1)} %get-tuple-element.46), channel_id=1, source_target_pairs={{0,3},{1,0},{2,1},{3,2},{4,7},{5,4},{6,5},{7,6},{8,11},{9,8},{10,9... | collective-permute-start | bytes 12296 | tf_op jit(solution)/shard_map/ppermute | solution.py:163
  61.0 14.5 %collective-permute-start.4 = (bf16[32,64]{0,1:T(8,128)(2,1)S(1)}, bf16[32,64]{0,1:T(8,128)(2,1)S(1)}, u32[]{:S(2)}, u32[]{:S(2)}) collective-permute-start(bf16[32,64]{0,1:T(8,128)(2,1)S(1)} %get-tuple-element.47), channel_id=1, source_target_pairs={{0,2},{1,3},{2,0},{3,1},{4,6},{5,7},{6,4},{7,5},{8,10},{9,11},{10,... | collective-permute-start | bytes 12296 | tf_op jit(solution)/shard_map/ppermute | solution.py:163
  65.1 10.4 %collective-permute-start.3 = (bf16[32,64]{0,1:T(8,128)(2,1)S(1)}, bf16[32,64]{0,1:T(8,128)(2,1)S(1)}, u32[]{:S(2)}, u32[]{:S(2)}) collective-permute-start(bf16[32,64]{0,1:T(8,128)(2,1)S(1)} %get-tuple-element.48), channel_id=1, source_target_pairs={{0,1},{1,2},{2,3},{3,0},{4,5},{5,6},{6,7},{7,4},{8,9},{9,10},{10,1... | collective-permute-start | bytes 12296 | tf_op jit(solution)/shard_map/ppermute | solution.py:163
  67.9 26.9 %copy-start.4 = (f32[8,8,256]{2,1,0:T(8,128)S(1)}, f32[8,8,256]{2,1,0:T(8,128)}, u32[]{:S(2)}) copy-start(f32[8,8,256]{2,1,0:T(8,128)} %reshape.445) | copy-start | bytes 196612
  70.1 10.1 %all-to-all-start.2 = ((bf16[8,8,256]{2,1,0:T(8,128)(2,1)}), bf16[8,8,256]{2,1,0:T(8,128)(2,1)S(1)}, u32[]{:S(2)}, u32[]{:S(2)}) async-start(bf16[8,8,256]{2,1,0:T(8,128)(2,1)} %broadcast_in_dim.31), calls=%async_computation.2 | async-start | bytes 65536 | tf_op jit(solution)/shard_map/all_to_all | solution.py:38
  81.0 13.7 %all-to-all-start.3 = ((bf16[32,8,256]{2,1,0:T(8,128)(2,1)}), bf16[32,8,256]{2,1,0:T(8,128)(2,1)S(1)}, u32[]{:S(2)}, u32[]{:S(2)}) async-start(bf16[32,8,256]{2,1,0:T(8,128)(2,1)} %bitcast.32), calls=%async_computation.3 | async-start | bytes 262144 | tf_op jit(solution)/shard_map/all_to_all | solution.py:38
  96.8 36.7 %all-to-all-start.4 = ((bf16[128,2,512]{2,1,0:T(2,128)(2,1)}), bf16[128,2,512]{2,1,0:T(2,128)(2,1)S(1)}, u32[]{:S(2)}, u32[]{:S(2)}) async-start(bf16[128,2,512]{2,1,0:T(2,128)(2,1)} %bitcast.49), calls=%async_computation.4 | async-start | bytes 524288 | tf_op jit(solution)/shard_map/all_to_all | solution.py:38
  133.8 4.6 %copy-start.7 = (f32[2048]{0:T(1024)S(1)}, f32[2048]{0:T(1024)}, u32[]{:S(2)}) copy-start(f32[2048]{0:T(1024)} %param.40) | copy-start | bytes 24580
  134.9 18.4 %all-to-all-start.5 = ((bf16[4,256,512]{1,2,0:T(8,128)(2,1)}), bf16[4,256,512]{1,2,0:T(8,128)(2,1)S(1)}, u32[]{:S(2)}, u32[]{:S(2)}) async-start(bf16[4,256,512]{1,2,0:T(8,128)(2,1)} %broadcast_in_dim.36), calls=%async_computation.5 | async-start | bytes 2097152 | tf_op jit(solution)/shard_map/all_to_all | solution.py:38
  153.6 1.1 copy-start.13
  154.7 4.7 %copy-start.2 = (bf16[176,512]{1,0:T(8,128)(2,1)S(1)}, bf16[176,512]{1,0:T(8,128)(2,1)}, u32[]{:S(2)}) copy-start(bf16[176,512]{1,0:T(8,128)(2,1)} %get-tuple-element.26) | copy-start | bytes 540676
  155.9 10.5 %all-to-all-start.6 = ((bf16[4,208,256]{2,1,0:T(8,128)(2,1)}), bf16[4,208,256]{2,1,0:T(8,128)(2,1)S(1)}, u32[]{:S(2)}, u32[]{:S(2)}) async-start(bf16[4,208,256]{2,1,0:T(8,128)(2,1)} %broadcast_in_dim.37), calls=%async_computation.6 | async-start | bytes 851968 | tf_op jit(solution)/shard_map/all_to_all | solution.py:38
  167.9 32.0 %all-to-all-start.7 = ((bf16[128,2,512]{2,1,0:T(2,128)(2,1)}), bf16[128,2,512]{2,1,0:T(2,128)(2,1)S(1)}, u32[]{:S(2)}, u32[]{:S(2)}) async-start(bf16[128,2,512]{2,1,0:T(2,128)(2,1)} %reshape.444), calls=%async_computation.7 | async-start | bytes 524288 | tf_op jit(solution)/shard_map/all_to_all | solution.py:38

commit v5 on v4

--- a/solution.py
+++ b/solution.py
@@ -4,6 +4,7 @@
 from jax.experimental import pallas as pl
 from jax.experimental.pallas import tpu as pltpu
 from jax.sharding import Mesh, PartitionSpec as P
+
 
 SUB = 64
 VD = 128
@@ -120,19 +121,32 @@
     picked = (slot_codes[:, :, None] == slots_iota).astype(jnp.float32)
     select = jnp.sum(picked, axis=1)
     combine_weights = jnp.sum(picked * expert_probs[:, :, None], axis=1)
-    lead_scale = jnp.sum(picked[:, 0] / expert_probs[:, :1], axis=0)
-    return (select, combine_weights, lead_scale)
-
-
-def split_pair(values):
-    high = lax.reduce_precision(values, 8, 7)
-    return high.astype(jnp.bfloat16), (values - high).astype(jnp.bfloat16)
-
-
-def message_body(query, key, value, out, gate, up, down, tags, message):
+    return (select, combine_weights)
+
+
+def message_body(ids, probs, query, key, value, out, gate, up, down, message):
     lanes = lax.broadcasted_iota(jnp.int32, (16, 256), 1)
+    narrow = lax.broadcasted_iota(jnp.int32, (16, 128), 1)
+    places = lax.broadcasted_iota(jnp.int32, (16, 128), 0)
     shared = jnp.concatenate((query[...], key[...], value[...], out[...]), axis=1)
     wide = [part[...].astype(jnp.float32) for part in (gate, up, down)]
+    tags = [jnp.zeros((16, 128), jnp.float32) for _ in range(2)]
+    for row in range(SEQ):
+        chosen = ids[0, row]
+        rank = jnp.int32(0)
+        for earlier in range(row):
+            for choice in range(TOP):
+                rank = rank + (ids[choice, earlier] == chosen).astype(jnp.int32)
+        slot = chosen * CAP + rank
+        for half in range(2):
+            tags[half] = jnp.where(places + 16 * half == slot, probs[0, row], tags[half])
+    for half in range(2):
+        used = tags[half] > 0.0
+        inverse = jnp.where(used, 1.0 / jnp.where(used, tags[half], 1.0), 0.0)
+        high = inverse.astype(jnp.bfloat16).astype(jnp.float32)
+        tags[half] = jnp.where(
+            narrow == 96, high, jnp.where(narrow == 97, inverse - high, 0.0)
+        )
     for rep in range(REP):
         turned = [
             pltpu.roll(part, (32 * (place - rep)) % 256, 1) for place, part in enumerate(wide)
@@ -140,18 +154,21 @@
         own = jnp.where(
             lanes < 32, turned[0], jnp.where(lanes < 64, turned[1], turned[2])
         )[:, :128]
-        own = jnp.where(lanes[:, :128] < 96, own, 0.0)
+        own = jnp.where(narrow < 96, own, 0.0)
         for half in range(2):
             message[2 * rep + half, :, :768] = shared
             message[2 * rep + half, :, 768:] = (own + tags[half]).astype(jnp.bfloat16)
 
 
-def build_message(*parts):
+def build_message(ids, probs, *parts):
+    scalars = pl.BlockSpec(memory_space=pltpu.SMEM)
+    whole = pl.BlockSpec(memory_space=pltpu.VMEM)
     return pl.pallas_call(
         message_body,
+        in_specs=[scalars, scalars] + [whole] * len(parts),
         out_shape=jax.ShapeDtypeStruct((N_Z, 16, 896), jnp.bfloat16),
         name="message",
-    )(*parts)
+    )(ids, probs, *parts)
 
 
 def trade_columns(weight, tp_index):
@@ -210,11 +227,10 @@
     tp_start = tp_index * share_width
     block = width // N_XC
 
-    select, combine_weights, lead_scale = route_tables(expert_ids, expert_probs)
-    high, low = split_pair(lead_scale)
-    tags = jnp.concatenate((high.reshape(2, 16, 1), low.reshape(2, 16, 1)), axis=2)
-    tags = jnp.pad(tags.astype(jnp.float32), ((0, 0), (0, 0), (96, 30)))
+    select, combine_weights = route_tables(expert_ids, expert_probs)
     message = build_message(
+        expert_ids.T,
+        expert_probs.T,
         query_weight,
         key_weight,
         value_weight,
@@ -222,12 +238,8 @@
         dense_gate_weight,
         dense_up_weight,
         dense_down_weight.T,
-        tags,
     )
     held = exchange(message, Z).reshape(N_Z * 16, 896)
-    down = trade_columns(expert_down[0], tp_index)
-    held, down = lax.optimization_barrier((held, down))
-    down = in_order(down, tp_index)
     dense_down = in_order(trade_columns(held[:, 832:864].T, tp_index), tp_index)
 
     residual = to_mixed(tokens).astype(jnp.float32)
@@ -268,6 +280,7 @@
     ).reshape(N_EP, CAP, share_width)
     incoming = exchange(outgoing, EP).reshape(N_EP * CAP, share_width)
 
+    down = in_order(trade_columns(expert_down[0], tp_index), tp_index)
     dense_held = jnp.concatenate((held[:, 768:], dense_down.T), axis=0)
     dense_held = lax.all_gather(dense_held, XC, axis=0)
     incoming, dense_held = lax.optimization_barrier((incoming, dense_held))

time: 202 us -> 191 us (0.946)
  waiting for transfers between devices: 62.3 us -> 50.3 us
    all_to_all x8, waiting for transfers between devices: 62.3 us -> 47.9 us  [exchange(): return lax.all_to_all(values, axes, split_axis=0, concat_axis=0, tiled=True)]
    ppermute x6, waiting for transfers between devices: 0.02 us -> 2.36 us  [trade_columns(): kept.append(lax.ppermute(sent, 'tp', pairs))]
  transfers between devices with their start and end apart: 14 -> 14, of which waited for: 6 -> 7; matrix products, arithmetic and copies ran while one was open for 7% -> 11% of each run, Pallas kernels for 0% -> 0%
where the time goes in v5:
time: 191 us; the launch traced here: 190 us
  starting transfers between devices  81.2 us (43%)
  waiting for transfers between devices  50.3 us (26%)
  blocking collectives  28.3 us (15%)
  local copies, waits for them, and re-layouts  15.2 us (8%)
  other arithmetic  7.91 us (4%)
  matrix products  4.66 us (2%)
    all_to_all x8, starting transfers between devices, exchange(): return lax.all_to_all(values, axes, split_axis=0, concat_axis=0, tiled=True)  62.3 us
    all_to_all x8, waiting for transfers between devices, exchange(): return lax.all_to_all(values, axes, split_axis=0, concat_axis=0, tiled=True)  47.9 us
    ppermute x6, starting transfers between devices, trade_columns(): kept.append(lax.ppermute(sent, 'tp', pairs))  19 us
    all_gather x1, blocking collectives, shards(): spread = lax.all_gather(normed, XC, axis=0)  14.2 us
    all_gather x1, blocking collectives, shards(): dense_held = lax.all_gather(dense_held, XC, axis=0)  14.1 us
  transfers between devices with their start and end apart: 14, of which 7 were waited for; matrix products, arithmetic and copies ran while one was open for 11% of the time, Pallas kernels for 0%

profile of v5, /device:TPU:33, one launch (start us, length us, event | category | flops | bytes accessed | tf_op | source)
XLA Modules:
  0.0 190.1 jit_solution(15799201841516821137)
XLA Ops:
  0.0 1.7 message.1
  1.8 14.7 %all-to-all-start = ((bf16[16,16,896]{2,1,0:T(8,128)(2,1)}), bf16[16,16,896]{2,1,0:T(8,128)(2,1)S(1)}, u32[]{:S(2)}, u32[]{:S(2)}) async-start(bf16[16,16,896]{2,1,0:T(8,128)(2,1)} %message.1), calls=%async_computation | async-start | bytes 917504 | tf_op jit(solution)/shard_map/all_to_all | solution.py:39
  16.4 0.8 copy.96
  17.2 1.0 reshape.420
  18.3 0.9 reshape.415
  19.2 0.9 reshape.416
  20.4 0.7 copy.98
  21.7 0.7 reduce_sum.141
  22.5 0.9 multiply_reduce_fusion.2
  23.4 0.9 fusion.26
  24.3 14.2 %all_gather.10 = bf16[8,8,8,256]{3,2,0,1:T(8,128)(2,1)S(1)} all-gather(bf16[1,8,8,256]{3,2,0,1:T(8,128)(2,1)S(1)} %fusion.26), channel_id=1, replica_groups=mesh['b'=8,'zp'=2,'x'=4,'c'=2,'tp'=4] {'x','c'}, dimensions={0}, use_global_device_ids=true | all-gather | bytes 294912 | tf_op jit(solution)/shard_map/all_gather | solution.py:248
  38.6 0.8 convert_reduce_fusion.2
  39.3 0.7 iota_compare_fusion
  40.1 0.8 add_rsqrt_fusion
  40.8 0.8 fusion.23
  41.7 5.4 %all-to-all-start.1 = ((f32[8,8,512]{2,1,0:T(8,128)}), f32[8,8,512]{2,1,0:T(8,128)S(1)}, u32[]{:S(2)}, u32[]{:S(2)}) async-start(f32[8,8,512]{2,1,0:T(8,128)} %fusion.23), calls=%async_computation.1 | async-start | bytes 262144 | tf_op jit(solution)/shard_map/all_to_all | solution.py:39
  47.4 4.6 %collective-permute-start.2 = (bf16[32,64]{0,1:T(8,128)(2,1)S(1)}, bf16[32,64]{0,1:T(8,128)(2,1)S(1)}, u32[]{:S(2)}, u32[]{:S(2)}) collective-permute-start(bf16[32,64]{0,1:T(8,128)(2,1)S(1)} %get-tuple-element.36), channel_id=1, source_target_pairs={{0,3},{1,0},{2,1},{3,2},{4,7},{5,4},{6,5},{7,6},{8,11},{9,8},{10,9... | collective-permute-start | bytes 12296 | tf_op jit(solution)/shard_map/ppermute | solution.py:180
  52.0 2.3 %collective-permute-start.1 = (bf16[32,64]{0,1:T(8,128)(2,1)S(1)}, bf16[32,64]{0,1:T(8,128)(2,1)S(1)}, u32[]{:S(2)}, u32[]{:S(2)}) collective-permute-start(bf16[32,64]{0,1:T(8,128)(2,1)S(1)} %get-tuple-element.37), channel_id=1, source_target_pairs={{0,2},{1,3},{2,0},{3,1},{4,6},{5,7},{6,4},{7,5},{8,10},{9,11},{10,... | collective-permute-start | bytes 12296 | tf_op jit(solution)/shard_map/ppermute | solution.py:180
  54.3 2.6 %collective-permute-start = (bf16[32,64]{0,1:T(8,128)(2,1)S(1)}, bf16[32,64]{0,1:T(8,128)(2,1)S(1)}, u32[]{:S(2)}, u32[]{:S(2)}) collective-permute-start(bf16[32,64]{0,1:T(8,128)(2,1)S(1)} %get-tuple-element.38), channel_id=1, source_target_pairs={{0,1},{1,2},{2,3},{3,0},{4,5},{5,6},{6,7},{7,4},{8,9},{9,10},{10,1... | collective-permute-start | bytes 12296 | tf_op jit(solution)/shard_map/ppermute | solution.py:180
  57.3 0.4 fusion.54
  59.3 0.6 broadcast_in_dim.31
  59.9 5.6 %all-to-all-start.2 = ((bf16[8,8,256]{2,1,0:T(8,128)(2,1)}), bf16[8,8,256]{2,1,0:T(8,128)(2,1)S(1)}, u32[]{:S(2)}, u32[]{:S(2)}) async-start(bf16[8,8,256]{2,1,0:T(8,128)(2,1)} %broadcast_in_dim.31), calls=%async_computation.2 | async-start | bytes 65536 | tf_op jit(solution)/shard_map/all_to_all | solution.py:39
  65.6 4.7 %all-to-all-done.2 = bf16[8,8,256]{2,1,0:T(8,128)(2,1)S(1)} async-done(((bf16[8,8,256]{2,1,0:T(8,128)(2,1)}), bf16[8,8,256]{2,1,0:T(8,128)(2,1)S(1)}, u32[]{:S(2)}, u32[]{:S(2)}) %all-to-all-start.2) | async-done | bytes 32800 | tf_op jit(solution)/shard_map/all_to_all | solution.py:39
  70.5 0.7 broadcast_in_dim.33
  71.1 5.0 %all-to-all-start.3 = ((bf16[32,8,256]{2,1,0:T(8,128)(2,1)}), bf16[32,8,256]{2,1,0:T(8,128)(2,1)S(1)}, u32[]{:S(2)}, u32[]{:S(2)}) async-start(bf16[32,8,256]{2,1,0:T(8,128)(2,1)} %bitcast.28), calls=%async_computation.3 | async-start | bytes 262144 | tf_op jit(solution)/shard_map/all_to_all | solution.py:39
  76.3 7.4 %all-to-all-done.3 = bf16[32,8,256]{2,1,0:T(8,128)(2,1)S(1)} async-done(((bf16[32,8,256]{2,1,0:T(8,128)(2,1)}), bf16[32,8,256]{2,1,0:T(8,128)(2,1)S(1)}, u32[]{:S(2)}, u32[]{:S(2)}) %all-to-all-start.3) | async-done | bytes 131104 | tf_op jit(solution)/shard_map/all_to_all | solution.py:39
  85.0 0.8 broadcast_in_dim.35
  85.8 12.8 %all-to-all-start.4 = ((bf16[128,2,512]{2,1,0:T(2,128)(2,1)}), bf16[128,2,512]{2,1,0:T(2,128)(2,1)S(1)}, u32[]{:S(2)}, u32[]{:S(2)}) async-start(bf16[128,2,512]{2,1,0:T(2,128)(2,1)} %bitcast.45), calls=%async_computation.4 | async-start | bytes 524288 | tf_op jit(solution)/shard_map/all_to_all | solution.py:39
  98.6 14.1 %all-gather = bf16[2560,128]{1,0:T(8,128)(2,1)S(1)} all-gather(bf16[320,128]{1,0:T(8,128)(2,1)S(1)} %pad_maximum_fusion.2), channel_id=2, replica_groups=mesh['b'=8,'zp'=2,'x'=4,'c'=2,'tp'=4] {'x','c'}, dimensions={0}, use_global_device_ids=true | all-gather | bytes 737280 | tf_op jit(solution)/shard_map/all_gather | solution.py:285
  112.7 8.5 %all-to-all-done.4 = bf16[128,2,512]{2,1,0:T(2,128)(2,1)S(1)} async-done(((bf16[128,2,512]{2,1,0:T(2,128)(2,1)}), bf16[128,2,512]{2,1,0:T(2,128)(2,1)S(1)}, u32[]{:S(2)}, u32[]{:S(2)}) %all-to-all-start.4) | async-done | bytes 262176 | tf_op jit(solution)/shard_map/all_to_all | solution.py:39
  121.4 1.1 broadcast_in_dim.36
  122.5 3.6 %all-to-all-start.5 = ((bf16[4,256,512]{1,2,0:T(8,128)(2,1)}), bf16[4,256,512]{1,2,0:T(8,128)(2,1)S(1)}, u32[]{:S(2)}, u32[]{:S(2)}) async-start(bf16[4,256,512]{1,2,0:T(8,128)(2,1)} %broadcast_in_dim.36), calls=%async_computation.5 | async-start | bytes 2097152 | tf_op jit(solution)/shard_map/all_to_all | solution.py:39
  126.1 1.9 %constant_dynamic-slice_fusion = (bf16[1,176,512]{2,1,0:T(8,128)(2,1)S(1)}, bf16[176,512]{1,0:T(8,128)(2,1)S(1)}, bf16[176,512]{1,0:T(8,128)(2,1)}, bf16[176,512]{1,0:T(8,128)(2,1)S(1)}) fusion(bf16[1,176,2048]{2,1,0:T(8,128)(2,1)} %param.45, s32[]{:T(128)S(6)} %select_n.69, s32[]{:T(128)S(6)} %select_n.71, s32[]{:T(128)S(6)} %select_n.73, s32[]{:T(128)S(6)} %select_n.72), kind=kLoop, calls=%fused_computation.96 | loop fusion | bytes 1441808 | tf_op jit(solution)/shard_map/dynamic_slice | solution.py:196
  128.1 4.5 %collective-permute-start.5 = (bf16[176,512]{1,0:T(8,128)(2,1)}, bf16[176,512]{1,0:T(8,128)(2,1)S(1)}, u32[]{:S(2)}, u32[]{:S(2)}) collective-permute-start(bf16[176,512]{1,0:T(8,128)(2,1)} %get-tuple-element.29), channel_id=1, source_target_pairs={{0,3},{1,0},{2,1},{3,2},{4,7},{5,4},{6,5},{7,6},{8,11},{9,8},{10,9... | collective-permute-start | bytes 540680 | tf_op jit(solution)/shard_map/ppermute | solution.py:180
  132.6 2.5 %collective-permute-start.4 = (bf16[176,512]{1,0:T(8,128)(2,1)S(1)}, bf16[176,512]{1,0:T(8,128)(2,1)}, u32[]{:S(2)}, u32[]{:S(2)}) collective-permute-start(bf16[176,512]{1,0:T(8,128)(2,1)S(1)} %get-tuple-element.30), channel_id=1, source_target_pairs={{0,2},{1,3},{2,0},{3,1},{4,6},{5,7},{6,4},{7,5},{8,10},{9,11},{10,... | collective-permute-start | bytes 540680 | tf_op jit(solution)/shard_map/ppermute | solution.py:180
  135.1 2.5 %collective-permute-start.3 = (bf16[176,512]{1,0:T(8,128)(2,1)S(1)}, bf16[176,512]{1,0:T(8,128)(2,1)}, u32[]{:S(2)}, u32[]{:S(2)}) collective-permute-start(bf16[176,512]{1,0:T(8,128)(2,1)S(1)} %get-tuple-element.28), channel_id=1, source_target_pairs={{0,1},{1,2},{2,3},{3,0},{4,5},{5,6},{6,7},{7,4},{8,9},{9,10},{10,1... | collective-permute-start | bytes 540680 | tf_op jit(solution)/shard_map/ppermute | solution.py:180
  138.2 2.7 %all-to-all-done.5 = bf16[4,256,512]{1,2,0:T(8,128)(2,1)S(1)} async-done(((bf16[4,256,512]{1,2,0:T(8,128)(2,1)}), bf16[4,256,512]{1,2,0:T(8,128)(2,1)S(1)}, u32[]{:S(2)}, u32[]{:S(2)}) %all-to-all-start.5) | async-done | bytes 1048608 | tf_op jit(solution)/shard_map/all_to_all | solution.py:39
  142.0 0.4 copy-done.10
  142.9 0.8 broadcast_in_dim.37
  143.6 3.5 %all-to-all-start.6 = ((bf16[4,208,256]{2,1,0:T(8,128)(2,1)}), bf16[4,208,256]{2,1,0:T(8,128)(2,1)S(1)}, u32[]{:S(2)}, u32[]{:S(2)}) async-start(bf16[4,208,256]{2,1,0:T(8,128)(2,1)} %broadcast_in_dim.37), calls=%async_computation.6 | async-start | bytes 851968 | tf_op jit(solution)/shard_map/all_to_all | solution.py:39
  147.1 2.3 %collective-permute-done.3 = bf16[176,512]{1,0:T(8,128)(2,1)} collective-permute-done((bf16[176,512]{1,0:T(8,128)(2,1)S(1)}, bf16[176,512]{1,0:T(8,128)(2,1)}, u32[]{:S(2)}, u32[]{:S(2)}) %collective-permute-start.3) | collective-permute-done | bytes 180256 | tf_op jit(solution)/shard_map/ppermute | solution.py:180
  149.5 1.1 pad_maximum_fusion
  150.6 2.8 %all-to-all-done.6 = bf16[4,208,256]{2,1,0:T(8,128)(2,1)S(1)} async-done(((bf16[4,208,256]{2,1,0:T(8,128)(2,1)}), bf16[4,208,256]{2,1,0:T(8,128)(2,1)S(1)}, u32[]{:S(2)}, u32[]{:S(2)}) %all-to-all-start.6) | async-done | bytes 426016 | tf_op jit(solution)/shard_map/all_to_all | solution.py:39
  153.5 0.4 fusion.12
  154.2 0.8 reshape.414
  155.0 11.7 %all-to-all-start.7 = ((bf16[128,2,512]{2,1,0:T(2,128)(2,1)}), bf16[128,2,512]{2,1,0:T(2,128)(2,1)S(1)}, u32[]{:S(2)}, u32[]{:S(2)}) async-start(bf16[128,2,512]{2,1,0:T(2,128)(2,1)} %reshape.414), calls=%async_computation.7 | async-start | bytes 524288 | tf_op jit(solution)/shard_map/all_to_all | solution.py:39
  167.4 21.8 %all-to-all-done.7 = bf16[128,2,512]{2,1,0:T(2,128)(2,1)S(1)} async-done(((bf16[128,2,512]{2,1,0:T(2,128)(2,1)}), bf16[128,2,512]{2,1,0:T(2,128)(2,1)S(1)}, u32[]{:S(2)}, u32[]{:S(2)}) %all-to-all-start.7) | async-done | bytes 262176 | tf_op jit(solution)/shard_map/all_to_all | solution.py:39
  189.4 0.8 fusion.6
  (119 shorter events, 8.3 us)
Async XLA Ops:
  0.0 141.6 %copy-start = (bf16[1,2048,176]{1,2,0:T(8,128)(2,1)S(1)}, bf16[1,2048,176]{1,2,0:T(8,128)(2,1)}, u32[]{:S(2)}) copy-start(bf16[1,2048,176]{1,2,0:T(8,128)(2,1)} %param.43) | copy-start | bytes 2162692
  1.8 39.1 %all-to-all-start = ((bf16[16,16,896]{2,1,0:T(8,128)(2,1)}), bf16[16,16,896]{2,1,0:T(8,128)(2,1)S(1)}, u32[]{:S(2)}, u32[]{:S(2)}) async-start(bf16[16,16,896]{2,1,0:T(8,128)(2,1)} %message.1), calls=%async_computation | async-start | bytes 917504 | tf_op jit(solution)/shard_map/all_to_all | solution.py:39
  16.4 4.6 %copy-start.3 = (f32[2048]{0:T(1024)S(1)}, f32[2048]{0:T(1024)}, u32[]{:S(2)}) copy-start(f32[2048]{0:T(1024)} %param.24) | copy-start | bytes 24580
  17.2 4.0 %copy-start.1 = (bf16[8,1,320,128]{3,2,1,0:T(8,128)(2,1)S(1)}, bf16[8,1,320,128]{3,2,1,0:T(8,128)(2,1)}, u32[]{:S(2)}) copy-start(bf16[8,1,320,128]{3,2,1,0:T(8,128)(2,1)} %param.31) | copy-start | bytes 1966084
  21.7 25.3 %copy-start.4 = (f32[2048]{0:T(1024)S(1)}, f32[2048]{0:T(1024)}, u32[]{:S(2)}) copy-start(f32[2048]{0:T(1024)} %param.36) | copy-start | bytes 24580
  22.5 34.8 %copy-start.6 = (f32[64]{0:T(128)S(1)}, f32[64]{0:T(128)}, u32[]{:S(2)}) copy-start(f32[64]{0:T(128)} %param.28) | copy-start | bytes 772
  22.5 34.9 %copy-start.7 = (f32[64]{0:T(128)S(1)}, f32[64]{0:T(128)}, u32[]{:S(2)}) copy-start(f32[64]{0:T(128)} %param.29) | copy-start | bytes 772
  41.7 16.8 %copy-start.9 = (f32[2]{0:T(128)S(1)}, f32[2]{0:T(128)}, u32[]{:S(2)}) copy-start(f32[2]{0:T(128)} %param.30) | copy-start | bytes 28
  41.7 17.2 %copy-start.11 = (bf16[8,1,320,128]{3,2,1,0:T(8,128)(2,1)S(1)}, bf16[8,1,320,128]{3,2,1,0:T(8,128)(2,1)}, u32[]{:S(2)}) copy-start(bf16[8,1,320,128]{3,2,1,0:T(8,128)(2,1)} %param.32) | copy-start | bytes 1966084
  41.7 15.2 %all-to-all-start.1 = ((f32[8,8,512]{2,1,0:T(8,128)}), f32[8,8,512]{2,1,0:T(8,128)S(1)}, u32[]{:S(2)}, u32[]{:S(2)}) async-start(f32[8,8,512]{2,1,0:T(8,128)} %fusion.23), calls=%async_computation.1 | async-start | bytes 262144 | tf_op jit(solution)/shard_map/all_to_all | solution.py:39
  47.3 11.9 %copy-start.8 = (f32[128]{0:T(128)S(1)}, f32[128]{0:T(128)}, u32[]{:S(2)}) copy-start(f32[128]{0:T(128)} %param.34) | copy-start | bytes 1540
  47.4 18.2 %collective-permute-start.2 = (bf16[32,64]{0,1:T(8,128)(2,1)S(1)}, bf16[32,64]{0,1:T(8,128)(2,1)S(1)}, u32[]{:S(2)}, u32[]{:S(2)}) collective-permute-start(bf16[32,64]{0,1:T(8,128)(2,1)S(1)} %get-tuple-element.36), channel_id=1, source_target_pairs={{0,3},{1,0},{2,1},{3,2},{4,7},{5,4},{6,5},{7,6},{8,11},{9,8},{10,9... | collective-permute-start | bytes 12296 | tf_op jit(solution)/shard_map/ppermute | solution.py:180
  52.0 13.6 %collective-permute-start.1 = (bf16[32,64]{0,1:T(8,128)(2,1)S(1)}, bf16[32,64]{0,1:T(8,128)(2,1)S(1)}, u32[]{:S(2)}, u32[]{:S(2)}) collective-permute-start(bf16[32,64]{0,1:T(8,128)(2,1)S(1)} %get-tuple-element.37), channel_id=1, source_target_pairs={{0,2},{1,3},{2,0},{3,1},{4,6},{5,7},{6,4},{7,5},{8,10},{9,11},{10,... | collective-permute-start | bytes 12296 | tf_op jit(solution)/shard_map/ppermute | solution.py:180
  54.3 11.3 %collective-permute-start = (bf16[32,64]{0,1:T(8,128)(2,1)S(1)}, bf16[32,64]{0,1:T(8,128)(2,1)S(1)}, u32[]{:S(2)}, u32[]{:S(2)}) collective-permute-start(bf16[32,64]{0,1:T(8,128)(2,1)S(1)} %get-tuple-element.38), channel_id=1, source_target_pairs={{0,1},{1,2},{2,3},{3,0},{4,5},{5,6},{6,7},{7,4},{8,9},{9,10},{10,1... | collective-permute-start | bytes 12296 | tf_op jit(solution)/shard_map/ppermute | solution.py:180
  57.8 26.0 %copy-start.2 = (f32[8,8,256]{2,1,0:T(8,128)S(1)}, f32[8,8,256]{2,1,0:T(8,128)}, u32[]{:S(2)}) copy-start(f32[8,8,256]{2,1,0:T(8,128)} %reshape.415) | copy-start | bytes 196612
  59.9 10.4 %all-to-all-start.2 = ((bf16[8,8,256]{2,1,0:T(8,128)(2,1)}), bf16[8,8,256]{2,1,0:T(8,128)(2,1)S(1)}, u32[]{:S(2)}, u32[]{:S(2)}) async-start(bf16[8,8,256]{2,1,0:T(8,128)(2,1)} %broadcast_in_dim.31), calls=%async_computation.2 | async-start | bytes 65536 | tf_op jit(solution)/shard_map/all_to_all | solution.py:39
  71.1 12.6 %all-to-all-start.3 = ((bf16[32,8,256]{2,1,0:T(8,128)(2,1)}), bf16[32,8,256]{2,1,0:T(8,128)(2,1)S(1)}, u32[]{:S(2)}, u32[]{:S(2)}) async-start(bf16[32,8,256]{2,1,0:T(8,128)(2,1)} %bitcast.28), calls=%async_computation.3 | async-start | bytes 262144 | tf_op jit(solution)/shard_map/all_to_all | solution.py:39
  85.8 35.4 %all-to-all-start.4 = ((bf16[128,2,512]{2,1,0:T(2,128)(2,1)}), bf16[128,2,512]{2,1,0:T(2,128)(2,1)S(1)}, u32[]{:S(2)}, u32[]{:S(2)}) async-start(bf16[128,2,512]{2,1,0:T(2,128)(2,1)} %bitcast.45), calls=%async_computation.4 | async-start | bytes 524288 | tf_op jit(solution)/shard_map/all_to_all | solution.py:39
  122.5 15.1 %copy-start.5 = (f32[2048]{0:T(1024)S(1)}, f32[2048]{0:T(1024)}, u32[]{:S(2)}) copy-start(f32[2048]{0:T(1024)} %param.40) | copy-start | bytes 24580
  122.5 18.5 %all-to-all-start.5 = ((bf16[4,256,512]{1,2,0:T(8,128)(2,1)}), bf16[4,256,512]{1,2,0:T(8,128)(2,1)S(1)}, u32[]{:S(2)}, u32[]{:S(2)}) async-start(bf16[4,256,512]{1,2,0:T(8,128)(2,1)} %broadcast_in_dim.36), calls=%async_computation.5 | async-start | bytes 2097152 | tf_op jit(solution)/shard_map/all_to_all | solution.py:39
  128.1 19.1 %collective-permute-start.5 = (bf16[176,512]{1,0:T(8,128)(2,1)}, bf16[176,512]{1,0:T(8,128)(2,1)S(1)}, u32[]{:S(2)}, u32[]{:S(2)}) collective-permute-start(bf16[176,512]{1,0:T(8,128)(2,1)} %get-tuple-element.29), channel_id=1, source_target_pairs={{0,3},{1,0},{2,1},{3,2},{4,7},{5,4},{6,5},{7,6},{8,11},{9,8},{10,9... | collective-permute-start | bytes 540680 | tf_op jit(solution)/shard_map/ppermute | solution.py:180
  132.6 14.5 %collective-permute-start.4 = (bf16[176,512]{1,0:T(8,128)(2,1)S(1)}, bf16[176,512]{1,0:T(8,128)(2,1)}, u32[]{:S(2)}, u32[]{:S(2)}) collective-permute-start(bf16[176,512]{1,0:T(8,128)(2,1)S(1)} %get-tuple-element.30), channel_id=1, source_target_pairs={{0,2},{1,3},{2,0},{3,1},{4,6},{5,7},{6,4},{7,5},{8,10},{9,11},{10,... | collective-permute-start | bytes 540680 | tf_op jit(solution)/shard_map/ppermute | solution.py:180
  135.1 14.4 %collective-permute-start.3 = (bf16[176,512]{1,0:T(8,128)(2,1)S(1)}, bf16[176,512]{1,0:T(8,128)(2,1)}, u32[]{:S(2)}, u32[]{:S(2)}) collective-permute-start(bf16[176,512]{1,0:T(8,128)(2,1)S(1)} %get-tuple-element.28), channel_id=1, source_target_pairs={{0,1},{1,2},{2,3},{3,0},{4,5},{5,6},{6,7},{7,4},{8,9},{9,10},{10,1... | collective-permute-start | bytes 540680 | tf_op jit(solution)/shard_map/ppermute | solution.py:180
  141.3 1.1 copy-start.10
  143.6 9.8 %all-to-all-start.6 = ((bf16[4,208,256]{2,1,0:T(8,128)(2,1)}), bf16[4,208,256]{2,1,0:T(8,128)(2,1)S(1)}, u32[]{:S(2)}, u32[]{:S(2)}) async-start(bf16[4,208,256]{2,1,0:T(8,128)(2,1)} %broadcast_in_dim.37), calls=%async_computation.6 | async-start | bytes 851968 | tf_op jit(solution)/shard_map/all_to_all | solution.py:39
  155.0 34.3 %all-to-all-start.7 = ((bf16[128,2,512]{2,1,0:T(2,128)(2,1)}), bf16[128,2,512]{2,1,0:T(2,128)(2,1)S(1)}, u32[]{:S(2)}, u32[]{:S(2)}) async-start(bf16[128,2,512]{2,1,0:T(2,128)(2,1)} %reshape.414), calls=%async_computation.7 | async-start | bytes 524288 | tf_op jit(solution)/shard_map/all_to_all | solution.py:39

commit v6 on v5

--- a/solution.py
+++ b/solution.py
@@ -4,7 +4,6 @@
 from jax.experimental import pallas as pl
 from jax.experimental.pallas import tpu as pltpu
 from jax.sharding import Mesh, PartitionSpec as P
-
 
 SUB = 64
 VD = 128
@@ -171,27 +170,6 @@
     )(ids, probs, *parts)
 
 
-def trade_columns(weight, tp_index):
-    share = weight.shape[1] // N_TP
-    kept = [own_columns(weight, tp_index * share, share)]
-    for shift in (1, 2, 3):
-        sent = own_columns(weight, ((tp_index + shift) & 3) * share, share)
-        pairs = [(index, (index + shift) % N_TP) for index in range(N_TP)]
-        kept.append(lax.ppermute(sent, "tp", pairs))
-    return kept
-
-
-def in_order(kept, tp_index):
-    kept = jnp.stack(kept)
-    return jnp.concatenate(
-        [
-            lax.dynamic_index_in_dim(kept, (tp_index - index) & 3, 0, False)
-            for index in range(N_TP)
-        ],
-        axis=0,
-    )
-
-
 def own_columns(values, tp_start, share_width):
     return lax.dynamic_slice_in_dim(values, tp_start, share_width, 1)
 
@@ -239,31 +217,34 @@
         dense_up_weight,
         dense_down_weight.T,
     )
-    held = exchange(message, Z).reshape(N_Z * 16, 896)
-    dense_down = in_order(trade_columns(held[:, 832:864].T, tp_index), tp_index)
+    with jax.named_scope("hold"):
+        held = exchange(message, Z).reshape(N_Z * 16, 896)
 
     residual = to_mixed(tokens).astype(jnp.float32)
     normed = mixed_scale(residual, to_mixed(norm_gain[None])).astype(jnp.bfloat16)
     xc_index = lax.axis_index(XC)
-    spread = lax.all_gather(normed, XC, axis=0)
-    spread = lax.dynamic_index_in_dim(spread, xc_index, 1, False).reshape(N_XC * SEQ, block)
+    with jax.named_scope("spread"):
+        spread = lax.all_gather(normed, XC, axis=0)
+        spread = lax.dynamic_index_in_dim(spread, xc_index, 1, False).reshape(N_XC * SEQ, block)
 
     partial_rows = jnp.dot(spread, held[:, :512], preferred_element_type=jnp.float32)
-    packed = jnp.sum(exchange(partial_rows.reshape(N_XC, SEQ, 512), XC), axis=0)
+    with jax.named_scope("project"):
+        packed = jnp.sum(exchange(partial_rows.reshape(N_XC, SEQ, 512), XC), axis=0)
     head_out = attend(
         packed, key_cache, value_cache, lengths, query_gain, key_gain, lambdas, head_gain
     )
-    all_heads = gather_small(head_out, XC, N_XC).reshape(N_XC * SEQ, 256)
+    with jax.named_scope("heads"):
+        all_heads = gather_small(head_out, XC, N_XC).reshape(N_XC * SEQ, 256)
     attended_part = lax.dot_general(
         all_heads, held[:, 512:768], (((1,), (1,)), ((), ())), preferred_element_type=jnp.float32
     ).astype(jnp.bfloat16)
-    parts = exchange(
-        jnp.broadcast_to(
-            attended_part.reshape(N_XC, 1, SEQ, block), (N_XC, N_TP, SEQ, block)
-        ).reshape(N_XC * N_TP, SEQ, block),
-        XC + ("tp",),
-    ).reshape(N_XC, N_TP, SEQ, block)
-    parts, dense_down = lax.optimization_barrier((parts, dense_down))
+    with jax.named_scope("attended"):
+        parts = exchange(
+            jnp.broadcast_to(
+                attended_part.reshape(N_XC, 1, SEQ, block), (N_XC, N_TP, SEQ, block)
+            ).reshape(N_XC * N_TP, SEQ, block),
+            XC + ("tp",),
+        ).reshape(N_XC, N_TP, SEQ, block)
     attended = jnp.sum(parts.astype(jnp.float32), axis=1)
     middle_mixed = lax.optimization_barrier((residual + attended).astype(jnp.bfloat16))
     ffn_input = from_mixed(
@@ -278,24 +259,21 @@
     outgoing = jnp.broadcast_to(
         chosen.reshape(1, EXPERTS, CAP, share_width), (REP, EXPERTS, CAP, share_width)
     ).reshape(N_EP, CAP, share_width)
-    incoming = exchange(outgoing, EP).reshape(N_EP * CAP, share_width)
-
-    down = in_order(trade_columns(expert_down[0], tp_index), tp_index)
-    dense_held = jnp.concatenate((held[:, 768:], dense_down.T), axis=0)
-    dense_held = lax.all_gather(dense_held, XC, axis=0)
+    with jax.named_scope("route"):
+        incoming = exchange(outgoing, EP).reshape(N_EP * CAP, share_width)
+
+    with jax.named_scope("dense"):
+        dense_held = lax.all_gather(held[:, 768:], XC, axis=0).reshape(N_XC, N_Z, 16, 128)
     incoming, dense_held = lax.optimization_barrier((incoming, dense_held))
-    dense_down = (
-        dense_held[:, 256:].reshape(N_XC, 4, 16, 128).transpose(1, 0, 2, 3).reshape(512, 128)
-    )
-    dense_held = dense_held[:, :256].reshape(N_XC, N_Z, 16, 128)
     tag = lax.dynamic_slice_in_dim(dense_held, 2 * xc_index, CAP, 2)[..., 96:98]
     tag = jnp.sum(tag.transpose(1, 0, 2, 3).reshape(N_EP * CAP, 2).astype(jnp.float32), axis=1)
-    dense_held = dense_held.transpose(1, 0, 2, 3).reshape(width, 128)[:, :64]
-
-    rows = gather_small(incoming, "tp", N_TP)
-    rows, dense_held, dense_down, tag = lax.optimization_barrier(
-        (rows, dense_held, dense_down, tag)
-    )
+    dense_held = dense_held.transpose(1, 0, 2, 3).reshape(width, 128)
+    down = jnp.concatenate((expert_down[0], dense_held[:, 64:96].T), axis=0)
+    dense_held = dense_held[:, :64]
+
+    with jax.named_scope("join"):
+        rows = gather_small(incoming, "tp", N_TP)
+    rows, dense_held, down, tag = lax.optimization_barrier((rows, dense_held, down, tag))
     rows = rows.transpose(1, 0, 2).reshape(N_EP * CAP, width)
     branch_weight = jax.nn.sigmoid(jnp.sum(rows.astype(jnp.float32) * branch_gate, axis=1))
     dense_scale = branch_weight * tag
@@ -310,19 +288,16 @@
     dense_hidden = (
         jax.nn.silu(dense_both[:32]) * dense_both[32:] * dense_scale[None]
     ).astype(jnp.bfloat16)
-    all_hidden = gather_small(jnp.concatenate((hidden, dense_hidden), axis=0), "tp", N_TP)
-
-    def summed(values, weight):
-        return lax.dot_general(
-            values.reshape(-1, N_EP * CAP),
-            weight,
-            (((0,), (0,)), ((), ())),
-            preferred_element_type=jnp.float32,
-        )
-
-    block_out = summed(all_hidden[:, :176], down) + summed(all_hidden[:, 176:], dense_down.T)
+    all_hidden = jnp.concatenate((hidden, dense_hidden), axis=0)
+    parts = lax.dot_general(
+        all_hidden, down, (((0,), (0,)), ((), ())), preferred_element_type=jnp.float32
+    ).astype(jnp.bfloat16)
+    parts = parts.reshape(N_EP * CAP, N_TP, share_width).transpose(1, 0, 2)
+    with jax.named_scope("reduce"):
+        block_out = jnp.sum(exchange(parts, "tp").astype(jnp.float32), axis=0)
     block_out = block_out.astype(jnp.bfloat16).reshape(N_EP, CAP, share_width)
-    returned = exchange(block_out, EP)
+    with jax.named_scope("return"):
+        returned = exchange(block_out, EP)
     expert_out = jnp.sum(
         returned.reshape(REP, EXPERTS * CAP, share_width).astype(jnp.float32), axis=0
     )

time: 191 us -> 187 us (0.979)
  starting transfers between devices: 81.2 us -> 54.3 us
  blocking collectives: 28.3 us -> 44.5 us
  waiting for transfers between devices: 50.3 us -> 63.1 us
  local copies, waits for them, and re-layouts: 15.2 us -> 11.7 us
  other arithmetic: 7.91 us -> 4.92 us
    ppermute x6 -> x0, starting transfers between devices: 19 us -> none  [trade_columns(): kept.append(lax.ppermute(sent, 'tp', pairs))]
    all_to_all x0 -> x1, blocking collectives: none -> 16.4 us  [exchange(): return lax.all_to_all(values, axes, split_axis=0, concat_axis=0, tiled=True)]
    all_to_all x8 -> x7, waiting for transfers between devices: 47.9 us -> 63.1 us  [exchange(): return lax.all_to_all(values, axes, split_axis=0, concat_axis=0, tiled=True)]
    all_to_all x8 -> x7, starting transfers between devices: 62.3 us -> 54.3 us  [exchange(): return lax.all_to_all(values, axes, split_axis=0, concat_axis=0, tiled=True)]
    ppermute x6 -> x0, waiting for transfers between devices: 2.36 us -> none  [trade_columns(): kept.append(lax.ppermute(sent, 'tp', pairs))]
    dynamic_slice x1 -> x0, local copies, waits for them, and re-layouts: 1.92 us -> none  [own_columns(): return lax.dynamic_slice_in_dim(values, tp_start, share_width, 1)]
  transfers between devices with their start and end apart: 14 -> 7, of which waited for: 7 -> 7; matrix products, arithmetic and copies ran while one was open for 11% -> 5% of each run, Pallas kernels for 0% -> 0%
where the time goes in v6:
time: 187 us; the launch traced here: 186 us
  waiting for transfers between devices  63.1 us (34%)
  starting transfers between devices  54.3 us (29%)
  blocking collectives  44.5 us (24%)
  local copies, waits for them, and re-layouts  11.7 us (6%)
  matrix products  5.59 us (3%)
  other arithmetic  4.92 us (3%)
    all_to_all x7, waiting for transfers between devices, exchange(): return lax.all_to_all(values, axes, split_axis=0, concat_axis=0, tiled=True)  63.1 us
    all_to_all x7, starting transfers between devices, exchange(): return lax.all_to_all(values, axes, split_axis=0, concat_axis=0, tiled=True)  54.3 us
    all_to_all x1, blocking collectives, exchange(): return lax.all_to_all(values, axes, split_axis=0, concat_axis=0, tiled=True)  16.4 us
    all_gather x1, blocking collectives, shards(): spread = lax.all_gather(normed, XC, axis=0)  14.3 us
    all_gather x1, blocking collectives, shards(): lax.all_gather(held[:, 768:], XC, axis=0).reshape(N_XC, N_Z, 16, 128)  13.8 us
  transfers between devices with their start and end apart: 7, of which 7 were waited for; matrix products, arithmetic and copies ran while one was open for 5% of the time, Pallas kernels for 0%

profile of v6, /device:TPU:33, one launch (start us, length us, event | category | flops | bytes accessed | tf_op | source)
XLA Modules:
  0.0 186.5 jit_solution(11772787087500565204)
XLA Ops:
  0.0 1.7 message.1
  1.7 14.8 %all-to-all-start = ((bf16[16,16,896]{2,1,0:T(8,128)(2,1)}), bf16[16,16,896]{2,1,0:T(8,128)(2,1)S(1)}, u32[]{:S(2)}, u32[]{:S(2)}) async-start(bf16[16,16,896]{2,1,0:T(8,128)(2,1)} %message.1), calls=%async_computation | async-start | bytes 917504 | tf_op jit(solution)/shard_map/hold/all_to_all | solution.py:38
  16.5 0.8 copy.100
  17.4 1.0 reshape.402
  18.5 0.2 reshape.397
  18.9 1.2 copy.90
  20.1 1.3 convert_multiply_fusion
  21.8 14.3 %all_gather.10 = bf16[8,8,8,256]{3,2,0,1:T(8,128)(2,1)S(1)} all-gather(bf16[1,8,8,256]{3,2,0,1:T(8,128)(2,1)S(1)} %fusion.20), channel_id=1, replica_groups=mesh['b'=8,'zp'=2,'x'=4,'c'=2,'tp'=4] {'x','c'}, dimensions={0}, use_global_device_ids=true | all-gather | bytes 294912 | tf_op jit(solution)/shard_map/spread/all_gather | solution.py:227
  36.1 3.3 %all-to-all-done = bf16[16,16,896]{2,1,0:T(8,128)(2,1)S(1)} async-done(((bf16[16,16,896]{2,1,0:T(8,128)(2,1)}), bf16[16,16,896]{2,1,0:T(8,128)(2,1)S(1)}, u32[]{:S(2)}, u32[]{:S(2)}) %all-to-all-start) | async-done | bytes 458784 | tf_op jit(solution)/shard_map/hold/all_to_all | solution.py:38
  39.4 0.8 fusion.14
  40.2 6.8 %all-to-all-start.1 = ((f32[8,8,512]{2,1,0:T(8,128)}), f32[8,8,512]{2,1,0:T(8,128)S(1)}, u32[]{:S(2)}, u32[]{:S(2)}) async-start(f32[8,8,512]{2,1,0:T(8,128)} %fusion.14), calls=%async_computation.1 | async-start | bytes 262144 | tf_op jit(solution)/shard_map/project/all_to_all | solution.py:38
  47.1 5.2 %all-to-all-done.1 = f32[8,8,512]{2,1,0:T(8,128)S(1)} async-done(((f32[8,8,512]{2,1,0:T(8,128)}), f32[8,8,512]{2,1,0:T(8,128)S(1)}, u32[]{:S(2)}, u32[]{:S(2)}) %all-to-all-start.1) | async-done | bytes 131104 | tf_op jit(solution)/shard_map/project/all_to_all | solution.py:38
  52.7 1.6 fusion.48
  55.4 0.3 multiply_reduce_fusion.3
  55.8 0.6 broadcast_in_dim.29
  56.4 4.1 %all-to-all-start.2 = ((bf16[8,8,256]{2,1,0:T(8,128)(2,1)}), bf16[8,8,256]{2,1,0:T(8,128)(2,1)S(1)}, u32[]{:S(2)}, u32[]{:S(2)}) async-start(bf16[8,8,256]{2,1,0:T(8,128)(2,1)} %broadcast_in_dim.29), calls=%async_computation.2 | async-start | bytes 65536 | tf_op jit(solution)/shard_map/heads/all_to_all | solution.py:38
  60.8 4.5 %all-to-all-done.2 = bf16[8,8,256]{2,1,0:T(8,128)(2,1)S(1)} async-done(((bf16[8,8,256]{2,1,0:T(8,128)(2,1)}), bf16[8,8,256]{2,1,0:T(8,128)(2,1)S(1)}, u32[]{:S(2)}, u32[]{:S(2)}) %all-to-all-start.2) | async-done | bytes 32800 | tf_op jit(solution)/shard_map/heads/all_to_all | solution.py:38
  65.4 0.7 broadcast_in_dim.31
  66.1 6.0 %all-to-all-start.3 = ((bf16[32,8,256]{2,1,0:T(8,128)(2,1)}), bf16[32,8,256]{2,1,0:T(8,128)(2,1)S(1)}, u32[]{:S(2)}, u32[]{:S(2)}) async-start(bf16[32,8,256]{2,1,0:T(8,128)(2,1)} %bitcast.28), calls=%async_computation.3 | async-start | bytes 262144 | tf_op jit(solution)/shard_map/attended/all_to_all | solution.py:38
  72.1 0.2 reshape.396
  72.7 6.9 %all-to-all-done.3 = bf16[32,8,256]{2,1,0:T(8,128)(2,1)S(1)} async-done(((bf16[32,8,256]{2,1,0:T(8,128)(2,1)}), bf16[32,8,256]{2,1,0:T(8,128)(2,1)S(1)}, u32[]{:S(2)}, u32[]{:S(2)}) %all-to-all-start.3) | async-done | bytes 131104 | tf_op jit(solution)/shard_map/attended/all_to_all | solution.py:38
  79.9 0.2 reshape.387
  80.3 0.3 reshape.388
  80.6 0.2 convolution_convert_fusion.1
  80.8 0.8 broadcast_in_dim.33
  81.7 10.6 %all-to-all-start.4 = ((bf16[128,2,512]{2,1,0:T(2,128)(2,1)}), bf16[128,2,512]{2,1,0:T(2,128)(2,1)S(1)}, u32[]{:S(2)}, u32[]{:S(2)}) async-start(bf16[128,2,512]{2,1,0:T(2,128)(2,1)} %bitcast.33), calls=%async_computation.4 | async-start | bytes 524288 | tf_op jit(solution)/shard_map/route/all_to_all | solution.py:38
  92.3 13.8 %all-gather = bf16[2048,128]{1,0:T(8,128)(2,1)S(1)} all-gather(bf16[256,128]{1,0:T(8,128)(2,1)S(1)} %slice.69), channel_id=2, replica_groups=mesh['b'=8,'zp'=2,'x'=4,'c'=2,'tp'=4] {'x','c'}, dimensions={0}, use_global_device_ids=true | all-gather | bytes 589824 | tf_op jit(solution)/shard_map/dense/all_gather | solution.py:266
  106.1 8.7 %all-to-all-done.4 = bf16[128,2,512]{2,1,0:T(2,128)(2,1)S(1)} async-done(((bf16[128,2,512]{2,1,0:T(2,128)(2,1)}), bf16[128,2,512]{2,1,0:T(2,128)(2,1)S(1)}, u32[]{:S(2)}, u32[]{:S(2)}) %all-to-all-start.4) | async-done | bytes 262176 | tf_op jit(solution)/shard_map/route/all_to_all | solution.py:38
  115.1 1.1 broadcast_in_dim.34
  116.2 3.5 %all-to-all-start.5 = ((bf16[4,256,512]{1,2,0:T(8,128)(2,1)}), bf16[4,256,512]{1,2,0:T(8,128)(2,1)S(1)}, u32[]{:S(2)}, u32[]{:S(2)}) async-start(bf16[4,256,512]{1,2,0:T(8,128)(2,1)} %broadcast_in_dim.34), calls=%async_computation.5 | async-start | bytes 2097152 | tf_op jit(solution)/shard_map/join/all_to_all | solution.py:38
  119.8 0.2 slice_bitcast_fusion
  120.2 0.3 convert_reduce_fusion.1
  120.7 1.2 pad_maximum_fusion
  121.9 12.7 %all-to-all-done.5 = bf16[4,256,512]{1,2,0:T(8,128)(2,1)S(1)} async-done(((bf16[4,256,512]{1,2,0:T(8,128)(2,1)}), bf16[4,256,512]{1,2,0:T(8,128)(2,1)S(1)}, u32[]{:S(2)}, u32[]{:S(2)}) %all-to-all-start.5) | async-done | bytes 1048608 | tf_op jit(solution)/shard_map/join/all_to_all | solution.py:38
  134.5 0.3 multiply_reduce_fusion
  134.9 0.3 fusion.50
  135.2 0.4 convolution_bitcast_fusion.1
  135.6 0.4 copy-done.12
  136.0 0.4 fusion.1
  136.4 0.5 convolution_convert_fusion
  136.9 16.4 %all_to_all.40 = bf16[4,256,512]{2,1,0:T(8,128)(2,1)S(1)} all-to-all(bf16[4,256,512]{2,1,0:T(8,128)(2,1)S(1)} %bitcast.174), channel_id=1, replica_groups=mesh['b'=8,'zp'=2,'x'=4,'c'=2,'tp'=4] {'tp'}, dimensions={0} | all-to-all | bytes 2097152 | tf_op jit(solution)/shard_map/reduce/all_to_all | solution.py:38
  153.4 0.2 reduce_sum.170
  153.6 0.8 reshape.395
  154.4 8.6 %all-to-all-start.7 = ((bf16[128,2,512]{2,1,0:T(2,128)(2,1)}), bf16[128,2,512]{2,1,0:T(2,128)(2,1)S(1)}, u32[]{:S(2)}, u32[]{:S(2)}) async-start(bf16[128,2,512]{2,1,0:T(2,128)(2,1)} %reshape.395), calls=%async_computation.7 | async-start | bytes 524288 | tf_op jit(solution)/shard_map/return/all_to_all | solution.py:38
  163.2 0.3 copy.99
  163.5 0.3 reshape.400
  163.8 21.8 %all-to-all-done.7 = bf16[128,2,512]{2,1,0:T(2,128)(2,1)S(1)} async-done(((bf16[128,2,512]{2,1,0:T(2,128)(2,1)}), bf16[128,2,512]{2,1,0:T(2,128)(2,1)S(1)}, u32[]{:S(2)}, u32[]{:S(2)}) %all-to-all-start.7) | async-done | bytes 262176 | tf_op jit(solution)/shard_map/return/all_to_all | solution.py:38
  185.7 0.8 fusion.5
  (98 shorter events, 4.6 us)
Async XLA Ops:
  0.0 135.2 %copy-start = (bf16[1,2048,176]{1,2,0:T(8,128)(2,1)S(1)}, bf16[1,2048,176]{1,2,0:T(8,128)(2,1)}, u32[]{:S(2)}) copy-start(bf16[1,2048,176]{1,2,0:T(8,128)(2,1)} %param.43) | copy-start | bytes 2162692
  1.7 17.0 %copy-start.3 = (f32[2048]{0:T(1024)S(1)}, f32[2048]{0:T(1024)}, u32[]{:S(2)}) copy-start(f32[2048]{0:T(1024)} %param.24) | copy-start | bytes 24580
  1.7 17.2 %copy-start.1 = (bf16[8,1,320,128]{3,2,1,0:T(8,128)(2,1)S(1)}, bf16[8,1,320,128]{3,2,1,0:T(8,128)(2,1)}, u32[]{:S(2)}) copy-start(bf16[8,1,320,128]{3,2,1,0:T(8,128)(2,1)} %param.31) | copy-start | bytes 1966084
  1.7 37.6 %all-to-all-start = ((bf16[16,16,896]{2,1,0:T(8,128)(2,1)}), bf16[16,16,896]{2,1,0:T(8,128)(2,1)S(1)}, u32[]{:S(2)}, u32[]{:S(2)}) async-start(bf16[16,16,896]{2,1,0:T(8,128)(2,1)} %message.1), calls=%async_computation | async-start | bytes 917504 | tf_op jit(solution)/shard_map/hold/all_to_all | solution.py:38
  20.1 1.5 copy-start.2
  21.3 25.7 %copy-start.8 = (s32[8]{0:T(128)S(1)}, s32[8]{0:T(128)}, u32[]{:S(2)}) copy-start(s32[8]{0:T(128)} %param.33) | copy-start | bytes 100
  21.4 31.3 %copy-start.7 = (f32[64]{0:T(128)S(1)}, f32[64]{0:T(128)}, u32[]{:S(2)}) copy-start(f32[64]{0:T(128)} %param.28) | copy-start | bytes 772
  21.4 31.3 %copy-start.9 = (f32[64]{0:T(128)S(1)}, f32[64]{0:T(128)}, u32[]{:S(2)}) copy-start(f32[64]{0:T(128)} %param.29) | copy-start | bytes 772
  21.8 33.2 %copy-start.11 = (f32[2]{0:T(128)S(1)}, f32[2]{0:T(128)}, u32[]{:S(2)}) copy-start(f32[2]{0:T(128)} %param.30) | copy-start | bytes 28
  36.0 19.3 %copy-start.13 = (bf16[8,1,320,128]{3,2,1,0:T(8,128)(2,1)S(1)}, bf16[8,1,320,128]{3,2,1,0:T(8,128)(2,1)}, u32[]{:S(2)}) copy-start(bf16[8,1,320,128]{3,2,1,0:T(8,128)(2,1)} %param.32) | copy-start | bytes 1966084
  40.2 12.1 %all-to-all-start.1 = ((f32[8,8,512]{2,1,0:T(8,128)}), f32[8,8,512]{2,1,0:T(8,128)S(1)}, u32[]{:S(2)}, u32[]{:S(2)}) async-start(f32[8,8,512]{2,1,0:T(8,128)} %fusion.14), calls=%async_computation.1 | async-start | bytes 262144 | tf_op jit(solution)/shard_map/project/all_to_all | solution.py:38
  47.0 8.7 %copy-start.10 = (f32[128]{0:T(128)S(1)}, f32[128]{0:T(128)}, u32[]{:S(2)}) copy-start(f32[128]{0:T(128)} %param.34) | copy-start | bytes 1540
  54.3 18.1 %copy-start.4 = (f32[2048]{0:T(1024)S(1)}, f32[2048]{0:T(1024)}, u32[]{:S(2)}) copy-start(f32[2048]{0:T(1024)} %param.36) | copy-start | bytes 24580
  54.3 18.3 %copy-start.6 = (f32[8,2]{0,1:T(2,128)S(1)}, f32[8,2]{0,1:T(2,128)}, u32[]{:S(2)}) copy-start(f32[8,2]{0,1:T(2,128)} %param.42) | copy-start | bytes 196
  56.4 8.8 %all-to-all-start.2 = ((bf16[8,8,256]{2,1,0:T(8,128)(2,1)}), bf16[8,8,256]{2,1,0:T(8,128)(2,1)S(1)}, u32[]{:S(2)}, u32[]{:S(2)}) async-start(bf16[8,8,256]{2,1,0:T(8,128)(2,1)} %broadcast_in_dim.29), calls=%async_computation.2 | async-start | bytes 65536 | tf_op jit(solution)/shard_map/heads/all_to_all | solution.py:38
  66.1 13.5 %all-to-all-start.3 = ((bf16[32,8,256]{2,1,0:T(8,128)(2,1)}), bf16[32,8,256]{2,1,0:T(8,128)(2,1)S(1)}, u32[]{:S(2)}, u32[]{:S(2)}) async-start(bf16[32,8,256]{2,1,0:T(8,128)(2,1)} %bitcast.28), calls=%async_computation.3 | async-start | bytes 262144 | tf_op jit(solution)/shard_map/attended/all_to_all | solution.py:38
  81.7 33.2 %all-to-all-start.4 = ((bf16[128,2,512]{2,1,0:T(2,128)(2,1)}), bf16[128,2,512]{2,1,0:T(2,128)(2,1)S(1)}, u32[]{:S(2)}, u32[]{:S(2)}) async-start(bf16[128,2,512]{2,1,0:T(2,128)(2,1)} %bitcast.33), calls=%async_computation.4 | async-start | bytes 524288 | tf_op jit(solution)/shard_map/route/all_to_all | solution.py:38
  115.1 4.6 %copy-start.5 = (f32[2048]{0:T(1024)S(1)}, f32[2048]{0:T(1024)}, u32[]{:S(2)}) copy-start(f32[2048]{0:T(1024)} %param.40) | copy-start | bytes 24580
  116.2 18.4 %all-to-all-start.5 = ((bf16[4,256,512]{1,2,0:T(8,128)(2,1)}), bf16[4,256,512]{1,2,0:T(8,128)(2,1)S(1)}, u32[]{:S(2)}, u32[]{:S(2)}) async-start(bf16[4,256,512]{1,2,0:T(8,128)(2,1)} %broadcast_in_dim.34), calls=%async_computation.5 | async-start | bytes 2097152 | tf_op jit(solution)/shard_map/join/all_to_all | solution.py:38
  134.9 1.1 copy-start.12
  154.4 31.2 %all-to-all-start.7 = ((bf16[128,2,512]{2,1,0:T(2,128)(2,1)}), bf16[128,2,512]{2,1,0:T(2,128)(2,1)S(1)}, u32[]{:S(2)}, u32[]{:S(2)}) async-start(bf16[128,2,512]{2,1,0:T(2,128)(2,1)} %reshape.395), calls=%async_computation.7 | async-start | bytes 524288 | tf_op jit(solution)/shard_map/return/all_to_all | solution.py:38

commit v7 on v6

--- a/solution.py
+++ b/solution.py
@@ -127,8 +127,9 @@
     lanes = lax.broadcasted_iota(jnp.int32, (16, 256), 1)
     narrow = lax.broadcasted_iota(jnp.int32, (16, 128), 1)
     places = lax.broadcasted_iota(jnp.int32, (16, 128), 0)
-    shared = jnp.concatenate((query[...], key[...], value[...], out[...]), axis=1)
+    shared = jnp.concatenate((query[...], key[...], value[...]), axis=1)
     wide = [part[...].astype(jnp.float32) for part in (gate, up, down)]
+    held = out[...].astype(jnp.float32)
     tags = [jnp.zeros((16, 128), jnp.float32) for _ in range(2)]
     for row in range(SEQ):
         chosen = ids[0, row]
@@ -139,13 +140,13 @@
         slot = chosen * CAP + rank
         for half in range(2):
             tags[half] = jnp.where(places + 16 * half == slot, probs[0, row], tags[half])
+    tagged = jnp.zeros((16, 128), jnp.float32)
     for half in range(2):
         used = tags[half] > 0.0
         inverse = jnp.where(used, 1.0 / jnp.where(used, tags[half], 1.0), 0.0)
         high = inverse.astype(jnp.bfloat16).astype(jnp.float32)
-        tags[half] = jnp.where(
-            narrow == 96, high, jnp.where(narrow == 97, inverse - high, 0.0)
-        )
+        tagged = jnp.where(narrow == 96 + 2 * half, high, tagged)
+        tagged = jnp.where(narrow == 97 + 2 * half, inverse - high, tagged)
     for rep in range(REP):
         turned = [
             pltpu.roll(part, (32 * (place - rep)) % 256, 1) for place, part in enumerate(wide)
@@ -153,10 +154,11 @@
         own = jnp.where(
             lanes < 32, turned[0], jnp.where(lanes < 64, turned[1], turned[2])
         )[:, :128]
-        own = jnp.where(narrow < 96, own, 0.0)
+        own = jnp.where(narrow < 96, own, tagged)
+        extra = jnp.concatenate((held, own, jnp.zeros((16, 128), jnp.float32)), axis=1)
         for half in range(2):
-            message[2 * rep + half, :, :768] = shared
-            message[2 * rep + half, :, 768:] = (own + tags[half]).astype(jnp.bfloat16)
+            message[2 * rep + half, :16, :] = shared
+            message[2 * rep + half, 16:, :] = extra[8 * half : 8 * half + 8].astype(jnp.bfloat16)
 
 
 def build_message(ids, probs, *parts):
@@ -165,7 +167,7 @@
     return pl.pallas_call(
         message_body,
         in_specs=[scalars, scalars] + [whole] * len(parts),
-        out_shape=jax.ShapeDtypeStruct((N_Z, 16, 896), jnp.bfloat16),
+        out_shape=jax.ShapeDtypeStruct((N_Z, 24, 512), jnp.bfloat16),
         name="message",
     )(ids, probs, *parts)
 
@@ -218,7 +220,10 @@
         dense_down_weight.T,
     )
     with jax.named_scope("hold"):
-        held = exchange(message, Z).reshape(N_Z * 16, 896)
+        held = exchange(message, Z)
+    with jax.named_scope("halves"):
+        extra = lax.all_gather(held[:, 16:, :384], "zp", axis=1).reshape(N_Z * 16, 384)
+    held = held[:, :16].reshape(N_Z * 16, 512)
 
     residual = to_mixed(tokens).astype(jnp.float32)
     normed = mixed_scale(residual, to_mixed(norm_gain[None])).astype(jnp.bfloat16)
@@ -227,7 +232,7 @@
         spread = lax.all_gather(normed, XC, axis=0)
         spread = lax.dynamic_index_in_dim(spread, xc_index, 1, False).reshape(N_XC * SEQ, block)
 
-    partial_rows = jnp.dot(spread, held[:, :512], preferred_element_type=jnp.float32)
+    partial_rows = jnp.dot(spread, held, preferred_element_type=jnp.float32)
     with jax.named_scope("project"):
         packed = jnp.sum(exchange(partial_rows.reshape(N_XC, SEQ, 512), XC), axis=0)
     head_out = attend(
@@ -236,7 +241,7 @@
     with jax.named_scope("heads"):
         all_heads = gather_small(head_out, XC, N_XC).reshape(N_XC * SEQ, 256)
     attended_part = lax.dot_general(
-        all_heads, held[:, 512:768], (((1,), (1,)), ((), ())), preferred_element_type=jnp.float32
+        all_heads, extra[:, :256], (((1,), (1,)), ((), ())), preferred_element_type=jnp.float32
     ).astype(jnp.bfloat16)
     with jax.named_scope("attended"):
         parts = exchange(
@@ -263,9 +268,10 @@
         incoming = exchange(outgoing, EP).reshape(N_EP * CAP, share_width)
 
     with jax.named_scope("dense"):
-        dense_held = lax.all_gather(held[:, 768:], XC, axis=0).reshape(N_XC, N_Z, 16, 128)
+        dense_held = lax.all_gather(extra[:, 256:], XC, axis=0).reshape(N_XC, N_Z, 16, 128)
     incoming, dense_held = lax.optimization_barrier((incoming, dense_held))
-    tag = lax.dynamic_slice_in_dim(dense_held, 2 * xc_index, CAP, 2)[..., 96:98]
+    tag = lax.dynamic_slice_in_dim(dense_held, 2 * xc_index, CAP, 2)[..., 96:100]
+    tag = jnp.where(lax.axis_index("zp") == 0, tag[..., :2], tag[..., 2:])
     tag = jnp.sum(tag.transpose(1, 0, 2, 3).reshape(N_EP * CAP, 2).astype(jnp.float32), axis=1)
     dense_held = dense_held.transpose(1, 0, 2, 3).reshape(width, 128)
     down = jnp.concatenate((expert_down[0], dense_held[:, 64:96].T), axis=0)

time: 187 us -> 187 us (level)
  waiting for transfers between devices: 63.1 us -> 56.5 us
  blocking collectives: 44.5 us -> 50 us
    all_to_all x7, waiting for transfers between devices: 63.1 us -> 56.5 us  [exchange(): return lax.all_to_all(values, axes, split_axis=0, concat_axis=0, tiled=True)]
    all_gather x1 -> x2, blocking collectives: 13.8 us -> 19.3 us  [the longest x1 13.8 us: shards(): lax.all_gather(extra[:, 256:], XC, axis=0).reshape(N_XC, N_Z, 16, 128)]
  transfers between devices with their start and end apart: 7 -> 7, of which waited for: 7 -> 6; matrix products, arithmetic and copies ran while one was open for 5% -> 5% of each run, Pallas kernels for 0% -> 0%
where the time goes in v7:
time: 187 us
  waiting for transfers between devices  56.5 us (30%)
  starting transfers between devices  55.5 us (30%)
  blocking collectives  50 us (27%)
  local copies, waits for them, and re-layouts  11.7 us (6%)
  matrix products  5.57 us (3%)
  other arithmetic  5.01 us (3%)
    all_to_all x7, waiting for transfers between devices, exchange(): return lax.all_to_all(values, axes, split_axis=0, concat_axis=0, tiled=True)  56.5 us
    all_to_all x7, starting transfers between devices, exchange(): return lax.all_to_all(values, axes, split_axis=0, concat_axis=0, tiled=True)  55.5 us
    all_to_all x1, blocking collectives, exchange(): return lax.all_to_all(values, axes, split_axis=0, concat_axis=0, tiled=True)  16.4 us
    all_gather x1, blocking collectives, shards(): spread = lax.all_gather(normed, XC, axis=0)  14.3 us
    all_gather x1, blocking collectives, shards(): lax.all_gather(extra[:, 256:], XC, axis=0).reshape(N_XC, N_Z, 16, 128)  13.8 us
    all_gather x1, blocking collectives, shards(): lax.all_gather(held[:, 16:, :384], 'zp', axis=1).reshape(N_Z * 16, 384)  5.5 us
  transfers between devices with their start and end apart: 7, of which 6 were waited for; matrix products, arithmetic and copies ran while one was open for 5% of the time, Pallas kernels for 0%

profile of v7, /device:TPU:33, one launch (start us, length us, event | category | flops | bytes accessed | tf_op | source)
XLA Modules:
  0.0 186.6 jit_solution(5946440366374416104)
XLA Ops:
  0.0 1.7 message.1
  1.7 14.8 %all-to-all-start = ((bf16[16,24,512]{2,1,0:T(8,128)(2,1)}), bf16[16,24,512]{2,1,0:T(8,128)(2,1)S(1)}, u32[]{:S(2)}, u32[]{:S(2)}) async-start(bf16[16,24,512]{2,1,0:T(8,128)(2,1)} %message.1), calls=%async_computation | async-start | bytes 786432 | tf_op jit(solution)/shard_map/hold/all_to_all | solution.py:38
  16.5 0.8 copy.99
  17.6 1.0 reshape.406
  18.7 0.2 reshape.401
  19.1 1.2 copy.89
  20.3 1.3 convert_multiply_fusion
  22.0 14.3 %all_gather.16 = bf16[8,8,8,256]{3,2,0,1:T(8,128)(2,1)S(1)} all-gather(bf16[1,8,8,256]{3,2,0,1:T(8,128)(2,1)S(1)} %fusion.19), channel_id=1, replica_groups=mesh['b'=8,'zp'=2,'x'=4,'c'=2,'tp'=4] {'x','c'}, dimensions={0}, use_global_device_ids=true | all-gather | bytes 294912 | tf_op jit(solution)/shard_map/spread/all_gather | solution.py:232
  36.3 1.3 all-to-all-done
  37.6 0.8 fusion.23
  38.4 6.3 %all-to-all-start.1 = ((f32[8,8,512]{2,1,0:T(8,128)}), f32[8,8,512]{2,1,0:T(8,128)S(1)}, u32[]{:S(2)}, u32[]{:S(2)}) async-start(f32[8,8,512]{2,1,0:T(8,128)} %fusion.23), calls=%async_computation.1 | async-start | bytes 262144 | tf_op jit(solution)/shard_map/project/all_to_all | solution.py:38
  44.8 5.1 %all-to-all-done.1 = f32[8,8,512]{2,1,0:T(8,128)S(1)} async-done(((f32[8,8,512]{2,1,0:T(8,128)}), f32[8,8,512]{2,1,0:T(8,128)S(1)}, u32[]{:S(2)}, u32[]{:S(2)}) %all-to-all-start.1) | async-done | bytes 131104 | tf_op jit(solution)/shard_map/project/all_to_all | solution.py:38
  50.4 0.4 fusion.48
  51.9 1.4 multiply_reduce_fusion.3
  53.5 0.6 broadcast_in_dim.29
  54.1 4.1 %all-to-all-start.2 = ((bf16[8,8,256]{2,1,0:T(8,128)(2,1)}), bf16[8,8,256]{2,1,0:T(8,128)(2,1)S(1)}, u32[]{:S(2)}, u32[]{:S(2)}) async-start(bf16[8,8,256]{2,1,0:T(8,128)(2,1)} %broadcast_in_dim.29), calls=%async_computation.2 | async-start | bytes 65536 | tf_op jit(solution)/shard_map/heads/all_to_all | solution.py:38
  58.2 5.5 %all-gather = bf16[16,16,384]{2,1,0:T(8,128)(2,1)S(1)} all-gather(bf16[16,8,384]{2,1,0:T(8,128)(2,1)S(1)} %slice.79), channel_id=2, replica_groups=mesh['b'=8,'zp'=2,'x'=4,'c'=2,'tp'=4] {'zp'}, dimensions={1}, use_global_device_ids=true | all-gather | bytes 294912 | tf_op jit(solution)/shard_map/halves/all_gather | solution.py:225
  63.9 0.7 broadcast_in_dim.31
  64.5 7.9 %all-to-all-start.3 = ((bf16[32,8,256]{2,1,0:T(8,128)(2,1)}), bf16[32,8,256]{2,1,0:T(8,128)(2,1)S(1)}, u32[]{:S(2)}, u32[]{:S(2)}) async-start(bf16[32,8,256]{2,1,0:T(8,128)(2,1)} %bitcast.29), calls=%async_computation.3 | async-start | bytes 262144 | tf_op jit(solution)/shard_map/attended/all_to_all | solution.py:38
  72.5 0.2 reshape.400
  73.1 6.9 %all-to-all-done.3 = bf16[32,8,256]{2,1,0:T(8,128)(2,1)S(1)} async-done(((bf16[32,8,256]{2,1,0:T(8,128)(2,1)}), bf16[32,8,256]{2,1,0:T(8,128)(2,1)S(1)}, u32[]{:S(2)}, u32[]{:S(2)}) %all-to-all-start.3) | async-done | bytes 131104 | tf_op jit(solution)/shard_map/attended/all_to_all | solution.py:38
  80.3 0.2 reshape.391
  80.7 0.3 reshape.392
  81.0 0.2 convolution_convert_fusion.1
  81.2 0.8 broadcast_in_dim.33
  82.1 10.1 %all-to-all-start.4 = ((bf16[128,2,512]{2,1,0:T(2,128)(2,1)}), bf16[128,2,512]{2,1,0:T(2,128)(2,1)S(1)}, u32[]{:S(2)}, u32[]{:S(2)}) async-start(bf16[128,2,512]{2,1,0:T(2,128)(2,1)} %bitcast.34), calls=%async_computation.4 | async-start | bytes 524288 | tf_op jit(solution)/shard_map/route/all_to_all | solution.py:38
  92.2 13.8 %all-gather.1 = bf16[2048,128]{1,0:T(8,128)(2,1)S(1)} all-gather(bf16[256,128]{1,0:T(8,128)(2,1)S(1)} %slice.81), channel_id=3, replica_groups=mesh['b'=8,'zp'=2,'x'=4,'c'=2,'tp'=4] {'x','c'}, dimensions={0}, use_global_device_ids=true | all-gather | bytes 589824 | tf_op jit(solution)/shard_map/dense/all_gather | solution.py:271
  106.0 8.7 %all-to-all-done.4 = bf16[128,2,512]{2,1,0:T(2,128)(2,1)S(1)} async-done(((bf16[128,2,512]{2,1,0:T(2,128)(2,1)}), bf16[128,2,512]{2,1,0:T(2,128)(2,1)S(1)}, u32[]{:S(2)}, u32[]{:S(2)}) %all-to-all-start.4) | async-done | bytes 262176 | tf_op jit(solution)/shard_map/route/all_to_all | solution.py:38
  115.0 1.1 broadcast_in_dim.34
  116.1 3.5 %all-to-all-start.5 = ((bf16[4,256,512]{1,2,0:T(8,128)(2,1)}), bf16[4,256,512]{1,2,0:T(8,128)(2,1)S(1)}, u32[]{:S(2)}, u32[]{:S(2)}) async-start(bf16[4,256,512]{1,2,0:T(8,128)(2,1)} %broadcast_in_dim.34), calls=%async_computation.5 | async-start | bytes 2097152 | tf_op jit(solution)/shard_map/join/all_to_all | solution.py:38
  119.7 0.2 slice_bitcast_fusion
  120.1 0.4 convert_reduce_fusion.1
  120.7 1.2 pad_maximum_fusion
  121.8 12.6 %all-to-all-done.5 = bf16[4,256,512]{1,2,0:T(8,128)(2,1)S(1)} async-done(((bf16[4,256,512]{1,2,0:T(8,128)(2,1)}), bf16[4,256,512]{1,2,0:T(8,128)(2,1)S(1)}, u32[]{:S(2)}, u32[]{:S(2)}) %all-to-all-start.5) | async-done | bytes 1048608 | tf_op jit(solution)/shard_map/join/all_to_all | solution.py:38
  134.4 0.3 multiply_reduce_fusion
  134.8 0.3 fusion.50
  135.1 0.4 convolution_bitcast_fusion.1
  135.5 0.4 copy-done.13
  135.9 0.4 fusion.1
  136.3 0.5 convolution_convert_fusion
  136.8 16.4 %all_to_all.40 = bf16[4,256,512]{2,1,0:T(8,128)(2,1)S(1)} all-to-all(bf16[4,256,512]{2,1,0:T(8,128)(2,1)S(1)} %bitcast.174), channel_id=1, replica_groups=mesh['b'=8,'zp'=2,'x'=4,'c'=2,'tp'=4] {'tp'}, dimensions={0} | all-to-all | bytes 2097152 | tf_op jit(solution)/shard_map/reduce/all_to_all | solution.py:38
  153.3 0.2 reduce_sum.170
  153.5 0.8 reshape.399
  154.3 8.8 %all-to-all-start.7 = ((bf16[128,2,512]{2,1,0:T(2,128)(2,1)}), bf16[128,2,512]{2,1,0:T(2,128)(2,1)S(1)}, u32[]{:S(2)}, u32[]{:S(2)}) async-start(bf16[128,2,512]{2,1,0:T(2,128)(2,1)} %reshape.399), calls=%async_computation.7 | async-start | bytes 524288 | tf_op jit(solution)/shard_map/return/all_to_all | solution.py:38
  163.3 0.3 copy.98
  163.6 0.3 reshape.404
  163.9 21.8 %all-to-all-done.7 = bf16[128,2,512]{2,1,0:T(2,128)(2,1)S(1)} async-done(((bf16[128,2,512]{2,1,0:T(2,128)(2,1)}), bf16[128,2,512]{2,1,0:T(2,128)(2,1)S(1)}, u32[]{:S(2)}, u32[]{:S(2)}) %all-to-all-start.7) | async-done | bytes 262176 | tf_op jit(solution)/shard_map/return/all_to_all | solution.py:38
  185.8 0.8 fusion.5
  (101 shorter events, 4.7 us)
Async XLA Ops:
  0.0 135.1 %copy-start = (bf16[1,2048,176]{1,2,0:T(8,128)(2,1)S(1)}, bf16[1,2048,176]{1,2,0:T(8,128)(2,1)}, u32[]{:S(2)}) copy-start(bf16[1,2048,176]{1,2,0:T(8,128)(2,1)} %param.43) | copy-start | bytes 2162692
  1.7 17.2 %copy-start.4 = (f32[2048]{0:T(1024)S(1)}, f32[2048]{0:T(1024)}, u32[]{:S(2)}) copy-start(f32[2048]{0:T(1024)} %param.24) | copy-start | bytes 24580
  1.7 17.4 %copy-start.2 = (bf16[8,1,320,128]{3,2,1,0:T(8,128)(2,1)S(1)}, bf16[8,1,320,128]{3,2,1,0:T(8,128)(2,1)}, u32[]{:S(2)}) copy-start(bf16[8,1,320,128]{3,2,1,0:T(8,128)(2,1)} %param.31) | copy-start | bytes 1966084
  1.7 35.8 %all-to-all-start = ((bf16[16,24,512]{2,1,0:T(8,128)(2,1)}), bf16[16,24,512]{2,1,0:T(8,128)(2,1)S(1)}, u32[]{:S(2)}, u32[]{:S(2)}) async-start(bf16[16,24,512]{2,1,0:T(8,128)(2,1)} %message.1), calls=%async_computation | async-start | bytes 786432 | tf_op jit(solution)/shard_map/hold/all_to_all | solution.py:38
  20.3 1.5 copy-start.3
  21.6 23.2 %copy-start.9 = (s32[8]{0:T(128)S(1)}, s32[8]{0:T(128)}, u32[]{:S(2)}) copy-start(s32[8]{0:T(128)} %param.33) | copy-start | bytes 100
  21.6 28.7 %copy-start.8 = (f32[64]{0:T(128)S(1)}, f32[64]{0:T(128)}, u32[]{:S(2)}) copy-start(f32[64]{0:T(128)} %param.28) | copy-start | bytes 772
  21.6 28.8 %copy-start.10 = (f32[64]{0:T(128)S(1)}, f32[64]{0:T(128)}, u32[]{:S(2)}) copy-start(f32[64]{0:T(128)} %param.29) | copy-start | bytes 772
  21.8 28.7 %copy-start.1 = (bf16[8,1,320,128]{2,3,0,1:T(8,128)(2,1)S(1)}, bf16[8,1,320,128]{2,3,0,1:T(8,128)(2,1)}, u32[]{:S(2)}) copy-start(bf16[8,1,320,128]{2,3,0,1:T(8,128)(2,1)} %copy.89) | copy-start | bytes 1966084
  37.5 14.0 %copy-start.12 = (f32[2]{0:T(128)S(1)}, f32[2]{0:T(128)}, u32[]{:S(2)}) copy-start(f32[2]{0:T(128)} %param.30) | copy-start | bytes 28
  38.4 11.6 %all-to-all-start.1 = ((f32[8,8,512]{2,1,0:T(8,128)}), f32[8,8,512]{2,1,0:T(8,128)S(1)}, u32[]{:S(2)}, u32[]{:S(2)}) async-start(f32[8,8,512]{2,1,0:T(8,128)} %fusion.23), calls=%async_computation.1 | async-start | bytes 262144 | tf_op jit(solution)/shard_map/project/all_to_all | solution.py:38
  44.8 8.6 %copy-start.11 = (f32[128]{0:T(128)S(1)}, f32[128]{0:T(128)}, u32[]{:S(2)}) copy-start(f32[128]{0:T(128)} %param.34) | copy-start | bytes 1540
  50.9 22.0 %copy-start.5 = (f32[2048]{0:T(1024)S(1)}, f32[2048]{0:T(1024)}, u32[]{:S(2)}) copy-start(f32[2048]{0:T(1024)} %param.36) | copy-start | bytes 24580
  50.9 22.2 %copy-start.7 = (f32[8,2]{0,1:T(2,128)S(1)}, f32[8,2]{0,1:T(2,128)}, u32[]{:S(2)}) copy-start(f32[8,2]{0,1:T(2,128)} %param.42) | copy-start | bytes 196
  54.1 9.6 %all-to-all-start.2 = ((bf16[8,8,256]{2,1,0:T(8,128)(2,1)}), bf16[8,8,256]{2,1,0:T(8,128)(2,1)S(1)}, u32[]{:S(2)}, u32[]{:S(2)}) async-start(bf16[8,8,256]{2,1,0:T(8,128)(2,1)} %broadcast_in_dim.29), calls=%async_computation.2 | async-start | bytes 65536 | tf_op jit(solution)/shard_map/heads/all_to_all | solution.py:38
  64.5 15.5 %all-to-all-start.3 = ((bf16[32,8,256]{2,1,0:T(8,128)(2,1)}), bf16[32,8,256]{2,1,0:T(8,128)(2,1)S(1)}, u32[]{:S(2)}, u32[]{:S(2)}) async-start(bf16[32,8,256]{2,1,0:T(8,128)(2,1)} %bitcast.29), calls=%async_computation.3 | async-start | bytes 262144 | tf_op jit(solution)/shard_map/attended/all_to_all | solution.py:38
  82.1 32.7 %all-to-all-start.4 = ((bf16[128,2,512]{2,1,0:T(2,128)(2,1)}), bf16[128,2,512]{2,1,0:T(2,128)(2,1)S(1)}, u32[]{:S(2)}, u32[]{:S(2)}) async-start(bf16[128,2,512]{2,1,0:T(2,128)(2,1)} %bitcast.34), calls=%async_computation.4 | async-start | bytes 524288 | tf_op jit(solution)/shard_map/route/all_to_all | solution.py:38
  115.0 4.6 %copy-start.6 = (f32[2048]{0:T(1024)S(1)}, f32[2048]{0:T(1024)}, u32[]{:S(2)}) copy-start(f32[2048]{0:T(1024)} %param.40) | copy-start | bytes 24580
  116.1 18.4 %all-to-all-start.5 = ((bf16[4,256,512]{1,2,0:T(8,128)(2,1)}), bf16[4,256,512]{1,2,0:T(8,128)(2,1)S(1)}, u32[]{:S(2)}, u32[]{:S(2)}) async-start(bf16[4,256,512]{1,2,0:T(8,128)(2,1)} %broadcast_in_dim.34), calls=%async_computation.5 | async-start | bytes 2097152 | tf_op jit(solution)/shard_map/join/all_to_all | solution.py:38
  134.8 1.1 copy-start.13
  154.3 31.4 %all-to-all-start.7 = ((bf16[128,2,512]{2,1,0:T(2,128)(2,1)}), bf16[128,2,512]{2,1,0:T(2,128)(2,1)S(1)}, u32[]{:S(2)}, u32[]{:S(2)}) async-start(bf16[128,2,512]{2,1,0:T(2,128)(2,1)} %reshape.399), calls=%async_computation.7 | async-start | bytes 524288 | tf_op jit(solution)/shard_map/return/all_to_all | solution.py:38

commit v8 on v7

--- a/solution.py
+++ b/solution.py
@@ -204,7 +204,7 @@
     width = tokens.shape[1]
     share_width = width // N_TP
     tp_index = lax.axis_index("tp")
-    tp_start = tp_index * share_width
+    tp_start = (tp_index * share_width).astype(jnp.uint32)
     block = width // N_XC
 
     select, combine_weights = route_tables(expert_ids, expert_probs)
@@ -223,8 +223,6 @@
         held = exchange(message, Z)
     with jax.named_scope("halves"):
         extra = lax.all_gather(held[:, 16:, :384], "zp", axis=1).reshape(N_Z * 16, 384)
-    held = held[:, :16].reshape(N_Z * 16, 512)
-
     residual = to_mixed(tokens).astype(jnp.float32)
     normed = mixed_scale(residual, to_mixed(norm_gain[None])).astype(jnp.bfloat16)
     xc_index = lax.axis_index(XC)
@@ -232,12 +230,24 @@
         spread = lax.all_gather(normed, XC, axis=0)
         spread = lax.dynamic_index_in_dim(spread, xc_index, 1, False).reshape(N_XC * SEQ, block)
 
+    held, select, combine_weights, ffn_scaling, residual = lax.optimization_barrier(
+        (
+            held[:, :16].reshape(N_Z * 16, 512),
+            select.astype(jnp.bfloat16).T,
+            combine_weights,
+            to_mixed(ffn_gain[None]),
+            residual,
+        )
+    )
     partial_rows = jnp.dot(spread, held, preferred_element_type=jnp.float32)
     with jax.named_scope("project"):
-        packed = jnp.sum(exchange(partial_rows.reshape(N_XC, SEQ, 512), XC), axis=0)
+        packed = exchange(partial_rows.reshape(N_XC, SEQ, 512), XC)
+        packed, extra = lax.optimization_barrier((packed, extra))
+        packed = jnp.sum(packed, axis=0)
     head_out = attend(
         packed, key_cache, value_cache, lengths, query_gain, key_gain, lambdas, head_gain
     )
+    head_out, tp_start = lax.optimization_barrier((head_out, tp_start))
     with jax.named_scope("heads"):
         all_heads = gather_small(head_out, XC, N_XC).reshape(N_XC * SEQ, 256)
     attended_part = lax.dot_general(
@@ -253,13 +263,13 @@
     attended = jnp.sum(parts.astype(jnp.float32), axis=1)
     middle_mixed = lax.optimization_barrier((residual + attended).astype(jnp.bfloat16))
     ffn_input = from_mixed(
-        mixed_scale(middle_mixed.astype(jnp.float32), to_mixed(ffn_gain[None])).astype(jnp.bfloat16)
-    )
-    middle = from_mixed(middle_mixed).astype(jnp.float32)
+        mixed_scale(middle_mixed.astype(jnp.float32), ffn_scaling).astype(jnp.bfloat16)
+    )
+    middle = own_columns(from_mixed(middle_mixed).astype(jnp.float32), tp_start, share_width)
 
     ffn_share = own_columns(ffn_input, tp_start, share_width)
     chosen = jnp.dot(
-        select.astype(jnp.bfloat16).T, ffn_share, preferred_element_type=jnp.float32
+        select, ffn_share, preferred_element_type=jnp.float32
     ).astype(jnp.bfloat16)
     outgoing = jnp.broadcast_to(
         chosen.reshape(1, EXPERTS, CAP, share_width), (REP, EXPERTS, CAP, share_width)
@@ -279,7 +289,9 @@
 
     with jax.named_scope("join"):
         rows = gather_small(incoming, "tp", N_TP)
-    rows, dense_held, down, tag = lax.optimization_barrier((rows, dense_held, down, tag))
+    rows, dense_held, down, tag, middle, combine_weights = lax.optimization_barrier(
+        (rows, dense_held, down, tag, middle, combine_weights)
+    )
     rows = rows.transpose(1, 0, 2).reshape(N_EP * CAP, width)
     branch_weight = jax.nn.sigmoid(jnp.sum(rows.astype(jnp.float32) * branch_gate, axis=1))
     dense_scale = branch_weight * tag
@@ -308,7 +320,7 @@
         returned.reshape(REP, EXPERTS * CAP, share_width).astype(jnp.float32), axis=0
     )
     routed = jnp.dot(combine_weights, expert_out, precision=lax.Precision.HIGHEST)
-    return (own_columns(middle, tp_start, share_width) + routed).astype(jnp.bfloat16)
+    return (middle + routed).astype(jnp.bfloat16)
 
 
 def solution(mesh):

time: 187 us -> 188 us (level)
  blocking collectives: 50 us -> 105 us
  waiting for transfers between devices: 56.5 us -> 20.6 us
  starting transfers between devices: 55.5 us -> 36.3 us
  other arithmetic: 5.01 us -> 7.55 us
    all_to_all x1 -> x4, blocking collectives: 16.4 us -> 71.4 us  [exchange(): return lax.all_to_all(values, axes, split_axis=0, concat_axis=0, tiled=True)]
    all_to_all x7 -> x4, waiting for transfers between devices: 56.5 us -> 20.6 us  [exchange(): return lax.all_to_all(values, axes, split_axis=0, concat_axis=0, tiled=True)]
    all_to_all x7 -> x4, starting transfers between devices: 55.5 us -> 36.3 us  [exchange(): return lax.all_to_all(values, axes, split_axis=0, concat_axis=0, tiled=True)]
  transfers between devices with their start and end apart: 7 -> 4, of which waited for: 6 -> 3; matrix products, arithmetic and copies ran while one was open for 5% -> 7% of each run, Pallas kernels for 0% -> 0%
where the time goes in v8:
time: 188 us; the launch traced here: 187 us
  blocking collectives  105 us (56%)
  starting transfers between devices  36.3 us (19%)
  waiting for transfers between devices  20.6 us (11%)
  local copies, waits for them, and re-layouts  11.3 us (6%)
  other arithmetic  7.55 us (4%)
  matrix products  4.45 us (2%)
    all_to_all x4, blocking collectives, exchange(): return lax.all_to_all(values, axes, split_axis=0, concat_axis=0, tiled=True)  71.4 us
    all_to_all x4, starting transfers between devices, exchange(): return lax.all_to_all(values, axes, split_axis=0, concat_axis=0, tiled=True)  36.3 us
    all_to_all x4, waiting for transfers between devices, exchange(): return lax.all_to_all(values, axes, split_axis=0, concat_axis=0, tiled=True)  20.6 us
    all_gather x1, blocking collectives, shards(): spread = lax.all_gather(normed, XC, axis=0)  14.2 us
    all_gather x1, blocking collectives, shards(): lax.all_gather(extra[:, 256:], XC, axis=0).reshape(N_XC, N_Z, 16, 128)  13.9 us
    all_gather x1, blocking collectives, shards(): lax.all_gather(held[:, 16:, :384], 'zp', axis=1).reshape(N_Z * 16, 384)  5 us
  transfers between devices with their start and end apart: 4, of which 3 were waited for; matrix products, arithmetic and copies ran while one was open for 7% of the time, Pallas kernels for 0%

profile of v8, /device:TPU:33, one launch (start us, length us, event | category | flops | bytes accessed | tf_op | source)
XLA Modules:
  0.0 186.9 jit_solution(15007509919670003083)
XLA Ops:
  0.0 1.7 message.1
  1.7 14.7 %all-to-all-start = ((bf16[16,24,512]{2,1,0:T(8,128)(2,1)}), bf16[16,24,512]{2,1,0:T(8,128)(2,1)S(1)}, u32[]{:S(2)}, u32[]{:S(2)}) async-start(bf16[16,24,512]{2,1,0:T(8,128)(2,1)} %message.1), calls=%async_computation | async-start | bytes 786432 | tf_op jit(solution)/shard_map/hold/all_to_all | solution.py:38
  16.4 0.8 copy.88
  17.1 1.0 reshape.412
  18.2 0.2 reshape.406
  18.5 0.9 reshape.407
  19.7 0.7 copy.90
  20.7 1.4 copy.93
  22.3 0.8 reduce_sum.156
  23.0 0.9 multiply_reduce_fusion.2
  24.0 0.9 fusion.21
  24.9 14.2 %all_gather.16 = bf16[8,8,8,256]{3,2,0,1:T(8,128)(2,1)S(1)} all-gather(bf16[1,8,8,256]{3,2,0,1:T(8,128)(2,1)S(1)} %fusion.21), channel_id=1, replica_groups=mesh['b'=8,'zp'=2,'x'=4,'c'=2,'tp'=4] {'x','c'}, dimensions={0}, use_global_device_ids=true | all-gather | bytes 294912 | tf_op jit(solution)/shard_map/spread/all_gather | solution.py:230
  39.1 0.8 select_reduce_fusion
  39.9 0.8 add_rsqrt_fusion
  40.7 0.8 fusion.14
  41.5 4.0 %all-to-all-start.1 = ((f32[8,8,512]{2,1,0:T(8,128)}), f32[8,8,512]{2,1,0:T(8,128)S(1)}, u32[]{:S(2)}, u32[]{:S(2)}) async-start(f32[8,8,512]{2,1,0:T(8,128)} %fusion.14), calls=%async_computation.1 | async-start | bytes 262144 | tf_op jit(solution)/shard_map/project/all_to_all | solution.py:38
  45.6 5.0 %all-gather = bf16[16,16,384]{2,1,0:T(8,128)(2,1)S(1)} all-gather(bf16[16,8,384]{2,1,0:T(8,128)(2,1)S(1)} %slice.72), channel_id=2, replica_groups=mesh['b'=8,'zp'=2,'x'=4,'c'=2,'tp'=4] {'zp'}, dimensions={1}, use_global_device_ids=true | all-gather | bytes 294912 | tf_op jit(solution)/shard_map/halves/all_gather | solution.py:225
  51.2 0.4 fusion.48
  52.7 0.3 multiply_reduce_fusion.3
  53.2 9.7 %all_to_all.40 = bf16[8,8,256]{2,1,0:T(8,128)(2,1)S(1)} all-to-all(bf16[8,8,256]{2,1,0:T(8,128)(2,1)S(1)} %broadcast_in_dim.26), channel_id=1, replica_groups=mesh['b'=8,'zp'=2,'x'=4,'c'=2,'tp'=4] {'x','c'}, dimensions={0} | all-to-all | bytes 65536 | tf_op jit(solution)/shard_map/heads/all_to_all | solution.py:38
  63.1 13.3 %all_to_all.41 = bf16[32,8,256]{2,1,0:T(8,128)(2,1)S(1)} all-to-all(bf16[32,8,256]{2,1,0:T(8,128)(2,1)S(1)} %bitcast.188), channel_id=1, replica_groups=mesh['b'=8,'zp'=2,'x'=4,'c'=2,'tp'=4] {'x','c','tp'}, dimensions={0} | all-to-all | bytes 262144 | tf_op jit(solution)/shard_map/attended/all_to_all | solution.py:38
  76.7 0.2 reshape.397
  76.9 0.2 copy.130
  77.1 0.3 reshape.398
  77.4 0.2 convolution_convert_fusion.1
  77.6 0.8 broadcast_in_dim.30
  78.4 14.2 %all-to-all-start.4 = ((bf16[128,2,512]{2,1,0:T(2,128)(2,1)}), bf16[128,2,512]{2,1,0:T(2,128)(2,1)S(1)}, u32[]{:S(2)}, u32[]{:S(2)}) async-start(bf16[128,2,512]{2,1,0:T(2,128)(2,1)} %bitcast.35), calls=%async_computation.4 | async-start | bytes 524288 | tf_op jit(solution)/shard_map/route/all_to_all | solution.py:38
  92.7 13.9 %all-gather.1 = bf16[2048,128]{1,0:T(8,128)(2,1)S(1)} all-gather(bf16[256,128]{1,0:T(8,128)(2,1)S(1)} %slice.64), channel_id=3, replica_groups=mesh['b'=8,'zp'=2,'x'=4,'c'=2,'tp'=4] {'x','c'}, dimensions={0}, use_global_device_ids=true | all-gather | bytes 589824 | tf_op jit(solution)/shard_map/dense/all_gather | solution.py:281
  106.7 0.3 copy.107
  107.0 0.3 reshape.410
  107.3 7.9 %all-to-all-done.4 = bf16[128,2,512]{2,1,0:T(2,128)(2,1)S(1)} async-done(((bf16[128,2,512]{2,1,0:T(2,128)(2,1)}), bf16[128,2,512]{2,1,0:T(2,128)(2,1)S(1)}, u32[]{:S(2)}, u32[]{:S(2)}) %all-to-all-start.4) | async-done | bytes 262176 | tf_op jit(solution)/shard_map/route/all_to_all | solution.py:38
  115.4 1.1 broadcast_in_dim.31
  116.5 3.5 %all-to-all-start.5 = ((bf16[4,256,512]{1,2,0:T(8,128)(2,1)}), bf16[4,256,512]{1,2,0:T(8,128)(2,1)S(1)}, u32[]{:S(2)}, u32[]{:S(2)}) async-start(bf16[4,256,512]{1,2,0:T(8,128)(2,1)} %broadcast_in_dim.31), calls=%async_computation.5 | async-start | bytes 2097152 | tf_op jit(solution)/shard_map/join/all_to_all | solution.py:38
  120.2 0.2 slice_bitcast_fusion
  120.4 0.2 copy.105
  120.5 0.4 convert_reduce_fusion.1
  121.2 1.2 pad_maximum_fusion
  122.3 12.5 %all-to-all-done.5 = bf16[4,256,512]{1,2,0:T(8,128)(2,1)S(1)} async-done(((bf16[4,256,512]{1,2,0:T(8,128)(2,1)}), bf16[4,256,512]{1,2,0:T(8,128)(2,1)S(1)}, u32[]{:S(2)}, u32[]{:S(2)}) %all-to-all-start.5) | async-done | bytes 1048608 | tf_op jit(solution)/shard_map/join/all_to_all | solution.py:38
  134.9 0.3 multiply_reduce_fusion
  135.2 0.3 fusion.50
  135.5 0.4 convolution_bitcast_fusion.1
  136.0 0.4 copy-done.9
  136.3 0.4 fusion.1
  136.7 0.5 convolution_convert_fusion
  137.3 16.6 %all_to_all.42 = bf16[4,256,512]{2,1,0:T(8,128)(2,1)S(1)} all-to-all(bf16[4,256,512]{2,1,0:T(8,128)(2,1)S(1)} %bitcast.178), channel_id=1, replica_groups=mesh['b'=8,'zp'=2,'x'=4,'c'=2,'tp'=4] {'tp'}, dimensions={0} | all-to-all | bytes 2097152 | tf_op jit(solution)/shard_map/reduce/all_to_all | solution.py:38
  153.9 0.2 reduce_sum.170
  154.2 31.8 %all_to_all.43 = bf16[128,2,512]{2,1,0:T(2,128)(2,1)S(1)} all-to-all(bf16[128,2,512]{2,1,0:T(2,128)(2,1)S(1)} %reshape.405), channel_id=1, replica_groups=mesh['b'=8,'zp'=2,'x'=4,'c'=2,'tp'=4] {'b','zp','x','c'}, dimensions={0} | all-to-all | bytes 524288 | tf_op jit(solution)/shard_map/return/all_to_all | solution.py:38
  186.1 0.8 fusion.5
  (93 shorter events, 4.2 us)
Async XLA Ops:
  0.0 135.5 %copy-start = (bf16[1,2048,176]{1,2,0:T(8,128)(2,1)S(1)}, bf16[1,2048,176]{1,2,0:T(8,128)(2,1)}, u32[]{:S(2)}) copy-start(bf16[1,2048,176]{1,2,0:T(8,128)(2,1)} %param.43) | copy-start | bytes 2162692
  1.7 39.0 %all-to-all-start = ((bf16[16,24,512]{2,1,0:T(8,128)(2,1)}), bf16[16,24,512]{2,1,0:T(8,128)(2,1)S(1)}, u32[]{:S(2)}, u32[]{:S(2)}) async-start(bf16[16,24,512]{2,1,0:T(8,128)(2,1)} %message.1), calls=%async_computation | async-start | bytes 786432 | tf_op jit(solution)/shard_map/hold/all_to_all | solution.py:38
  16.4 3.9 %copy-start.1 = (f32[2048]{0:T(1024)S(1)}, f32[2048]{0:T(1024)}, u32[]{:S(2)}) copy-start(f32[2048]{0:T(1024)} %param.36) | copy-start | bytes 24580
  16.4 4.1 %copy-start.2 = (f32[2048]{0:T(1024)S(1)}, f32[2048]{0:T(1024)}, u32[]{:S(2)}) copy-start(f32[2048]{0:T(1024)} %param.24) | copy-start | bytes 24580
  23.0 22.5 %copy-start.5 = (s32[8]{0:T(128)S(1)}, s32[8]{0:T(128)}, u32[]{:S(2)}) copy-start(s32[8]{0:T(128)} %param.33) | copy-start | bytes 100
  23.0 28.1 %copy-start.4 = (f32[64]{0:T(128)S(1)}, f32[64]{0:T(128)}, u32[]{:S(2)}) copy-start(f32[64]{0:T(128)} %param.28) | copy-start | bytes 772
  23.0 28.2 %copy-start.6 = (f32[64]{0:T(128)S(1)}, f32[64]{0:T(128)}, u32[]{:S(2)}) copy-start(f32[64]{0:T(128)} %param.29) | copy-start | bytes 772
  41.5 10.8 %copy-start.8 = (f32[2]{0:T(128)S(1)}, f32[2]{0:T(128)}, u32[]{:S(2)}) copy-start(f32[2]{0:T(128)} %param.30) | copy-start | bytes 28
  41.5 11.2 %copy-start.10 = (bf16[8,1,320,128]{3,2,1,0:T(8,128)(2,1)S(1)}, bf16[8,1,320,128]{3,2,1,0:T(8,128)(2,1)}, u32[]{:S(2)}) copy-start(bf16[8,1,320,128]{3,2,1,0:T(8,128)(2,1)} %param.32) | copy-start | bytes 1966084
  41.5 9.2 %all-to-all-start.1 = ((f32[8,8,512]{2,1,0:T(8,128)}), f32[8,8,512]{2,1,0:T(8,128)S(1)}, u32[]{:S(2)}, u32[]{:S(2)}) async-start(f32[8,8,512]{2,1,0:T(8,128)} %fusion.14), calls=%async_computation.1 | async-start | bytes 262144 | tf_op jit(solution)/shard_map/project/all_to_all | solution.py:38
  50.6 2.5 %copy-start.7 = (f32[128]{0:T(128)S(1)}, f32[128]{0:T(128)}, u32[]{:S(2)}) copy-start(f32[128]{0:T(128)} %param.34) | copy-start | bytes 1540
  62.9 29.8 %copy-start.3 = (f32[2048]{0:T(1024)S(1)}, f32[2048]{0:T(1024)}, u32[]{:S(2)}) copy-start(f32[2048]{0:T(1024)} %param.40) | copy-start | bytes 24580
  78.4 36.7 %all-to-all-start.4 = ((bf16[128,2,512]{2,1,0:T(2,128)(2,1)}), bf16[128,2,512]{2,1,0:T(2,128)(2,1)S(1)}, u32[]{:S(2)}, u32[]{:S(2)}) async-start(bf16[128,2,512]{2,1,0:T(2,128)(2,1)} %bitcast.35), calls=%async_computation.4 | async-start | bytes 524288 | tf_op jit(solution)/shard_map/route/all_to_all | solution.py:38
  116.5 18.4 %all-to-all-start.5 = ((bf16[4,256,512]{1,2,0:T(8,128)(2,1)}), bf16[4,256,512]{1,2,0:T(8,128)(2,1)S(1)}, u32[]{:S(2)}, u32[]{:S(2)}) async-start(bf16[4,256,512]{1,2,0:T(8,128)(2,1)} %broadcast_in_dim.31), calls=%async_computation.5 | async-start | bytes 2097152 | tf_op jit(solution)/shard_map/join/all_to_all | solution.py:38
  135.2 1.1 copy-start.9

commit v9 on v8

--- a/solution.py
+++ b/solution.py
@@ -240,9 +240,9 @@
         )
     )
     partial_rows = jnp.dot(spread, held, preferred_element_type=jnp.float32)
+    partial_rows, key_cache = lax.optimization_barrier((partial_rows, key_cache))
     with jax.named_scope("project"):
         packed = exchange(partial_rows.reshape(N_XC, SEQ, 512), XC)
-        packed, extra = lax.optimization_barrier((packed, extra))
         packed = jnp.sum(packed, axis=0)
     head_out = attend(
         packed, key_cache, value_cache, lengths, query_gain, key_gain, lambdas, head_gain
@@ -250,6 +250,7 @@
     head_out, tp_start = lax.optimization_barrier((head_out, tp_start))
     with jax.named_scope("heads"):
         all_heads = gather_small(head_out, XC, N_XC).reshape(N_XC * SEQ, 256)
+    all_heads, extra = lax.optimization_barrier((all_heads, extra))
     attended_part = lax.dot_general(
         all_heads, extra[:, :256], (((1,), (1,)), ((), ())), preferred_element_type=jnp.float32
     ).astype(jnp.bfloat16)

time: 188 us -> 187 us (level)
  blocking collectives: 105 us -> 97.3 us
  waiting for transfers between devices: 20.6 us -> 26.2 us
  starting transfers between devices: 36.3 us -> 38.4 us
    all_to_all x4 -> x3, blocking collectives: 71.4 us -> 63.7 us  [exchange(): return lax.all_to_all(values, axes, split_axis=0, concat_axis=0, tiled=True)]
    all_to_all x4 -> x5, waiting for transfers between devices: 20.6 us -> 26.2 us  [exchange(): return lax.all_to_all(values, axes, split_axis=0, concat_axis=0, tiled=True)]
    all_to_all x4 -> x5, starting transfers between devices: 36.3 us -> 38.4 us  [exchange(): return lax.all_to_all(values, axes, split_axis=0, concat_axis=0, tiled=True)]
  transfers between devices with their start and end apart: 4 -> 5, of which waited for: 3 -> 4; matrix products, arithmetic and copies ran while one was open for 7% -> 5% of each run, Pallas kernels for 0% -> 0%
where the time goes in v9:
time: 187 us; the launch traced here: 186 us
  blocking collectives  97.3 us (52%)
  starting transfers between devices  38.4 us (21%)
  waiting for transfers between devices  26.2 us (14%)
  local copies, waits for them, and re-layouts  9.76 us (5%)
  other arithmetic  7.42 us (4%)
  matrix products  5.16 us (3%)
    all_to_all x3, blocking collectives, exchange(): return lax.all_to_all(values, axes, split_axis=0, concat_axis=0, tiled=True)  63.7 us
    all_to_all x5, starting transfers between devices, exchange(): return lax.all_to_all(values, axes, split_axis=0, concat_axis=0, tiled=True)  38.4 us
    all_to_all x5, waiting for transfers between devices, exchange(): return lax.all_to_all(values, axes, split_axis=0, concat_axis=0, tiled=True)  26.2 us
    all_gather x1, blocking collectives, shards(): spread = lax.all_gather(normed, XC, axis=0)  14.2 us
    all_gather x1, blocking collectives, shards(): lax.all_gather(extra[:, 256:], XC, axis=0).reshape(N_XC, N_Z, 16, 128)  13.9 us
    all_gather x1, blocking collectives, shards(): lax.all_gather(held[:, 16:, :384], 'zp', axis=1).reshape(N_Z * 16, 384)  5.5 us
  transfers between devices with their start and end apart: 5, of which 4 were waited for; matrix products, arithmetic and copies ran while one was open for 5% of the time, Pallas kernels for 0%

profile of v9, /device:TPU:33, one launch (start us, length us, event | category | flops | bytes accessed | tf_op | source)
XLA Modules:
  0.0 186.4 jit_solution(16874243171070856214)
XLA Ops:
  0.0 1.7 message.1
  1.7 14.7 %all-to-all-start = ((bf16[16,24,512]{2,1,0:T(8,128)(2,1)}), bf16[16,24,512]{2,1,0:T(8,128)(2,1)S(1)}, u32[]{:S(2)}, u32[]{:S(2)}) async-start(bf16[16,24,512]{2,1,0:T(8,128)(2,1)} %message.1), calls=%async_computation | async-start | bytes 786432 | tf_op jit(solution)/shard_map/hold/all_to_all | solution.py:38
  16.4 0.8 copy.84
  17.2 1.0 reshape.416
  18.3 0.2 reshape.410
  18.6 0.2 reshape.411
  19.9 14.2 %all_gather.16 = bf16[8,8,8,256]{3,2,1,0:T(8,128)(2,1)S(1)} all-gather(bf16[1,8,8,256]{3,2,1,0:T(8,128)(2,1)S(1)} %multiply_convert_fusion.3), channel_id=1, replica_groups=mesh['b'=8,'zp'=2,'x'=4,'c'=2,'tp'=4] {'x','c'}, dimensions={0}, use_global_device_ids=true | all-gather | bytes 294912 | tf_op jit(solution)/shard_map/spread/all_gather | solution.py:230
  34.2 0.7 iota_compare_fusion
  34.9 2.5 %all-to-all-done = bf16[16,24,512]{2,1,0:T(8,128)(2,1)S(1)} async-done(((bf16[16,24,512]{2,1,0:T(8,128)(2,1)}), bf16[16,24,512]{2,1,0:T(8,128)(2,1)S(1)}, u32[]{:S(2)}, u32[]{:S(2)}) %all-to-all-start) | async-done | bytes 393248 | tf_op jit(solution)/shard_map/hold/all_to_all | solution.py:38
  37.4 0.8 fusion.20
  38.2 6.3 %all-to-all-start.1 = ((f32[8,8,512]{2,1,0:T(8,128)}), f32[8,8,512]{2,1,0:T(8,128)}, u32[]{:S(2)}, u32[]{:S(2)}) async-start(f32[8,8,512]{2,1,0:T(8,128)} %bitcast.12), calls=%async_computation.1 | async-start | bytes 262144 | tf_op jit(solution)/shard_map/project/all_to_all | solution.py:38
  44.6 0.4 copy.90
  45.1 0.7 reduce_sum.157
  45.8 0.8 add_rsqrt_fusion
  46.7 3.2 %all-to-all-done.1 = f32[8,8,512]{2,1,0:T(8,128)} async-done(((f32[8,8,512]{2,1,0:T(8,128)}), f32[8,8,512]{2,1,0:T(8,128)}, u32[]{:S(2)}, u32[]{:S(2)}) %all-to-all-start.1) | async-done | bytes 131104 | tf_op jit(solution)/shard_map/project/all_to_all | solution.py:38
  49.9 0.9 reduce_sum.158
  51.2 0.7 multiply_convert_fusion.4
  51.9 1.1 fusion.44
  54.1 0.4 multiply_reduce_fusion.3
  54.6 0.6 broadcast_in_dim.26
  55.2 4.1 %all-to-all-start.2 = ((bf16[8,8,256]{2,1,0:T(8,128)(2,1)}), bf16[8,8,256]{2,1,0:T(8,128)(2,1)S(1)}, u32[]{:S(2)}, u32[]{:S(2)}) async-start(bf16[8,8,256]{2,1,0:T(8,128)(2,1)} %broadcast_in_dim.26), calls=%async_computation.2 | async-start | bytes 65536 | tf_op jit(solution)/shard_map/heads/all_to_all | solution.py:38
  59.3 5.5 %all-gather = bf16[16,16,384]{2,1,0:T(8,128)(2,1)S(1)} all-gather(bf16[16,8,384]{2,1,0:T(8,128)(2,1)S(1)} %slice.79), channel_id=2, replica_groups=mesh['b'=8,'zp'=2,'x'=4,'c'=2,'tp'=4] {'zp'}, dimensions={1}, use_global_device_ids=true | all-gather | bytes 294912 | tf_op jit(solution)/shard_map/halves/all_gather | solution.py:225
  65.0 15.3 %all_to_all.40 = bf16[32,8,256]{2,1,0:T(8,128)(2,1)S(1)} all-to-all(bf16[32,8,256]{2,1,0:T(8,128)(2,1)S(1)} %bitcast.180), channel_id=1, replica_groups=mesh['b'=8,'zp'=2,'x'=4,'c'=2,'tp'=4] {'x','c','tp'}, dimensions={0} | all-to-all | bytes 262144 | tf_op jit(solution)/shard_map/attended/all_to_all | solution.py:38
  80.6 0.2 reshape.401
  81.0 0.3 reshape.402
  81.3 0.2 convolution_convert_fusion.1
  81.5 0.8 broadcast_in_dim.30
  82.3 9.8 %all-to-all-start.4 = ((bf16[128,2,512]{2,1,0:T(2,128)(2,1)}), bf16[128,2,512]{2,1,0:T(2,128)(2,1)S(1)}, u32[]{:S(2)}, u32[]{:S(2)}) async-start(bf16[128,2,512]{2,1,0:T(2,128)(2,1)} %bitcast.34), calls=%async_computation.4 | async-start | bytes 524288 | tf_op jit(solution)/shard_map/route/all_to_all | solution.py:38
  92.2 13.9 %all-gather.1 = bf16[2048,128]{1,0:T(8,128)(2,1)S(1)} all-gather(bf16[256,128]{1,0:T(8,128)(2,1)S(1)} %slice.64), channel_id=3, replica_groups=mesh['b'=8,'zp'=2,'x'=4,'c'=2,'tp'=4] {'x','c'}, dimensions={0}, use_global_device_ids=true | all-gather | bytes 589824 | tf_op jit(solution)/shard_map/dense/all_gather | solution.py:282
  106.2 0.3 copy.102
  106.5 0.3 reshape.414
  106.8 7.9 %all-to-all-done.4 = bf16[128,2,512]{2,1,0:T(2,128)(2,1)S(1)} async-done(((bf16[128,2,512]{2,1,0:T(2,128)(2,1)}), bf16[128,2,512]{2,1,0:T(2,128)(2,1)S(1)}, u32[]{:S(2)}, u32[]{:S(2)}) %all-to-all-start.4) | async-done | bytes 262176 | tf_op jit(solution)/shard_map/route/all_to_all | solution.py:38
  114.9 1.1 broadcast_in_dim.31
  116.0 3.5 %all-to-all-start.5 = ((bf16[4,256,512]{1,2,0:T(8,128)(2,1)}), bf16[4,256,512]{1,2,0:T(8,128)(2,1)S(1)}, u32[]{:S(2)}, u32[]{:S(2)}) async-start(bf16[4,256,512]{1,2,0:T(8,128)(2,1)} %broadcast_in_dim.31), calls=%async_computation.5 | async-start | bytes 2097152 | tf_op jit(solution)/shard_map/join/all_to_all | solution.py:38
  119.6 0.2 slice_bitcast_fusion
  120.0 0.4 convert_reduce_fusion.1
  120.7 1.2 pad_maximum_fusion
  121.8 12.5 %all-to-all-done.5 = bf16[4,256,512]{1,2,0:T(8,128)(2,1)S(1)} async-done(((bf16[4,256,512]{1,2,0:T(8,128)(2,1)}), bf16[4,256,512]{1,2,0:T(8,128)(2,1)S(1)}, u32[]{:S(2)}, u32[]{:S(2)}) %all-to-all-start.5) | async-done | bytes 1048608 | tf_op jit(solution)/shard_map/join/all_to_all | solution.py:38
  134.4 0.3 multiply_reduce_fusion
  134.7 0.3 fusion.46
  135.0 0.4 convolution_bitcast_fusion.1
  135.4 0.4 copy-done.11
  135.8 0.4 fusion.1
  136.2 0.5 convolution_convert_fusion
  136.8 16.6 %all_to_all.41 = bf16[4,256,512]{2,1,0:T(8,128)(2,1)S(1)} all-to-all(bf16[4,256,512]{2,1,0:T(8,128)(2,1)S(1)} %bitcast.170), channel_id=1, replica_groups=mesh['b'=8,'zp'=2,'x'=4,'c'=2,'tp'=4] {'tp'}, dimensions={0} | all-to-all | bytes 2097152 | tf_op jit(solution)/shard_map/reduce/all_to_all | solution.py:38
  153.4 0.2 reduce_sum.170
  153.7 31.8 %all_to_all.42 = bf16[128,2,512]{2,1,0:T(2,128)(2,1)S(1)} all-to-all(bf16[128,2,512]{2,1,0:T(2,128)(2,1)S(1)} %reshape.409), channel_id=1, replica_groups=mesh['b'=8,'zp'=2,'x'=4,'c'=2,'tp'=4] {'b','zp','x','c'}, dimensions={0} | all-to-all | bytes 524288 | tf_op jit(solution)/shard_map/return/all_to_all | solution.py:38
  185.6 0.8 fusion.5
  (98 shorter events, 4.7 us)
Async XLA Ops:
  0.0 135.0 %copy-start = (bf16[1,2048,176]{1,2,0:T(8,128)(2,1)S(1)}, bf16[1,2048,176]{1,2,0:T(8,128)(2,1)}, u32[]{:S(2)}) copy-start(bf16[1,2048,176]{1,2,0:T(8,128)(2,1)} %param.43) | copy-start | bytes 2162692
  1.7 35.7 %all-to-all-start = ((bf16[16,24,512]{2,1,0:T(8,128)(2,1)}), bf16[16,24,512]{2,1,0:T(8,128)(2,1)S(1)}, u32[]{:S(2)}, u32[]{:S(2)}) async-start(bf16[16,24,512]{2,1,0:T(8,128)(2,1)} %message.1), calls=%async_computation | async-start | bytes 786432 | tf_op jit(solution)/shard_map/hold/all_to_all | solution.py:38
  16.4 2.9 %copy-start.3 = (f32[2048]{0:T(1024)S(1)}, f32[2048]{0:T(1024)}, u32[]{:S(2)}) copy-start(f32[2048]{0:T(1024)} %param.36) | copy-start | bytes 24580
  16.4 3.1 %copy-start.4 = (f32[2048]{0:T(1024)S(1)}, f32[2048]{0:T(1024)}, u32[]{:S(2)}) copy-start(f32[2048]{0:T(1024)} %param.24) | copy-start | bytes 24580
  17.1 2.5 %copy-start.2 = (bf16[8,2048]{1,0:T(8,128)(2,1)S(1)}, bf16[8,2048]{1,0:T(8,128)(2,1)}, u32[]{:S(2)}) copy-start(bf16[8,2048]{1,0:T(8,128)(2,1)} %param.23) | copy-start | bytes 98308
  18.2 15.9 %copy-start.6 = (f32[8,2]{0,1:T(2,128)S(1)}, f32[8,2]{0,1:T(2,128)}, u32[]{:S(2)}) copy-start(f32[8,2]{0,1:T(2,128)} %param.42) | copy-start | bytes 196
  18.2 16.0 %copy-start.7 = (s32[8]{0:T(128)S(1)}, s32[8]{0:T(128)}, u32[]{:S(2)}) copy-start(s32[8]{0:T(128)} %param.33) | copy-start | bytes 100
  18.6 26.0 %copy-start.1 = (bf16[8,1,320,128]{3,2,1,0:T(8,128)(2,1)S(1)}, bf16[8,1,320,128]{3,2,1,0:T(8,128)(2,1)}, u32[]{:S(2)}) copy-start(bf16[8,1,320,128]{3,2,1,0:T(8,128)(2,1)} %param.31) | copy-start | bytes 1966084
  38.2 11.7 %all-to-all-start.1 = ((f32[8,8,512]{2,1,0:T(8,128)}), f32[8,8,512]{2,1,0:T(8,128)}, u32[]{:S(2)}, u32[]{:S(2)}) async-start(f32[8,8,512]{2,1,0:T(8,128)} %bitcast.12), calls=%async_computation.1 | async-start | bytes 262144 | tf_op jit(solution)/shard_map/project/all_to_all | solution.py:38
  45.8 7.6 %copy-start.8 = (f32[64]{0:T(128)S(1)}, f32[64]{0:T(128)}, u32[]{:S(2)}) copy-start(f32[64]{0:T(128)} %param.29) | copy-start | bytes 772
  45.8 7.9 %copy-start.10 = (f32[2]{0:T(128)S(1)}, f32[2]{0:T(128)}, u32[]{:S(2)}) copy-start(f32[2]{0:T(128)} %param.30) | copy-start | bytes 28
  45.8 8.3 %copy-start.12 = (bf16[8,1,320,128]{3,2,1,0:T(8,128)(2,1)S(1)}, bf16[8,1,320,128]{3,2,1,0:T(8,128)(2,1)}, u32[]{:S(2)}) copy-start(bf16[8,1,320,128]{3,2,1,0:T(8,128)(2,1)} %param.32) | copy-start | bytes 1966084
  45.8 8.7 %copy-start.9 = (f32[128]{0:T(128)S(1)}, f32[128]{0:T(128)}, u32[]{:S(2)}) copy-start(f32[128]{0:T(128)} %param.34) | copy-start | bytes 1540
  55.2 9.6 %all-to-all-start.2 = ((bf16[8,8,256]{2,1,0:T(8,128)(2,1)}), bf16[8,8,256]{2,1,0:T(8,128)(2,1)S(1)}, u32[]{:S(2)}, u32[]{:S(2)}) async-start(bf16[8,8,256]{2,1,0:T(8,128)(2,1)} %broadcast_in_dim.26), calls=%async_computation.2 | async-start | bytes 65536 | tf_op jit(solution)/shard_map/heads/all_to_all | solution.py:38
  64.8 27.3 %copy-start.5 = (f32[2048]{0:T(1024)S(1)}, f32[2048]{0:T(1024)}, u32[]{:S(2)}) copy-start(f32[2048]{0:T(1024)} %param.40) | copy-start | bytes 24580
  82.3 32.3 %all-to-all-start.4 = ((bf16[128,2,512]{2,1,0:T(2,128)(2,1)}), bf16[128,2,512]{2,1,0:T(2,128)(2,1)S(1)}, u32[]{:S(2)}, u32[]{:S(2)}) async-start(bf16[128,2,512]{2,1,0:T(2,128)(2,1)} %bitcast.34), calls=%async_computation.4 | async-start | bytes 524288 | tf_op jit(solution)/shard_map/route/all_to_all | solution.py:38
  116.0 18.4 %all-to-all-start.5 = ((bf16[4,256,512]{1,2,0:T(8,128)(2,1)}), bf16[4,256,512]{1,2,0:T(8,128)(2,1)S(1)}, u32[]{:S(2)}, u32[]{:S(2)}) async-start(bf16[4,256,512]{1,2,0:T(8,128)(2,1)} %broadcast_in_dim.31), calls=%async_computation.5 | async-start | bytes 2097152 | tf_op jit(solution)/shard_map/join/all_to_all | solution.py:38
  134.7 1.1 copy-start.11

commit v10 on v9

--- a/solution.py
+++ b/solution.py
@@ -127,9 +127,8 @@
     lanes = lax.broadcasted_iota(jnp.int32, (16, 256), 1)
     narrow = lax.broadcasted_iota(jnp.int32, (16, 128), 1)
     places = lax.broadcasted_iota(jnp.int32, (16, 128), 0)
-    shared = jnp.concatenate((query[...], key[...], value[...]), axis=1)
+    shared = jnp.concatenate((query[...], key[...], value[...], out[...]), axis=1)
     wide = [part[...].astype(jnp.float32) for part in (gate, up, down)]
-    held = out[...].astype(jnp.float32)
     tags = [jnp.zeros((16, 128), jnp.float32) for _ in range(2)]
     for row in range(SEQ):
         chosen = ids[0, row]
@@ -140,13 +139,13 @@
         slot = chosen * CAP + rank
         for half in range(2):
             tags[half] = jnp.where(places + 16 * half == slot, probs[0, row], tags[half])
-    tagged = jnp.zeros((16, 128), jnp.float32)
     for half in range(2):
         used = tags[half] > 0.0
         inverse = jnp.where(used, 1.0 / jnp.where(used, tags[half], 1.0), 0.0)
         high = inverse.astype(jnp.bfloat16).astype(jnp.float32)
-        tagged = jnp.where(narrow == 96 + 2 * half, high, tagged)
-        tagged = jnp.where(narrow == 97 + 2 * half, inverse - high, tagged)
+        tags[half] = jnp.where(
+            narrow == 96, high, jnp.where(narrow == 97, inverse - high, 0.0)
+        )
     for rep in range(REP):
         turned = [
             pltpu.roll(part, (32 * (place - rep)) % 256, 1) for place, part in enumerate(wide)
@@ -154,11 +153,10 @@
         own = jnp.where(
             lanes < 32, turned[0], jnp.where(lanes < 64, turned[1], turned[2])
         )[:, :128]
-        own = jnp.where(narrow < 96, own, tagged)
-        extra = jnp.concatenate((held, own, jnp.zeros((16, 128), jnp.float32)), axis=1)
+        own = jnp.where(narrow < 96, own, 0.0)
         for half in range(2):
-            message[2 * rep + half, :16, :] = shared
-            message[2 * rep + half, 16:, :] = extra[8 * half : 8 * half + 8].astype(jnp.bfloat16)
+            message[2 * rep + half, :, :768] = shared
+            message[2 * rep + half, :, 768:] = (own + tags[half]).astype(jnp.bfloat16)
 
 
 def build_message(ids, probs, *parts):
@@ -167,7 +165,7 @@
     return pl.pallas_call(
         message_body,
         in_specs=[scalars, scalars] + [whole] * len(parts),
-        out_shape=jax.ShapeDtypeStruct((N_Z, 24, 512), jnp.bfloat16),
+        out_shape=jax.ShapeDtypeStruct((N_Z, 16, 896), jnp.bfloat16),
         name="message",
     )(ids, probs, *parts)
 
@@ -221,8 +219,8 @@
     )
     with jax.named_scope("hold"):
         held = exchange(message, Z)
-    with jax.named_scope("halves"):
-        extra = lax.all_gather(held[:, 16:, :384], "zp", axis=1).reshape(N_Z * 16, 384)
+    held = held.reshape(N_Z * 16, 896)
+    held, extra = held[:, :512], held[:, 512:]
     residual = to_mixed(tokens).astype(jnp.float32)
     normed = mixed_scale(residual, to_mixed(norm_gain[None])).astype(jnp.bfloat16)
     xc_index = lax.axis_index(XC)
@@ -232,7 +230,7 @@
 
     held, select, combine_weights, ffn_scaling, residual = lax.optimization_barrier(
         (
-            held[:, :16].reshape(N_Z * 16, 512),
+            held,
             select.astype(jnp.bfloat16).T,
             combine_weights,
             to_mixed(ffn_gain[None]),
@@ -250,7 +248,6 @@
     head_out, tp_start = lax.optimization_barrier((head_out, tp_start))
     with jax.named_scope("heads"):
         all_heads = gather_small(head_out, XC, N_XC).reshape(N_XC * SEQ, 256)
-    all_heads, extra = lax.optimization_barrier((all_heads, extra))
     attended_part = lax.dot_general(
         all_heads, extra[:, :256], (((1,), (1,)), ((), ())), preferred_element_type=jnp.float32
     ).astype(jnp.bfloat16)
@@ -281,8 +278,7 @@
     with jax.named_scope("dense"):
         dense_held = lax.all_gather(extra[:, 256:], XC, axis=0).reshape(N_XC, N_Z, 16, 128)
     incoming, dense_held = lax.optimization_barrier((incoming, dense_held))
-    tag = lax.dynamic_slice_in_dim(dense_held, 2 * xc_index, CAP, 2)[..., 96:100]
-    tag = jnp.where(lax.axis_index("zp") == 0, tag[..., :2], tag[..., 2:])
+    tag = lax.dynamic_slice_in_dim(dense_held, 2 * xc_index, CAP, 2)[..., 96:98]
     tag = jnp.sum(tag.transpose(1, 0, 2, 3).reshape(N_EP * CAP, 2).astype(jnp.float32), axis=1)
     dense_held = dense_held.transpose(1, 0, 2, 3).reshape(width, 128)
     down = jnp.concatenate((expert_down[0], dense_held[:, 64:96].T), axis=0)

time: 187 us -> 186 us (level)
  starting transfers between devices: 38.4 us -> 35.6 us
    all_to_all x3 -> x4, blocking collectives: 63.7 us -> 69.5 us  [exchange(): return lax.all_to_all(values, axes, split_axis=0, concat_axis=0, tiled=True)]
    all_gather x1 -> x0, blocking collectives: 5.5 us -> none  [shards(): lax.all_gather(held[:, 16:, :384], 'zp', axis=1).reshape(N_Z * 16, 384)]
    all_to_all x5 -> x4, starting transfers between devices: 38.4 us -> 35.6 us  [exchange(): return lax.all_to_all(values, axes, split_axis=0, concat_axis=0, tiled=True)]
    all_to_all x5 -> x4, waiting for transfers between devices: 26.2 us -> 27.5 us  [exchange(): return lax.all_to_all(values, axes, split_axis=0, concat_axis=0, tiled=True)]
  transfers between devices with their start and end apart: 5 -> 4, of which waited for: 4 -> 4; matrix products, arithmetic and copies ran while one was open for 5% -> 5% of each run, Pallas kernels for 0% -> 0%
where the time goes in v10:
time: 186 us; the launch traced here: 185 us
  blocking collectives  97.6 us (52%)
  starting transfers between devices  35.6 us (19%)
  waiting for transfers between devices  27.5 us (15%)
  local copies, waits for them, and re-layouts  9.75 us (5%)
  other arithmetic  7.33 us (4%)
  matrix products  5.19 us (3%)
    all_to_all x4, blocking collectives, exchange(): return lax.all_to_all(values, axes, split_axis=0, concat_axis=0, tiled=True)  69.5 us
    all_to_all x4, starting transfers between devices, exchange(): return lax.all_to_all(values, axes, split_axis=0, concat_axis=0, tiled=True)  35.6 us
    all_to_all x4, waiting for transfers between devices, exchange(): return lax.all_to_all(values, axes, split_axis=0, concat_axis=0, tiled=True)  27.5 us
    all_gather x1, blocking collectives, shards(): spread = lax.all_gather(normed, XC, axis=0)  14.2 us
    all_gather x1, blocking collectives, shards(): lax.all_gather(extra[:, 256:], XC, axis=0).reshape(N_XC, N_Z, 16, 128)  13.9 us
  transfers between devices with their start and end apart: 4, of which 4 were waited for; matrix products, arithmetic and copies ran while one was open for 5% of the time, Pallas kernels for 0%

profile of v10, /device:TPU:33, one launch (start us, length us, event | category | flops | bytes accessed | tf_op | source)
XLA Modules:
  0.0 185.2 jit_solution(5163243467648755660)
XLA Ops:
  0.0 1.7 message.1
  1.8 14.7 %all-to-all-start = ((bf16[16,16,896]{2,1,0:T(8,128)(2,1)}), bf16[16,16,896]{2,1,0:T(8,128)(2,1)S(1)}, u32[]{:S(2)}, u32[]{:S(2)}) async-start(bf16[16,16,896]{2,1,0:T(8,128)(2,1)} %message.1), calls=%async_computation | async-start | bytes 917504 | tf_op jit(solution)/shard_map/hold/all_to_all | solution.py:38
  16.4 0.8 copy.84
  17.2 1.0 reshape.412
  18.4 0.9 reshape.406
  19.2 0.2 reshape.407
  20.5 14.2 %all_gather.10 = bf16[8,8,8,256]{3,2,1,0:T(8,128)(2,1)S(1)} all-gather(bf16[1,8,8,256]{3,2,1,0:T(8,128)(2,1)S(1)} %multiply_convert_fusion.3), channel_id=1, replica_groups=mesh['b'=8,'zp'=2,'x'=4,'c'=2,'tp'=4] {'x','c'}, dimensions={0}, use_global_device_ids=true | all-gather | bytes 294912 | tf_op jit(solution)/shard_map/spread/all_gather | solution.py:228
  34.9 0.7 iota_compare_fusion
  35.5 3.7 %all-to-all-done = bf16[16,16,896]{2,1,0:T(8,128)(2,1)S(1)} async-done(((bf16[16,16,896]{2,1,0:T(8,128)(2,1)}), bf16[16,16,896]{2,1,0:T(8,128)(2,1)S(1)}, u32[]{:S(2)}, u32[]{:S(2)}) %all-to-all-start) | async-done | bytes 458784 | tf_op jit(solution)/shard_map/hold/all_to_all | solution.py:38
  39.3 0.8 fusion.21
  40.1 6.8 %all-to-all-start.1 = ((f32[8,8,512]{2,1,0:T(8,128)}), f32[8,8,512]{2,1,0:T(8,128)}, u32[]{:S(2)}, u32[]{:S(2)}) async-start(f32[8,8,512]{2,1,0:T(8,128)} %bitcast.12), calls=%async_computation.1 | async-start | bytes 262144 | tf_op jit(solution)/shard_map/project/all_to_all | solution.py:38
  46.9 0.4 copy.90
  47.4 0.7 reduce_sum.157
  48.2 0.8 add_rsqrt_fusion
  49.0 3.3 %all-to-all-done.1 = f32[8,8,512]{2,1,0:T(8,128)} async-done(((f32[8,8,512]{2,1,0:T(8,128)}), f32[8,8,512]{2,1,0:T(8,128)}, u32[]{:S(2)}, u32[]{:S(2)}) %all-to-all-start.1) | async-done | bytes 131104 | tf_op jit(solution)/shard_map/project/all_to_all | solution.py:38
  52.3 0.9 reduce_sum.158
  53.5 0.7 multiply_convert_fusion.4
  54.3 1.2 fusion.45
  56.5 0.3 multiply_reduce_fusion.3
  57.0 7.9 %all_to_all.40 = bf16[8,8,256]{2,1,0:T(8,128)(2,1)S(1)} all-to-all(bf16[8,8,256]{2,1,0:T(8,128)(2,1)S(1)} %broadcast_in_dim.26), channel_id=1, replica_groups=mesh['b'=8,'zp'=2,'x'=4,'c'=2,'tp'=4] {'x','c'}, dimensions={0} | all-to-all | bytes 65536 | tf_op jit(solution)/shard_map/heads/all_to_all | solution.py:38
  65.2 13.3 %all_to_all.41 = bf16[32,8,256]{2,1,0:T(8,128)(2,1)S(1)} all-to-all(bf16[32,8,256]{2,1,0:T(8,128)(2,1)S(1)} %bitcast.180), channel_id=1, replica_groups=mesh['b'=8,'zp'=2,'x'=4,'c'=2,'tp'=4] {'x','c','tp'}, dimensions={0} | all-to-all | bytes 262144 | tf_op jit(solution)/shard_map/attended/all_to_all | solution.py:38
  78.7 0.2 reshape.397
  79.0 0.2 copy.125
  79.2 0.3 reshape.398
  79.5 0.2 convolution_convert_fusion.1
  79.7 0.8 broadcast_in_dim.30
  80.5 10.6 %all-to-all-start.4 = ((bf16[128,2,512]{2,1,0:T(2,128)(2,1)}), bf16[128,2,512]{2,1,0:T(2,128)(2,1)S(1)}, u32[]{:S(2)}, u32[]{:S(2)}) async-start(bf16[128,2,512]{2,1,0:T(2,128)(2,1)} %bitcast.33), calls=%async_computation.4 | async-start | bytes 524288 | tf_op jit(solution)/shard_map/route/all_to_all | solution.py:38
  91.2 13.9 %all-gather = bf16[2048,128]{1,0:T(8,128)(2,1)S(1)} all-gather(bf16[256,128]{1,0:T(8,128)(2,1)S(1)} %slice.72), channel_id=2, replica_groups=mesh['b'=8,'zp'=2,'x'=4,'c'=2,'tp'=4] {'x','c'}, dimensions={0}, use_global_device_ids=true | all-gather | bytes 589824 | tf_op jit(solution)/shard_map/dense/all_gather | solution.py:279
  105.2 0.3 copy.102
  105.5 0.3 reshape.410
  105.8 7.9 %all-to-all-done.4 = bf16[128,2,512]{2,1,0:T(2,128)(2,1)S(1)} async-done(((bf16[128,2,512]{2,1,0:T(2,128)(2,1)}), bf16[128,2,512]{2,1,0:T(2,128)(2,1)S(1)}, u32[]{:S(2)}, u32[]{:S(2)}) %all-to-all-start.4) | async-done | bytes 262176 | tf_op jit(solution)/shard_map/route/all_to_all | solution.py:38
  113.9 1.1 broadcast_in_dim.31
  115.0 3.5 %all-to-all-start.5 = ((bf16[4,256,512]{1,2,0:T(8,128)(2,1)}), bf16[4,256,512]{1,2,0:T(8,128)(2,1)S(1)}, u32[]{:S(2)}, u32[]{:S(2)}) async-start(bf16[4,256,512]{1,2,0:T(8,128)(2,1)} %broadcast_in_dim.31), calls=%async_computation.5 | async-start | bytes 2097152 | tf_op jit(solution)/shard_map/join/all_to_all | solution.py:38
  118.7 0.2 slice_bitcast_fusion
  118.9 0.2 copy.100
  119.0 0.3 convert_reduce_fusion.1
  119.6 1.2 pad_maximum_fusion
  120.7 12.6 %all-to-all-done.5 = bf16[4,256,512]{1,2,0:T(8,128)(2,1)S(1)} async-done(((bf16[4,256,512]{1,2,0:T(8,128)(2,1)}), bf16[4,256,512]{1,2,0:T(8,128)(2,1)S(1)}, u32[]{:S(2)}, u32[]{:S(2)}) %all-to-all-start.5) | async-done | bytes 1048608 | tf_op jit(solution)/shard_map/join/all_to_all | solution.py:38
  133.4 0.3 multiply_reduce_fusion
  133.7 0.3 fusion.47
  134.0 0.4 convolution_bitcast_fusion.1
  134.5 0.4 copy-done.12
  134.8 0.4 fusion.1
  135.2 0.5 convolution_convert_fusion
  135.8 16.4 %all_to_all.42 = bf16[4,256,512]{2,1,0:T(8,128)(2,1)S(1)} all-to-all(bf16[4,256,512]{2,1,0:T(8,128)(2,1)S(1)} %bitcast.170), channel_id=1, replica_groups=mesh['b'=8,'zp'=2,'x'=4,'c'=2,'tp'=4] {'tp'}, dimensions={0} | all-to-all | bytes 2097152 | tf_op jit(solution)/shard_map/reduce/all_to_all | solution.py:38
  152.2 0.2 reduce_sum.170
  152.6 31.8 %all_to_all.43 = bf16[128,2,512]{2,1,0:T(2,128)(2,1)S(1)} all-to-all(bf16[128,2,512]{2,1,0:T(2,128)(2,1)S(1)} %reshape.405), channel_id=1, replica_groups=mesh['b'=8,'zp'=2,'x'=4,'c'=2,'tp'=4] {'b','zp','x','c'}, dimensions={0} | all-to-all | bytes 524288 | tf_op jit(solution)/shard_map/return/all_to_all | solution.py:38
  184.5 0.8 fusion.5
  (97 shorter events, 4.3 us)
Async XLA Ops:
  0.0 134.0 %copy-start = (bf16[1,2048,176]{1,2,0:T(8,128)(2,1)S(1)}, bf16[1,2048,176]{1,2,0:T(8,128)(2,1)}, u32[]{:S(2)}) copy-start(bf16[1,2048,176]{1,2,0:T(8,128)(2,1)} %param.43) | copy-start | bytes 2162692
  1.8 37.5 %all-to-all-start = ((bf16[16,16,896]{2,1,0:T(8,128)(2,1)}), bf16[16,16,896]{2,1,0:T(8,128)(2,1)S(1)}, u32[]{:S(2)}, u32[]{:S(2)}) async-start(bf16[16,16,896]{2,1,0:T(8,128)(2,1)} %message.1), calls=%async_computation | async-start | bytes 917504 | tf_op jit(solution)/shard_map/hold/all_to_all | solution.py:38
  16.4 3.5 %copy-start.4 = (f32[2048]{0:T(1024)S(1)}, f32[2048]{0:T(1024)}, u32[]{:S(2)}) copy-start(f32[2048]{0:T(1024)} %param.36) | copy-start | bytes 24580
  16.4 3.7 %copy-start.5 = (f32[2048]{0:T(1024)S(1)}, f32[2048]{0:T(1024)}, u32[]{:S(2)}) copy-start(f32[2048]{0:T(1024)} %param.24) | copy-start | bytes 24580
  17.2 3.1 %copy-start.3 = (bf16[8,2048]{1,0:T(8,128)(2,1)S(1)}, bf16[8,2048]{1,0:T(8,128)(2,1)}, u32[]{:S(2)}) copy-start(bf16[8,2048]{1,0:T(8,128)(2,1)} %param.23) | copy-start | bytes 98308
  18.2 16.5 %copy-start.7 = (f32[8,2]{0,1:T(2,128)S(1)}, f32[8,2]{0,1:T(2,128)}, u32[]{:S(2)}) copy-start(f32[8,2]{0,1:T(2,128)} %param.42) | copy-start | bytes 196
  18.3 16.6 %copy-start.8 = (s32[8]{0:T(128)S(1)}, s32[8]{0:T(128)}, u32[]{:S(2)}) copy-start(s32[8]{0:T(128)} %param.33) | copy-start | bytes 100
  19.2 27.7 %copy-start.1 = (bf16[8,1,320,128]{3,2,1,0:T(8,128)(2,1)S(1)}, bf16[8,1,320,128]{3,2,1,0:T(8,128)(2,1)}, u32[]{:S(2)}) copy-start(bf16[8,1,320,128]{3,2,1,0:T(8,128)(2,1)} %param.31) | copy-start | bytes 1966084
  40.1 12.2 %all-to-all-start.1 = ((f32[8,8,512]{2,1,0:T(8,128)}), f32[8,8,512]{2,1,0:T(8,128)}, u32[]{:S(2)}, u32[]{:S(2)}) async-start(f32[8,8,512]{2,1,0:T(8,128)} %bitcast.12), calls=%async_computation.1 | async-start | bytes 262144 | tf_op jit(solution)/shard_map/project/all_to_all | solution.py:38
  48.2 7.6 %copy-start.9 = (f32[64]{0:T(128)S(1)}, f32[64]{0:T(128)}, u32[]{:S(2)}) copy-start(f32[64]{0:T(128)} %param.29) | copy-start | bytes 772
  48.2 8.0 %copy-start.11 = (f32[2]{0:T(128)S(1)}, f32[2]{0:T(128)}, u32[]{:S(2)}) copy-start(f32[2]{0:T(128)} %param.30) | copy-start | bytes 28
  48.2 8.4 %copy-start.13 = (bf16[8,1,320,128]{3,2,1,0:T(8,128)(2,1)S(1)}, bf16[8,1,320,128]{3,2,1,0:T(8,128)(2,1)}, u32[]{:S(2)}) copy-start(bf16[8,1,320,128]{3,2,1,0:T(8,128)(2,1)} %param.32) | copy-start | bytes 1966084
  48.2 8.7 %copy-start.10 = (f32[128]{0:T(128)S(1)}, f32[128]{0:T(128)}, u32[]{:S(2)}) copy-start(f32[128]{0:T(128)} %param.34) | copy-start | bytes 1540
  54.3 24.2 %copy-start.2 = (f32[8,8,256]{2,1,0:T(8,128)S(1)}, f32[8,8,256]{2,1,0:T(8,128)}, u32[]{:S(2)}) copy-start(f32[8,8,256]{2,1,0:T(8,128)} %reshape.406) | copy-start | bytes 196612
  64.9 26.2 %copy-start.6 = (f32[2048]{0:T(1024)S(1)}, f32[2048]{0:T(1024)}, u32[]{:S(2)}) copy-start(f32[2048]{0:T(1024)} %param.40) | copy-start | bytes 24580
  80.5 33.2 %all-to-all-start.4 = ((bf16[128,2,512]{2,1,0:T(2,128)(2,1)}), bf16[128,2,512]{2,1,0:T(2,128)(2,1)S(1)}, u32[]{:S(2)}, u32[]{:S(2)}) async-start(bf16[128,2,512]{2,1,0:T(2,128)(2,1)} %bitcast.33), calls=%async_computation.4 | async-start | bytes 524288 | tf_op jit(solution)/shard_map/route/all_to_all | solution.py:38
  115.0 18.4 %all-to-all-start.5 = ((bf16[4,256,512]{1,2,0:T(8,128)(2,1)}), bf16[4,256,512]{1,2,0:T(8,128)(2,1)S(1)}, u32[]{:S(2)}, u32[]{:S(2)}) async-start(bf16[4,256,512]{1,2,0:T(8,128)(2,1)} %broadcast_in_dim.31), calls=%async_computation.5 | async-start | bytes 2097152 | tf_op jit(solution)/shard_map/join/all_to_all | solution.py:38
  133.7 1.1 copy-start.12
